TPU v7x, 128 devices: a whole 4x4x4 slice. The times are simulated.
128 devices in a mesh: tp: 16 (over z, y), dp: 8 (over x, core).
Axes of the slice: x: 4, y: 4, z: 4, core: 2. Of those that a mesh axis runs over, the one named last changes fastest.
Arguments:
- tokens: bfloat16 [256, 4096], P('dp', 'tp'), may hold values from -6 to 6
- lengths: int32 [256], P('dp'), may hold values from 1 to 96, 6144 in all
- norm_gain: float32 [2, 4096], replicated, may hold values from 0.1 to 1.9
- w_recept: bfloat16 [2, 4096, 4096], P(None, None, ('tp', 'dp')), may hold values from -0.09375 to 0.09375
- w_key: bfloat16 [2, 4096, 4096], P(None, None, ('tp', 'dp')), may hold values from -0.09375 to 0.09375
- w_value: bfloat16 [2, 4096, 4096], P(None, None, ('tp', 'dp')), may hold values from -0.09375 to 0.09375
- w_decay: bfloat16 [2, 4096, 4096], P(None, None, ('tp', 'dp')), may hold values from -0.09375 to 0.09375
- w_rate: bfloat16 [2, 4096, 4096], P(None, None, ('tp', 'dp')), may hold values from -0.09375 to 0.09375
- w_gate: bfloat16 [2, 4096, 4096], P(None, None, ('tp', 'dp')), may hold values from -0.09375 to 0.09375
- w_out: bfloat16 [2, 4096, 4096], P(None, None, ('tp', 'dp')), may hold values from -0.09375 to 0.09375
- decay_base: float32 [2, 4096], P(None, 'tp'), may hold values from -3 to 1
- rate_base: float32 [2, 4096], P(None, 'tp'), may hold values from -3 to 3
- group_gain: float32 [2, 4096], P(None, 'tp'), may hold values from 0.1 to 1.9
- state: float32 [2, 256, 64, 64, 64], P(None, 'dp', 'tp'), may hold values from -6 to 6
Outputs:
- mixed: bfloat16 [256, 4096], P('dp', 'tp')
- new_state: float32 [2, 256, 64, 64, 64], P(None, 'dp', 'tp')
Inputs may be any that keep to these rules, and one draw needn't show every extreme that they name: Each sequence's live length lies between 1 and 96, some sequences reach 96, and the lengths sum to 6144.
All inputs are finite; a program needn't handle non-finite values.
Results may differ from a plain program's by a relative error of at most 0.025.
Values may be sent and summed in bfloat16 or wider, within the bound.
No kernel may reach another device: no remote copies, remote signals or barrier semaphores. Data moves between devices by JAX's collectives and lax.ppermute only.
A program may use at most 128 MiB of HBM per device.

v0:
```python
import functools
import math

import jax
import jax.numpy as jnp
from jax import lax
from jax.experimental import pallas as pl
from jax.experimental.pallas import tpu as pltpu
from jax.sharding import Mesh
from jax.sharding import PartitionSpec as P


STEP = 16
RMS_EPS = 1e-06
GROUP_EPS = 0.00064
TP = ("z", "y")
DP = ("x", "c")
CHIPS = ("z", "y", "x")
PAIR = [(0, 1), (1, 0)]
SLOTS = 24
LANES = 128
ROWS_BY_ROWS = (((1,), (1,)), ((), ()))
ANY = pl.BlockSpec(memory_space=pltpu.HBM)
VMEM = pl.BlockSpec(memory_space=pltpu.VMEM)
SMEM = pl.BlockSpec(memory_space=pltpu.SMEM)


COST = pl.CostEstimate(flops=1 << 31, bytes_accessed=8 << 20, transcendentals=0)
LIMIT = pltpu.CompilerParams(vmem_limit_bytes=24 << 20)


def in_hbm(array):
    return pltpu.with_memory_space_constraint(array, pltpu.HBM)


def live_slots(lengths_row, first, slots):
    live = (lengths_row > STEP).astype(jnp.float32)
    count = live.shape[1]
    before = lax.broadcasted_iota(jnp.int32, (count, count), 0)
    before = before < lax.broadcasted_iota(jnp.int32, (count, count), 1)
    place = jnp.dot(
        jnp.broadcast_to(live, (8, count)), before.astype(jnp.float32),
        preferred_element_type=jnp.float32,
    )[:1]
    wanted = lax.broadcasted_iota(jnp.int32, (slots, count), 0) + first
    return jnp.where((place == wanted.astype(jnp.float32)) & (live > 0), 1.0, 0.0)


def choose_kernel(lengths_ref, tokens_ref, out_ref, count_ref):
    chosen = live_slots(lengths_ref[...], 0, out_ref.shape[1]).astype(jnp.bfloat16)
    rows = jnp.dot(chosen, tokens_ref[...], preferred_element_type=jnp.float32)
    rows = rows.astype(jnp.bfloat16)
    for copy in range(out_ref.shape[0]):
        out_ref[copy] = rows
    live = (lengths_ref[...] > STEP).astype(jnp.float32)
    count = jnp.sum(live, axis=1, keepdims=True)
    count_ref[...] = jnp.broadcast_to(count, count_ref.shape).astype(jnp.bfloat16)


def choose(lengths_row, tokens, slots, copies):
    return pl.pallas_call(
        choose_kernel,
        out_shape=(
            pltpu.HBM((copies, slots, tokens.shape[1]), jnp.bfloat16),
            jax.ShapeDtypeStruct((lengths_row.shape[1], LANES), jnp.bfloat16),
        ),
        in_specs=[VMEM, VMEM],
        out_specs=(VMEM, VMEM),
        compiler_params=LIMIT,
        name="choose",
    )(lengths_row, tokens)


def project_kernel(layer, core_ref, acts_ref, gain_ref, *rest):
    weights, (out_ref, held, sems) = rest[:12], rest[12:]
    blocks, rows, feats = acts_ref.shape
    wide, depth = held.shape
    slim = weights[0].shape[1]
    chunks = sems.shape[0]
    core = core_ref[0]
    copies = []
    for chunk in range(chunks):
        span = pl.ds(chunk * (depth // chunks), depth // chunks)
        for idx, weight in enumerate(weights):
            half = core if idx % 2 == 0 else 1 - core
            start = pl.multiple_of((idx // 2) * 2 * slim + half * slim, slim)
            copy = pltpu.make_async_copy(
                weight.at[layer, :, span], held.at[pl.ds(start, slim), span], sems.at[chunk, idx]
            )
            copy.start()
            copies.append(copy)
    squares = jnp.zeros((rows, feats), jnp.float32)
    for t in range(blocks):
        part = acts_ref[t].astype(jnp.float32)
        squares += part * part
    mean = jnp.sum(squares, axis=1, keepdims=True) / (blocks * feats)
    factor = lax.rsqrt(mean + RMS_EPS)
    result = jnp.zeros((rows, wide), jnp.float32)
    for t in range(blocks):
        if t % (blocks // chunks) == 0:
            first = t // (blocks // chunks) * len(weights)
            for copy in copies[first : first + len(weights)]:
                copy.wait()
        span = slice(t * feats, (t + 1) * feats)
        part = acts_ref[t].astype(jnp.float32) * factor * gain_ref[layer : layer + 1, span]
        result += lax.dot_general(
            part.astype(jnp.bfloat16), held[:, span], ROWS_BY_ROWS,
            preferred_element_type=jnp.float32,
        )
    result = result.astype(jnp.bfloat16)
    per = out_ref.shape[1]
    for x in range(out_ref.shape[0]):
        out_ref[x] = result[x * per : (x + 1) * per]


def project(layer, core, acts, gain, weights, n_x):
    rows = acts.shape[1]
    slim, depth = weights[0].shape[1:]
    wide = slim * len(weights)
    return pl.pallas_call(
        functools.partial(project_kernel, layer),
        out_shape=pltpu.HBM((n_x, rows // n_x, wide), jnp.bfloat16),
        in_specs=[SMEM, VMEM, VMEM] + [ANY] * len(weights),
        out_specs=VMEM,
        scratch_shapes=[
            pltpu.VMEM((wide, depth), jnp.bfloat16),
            pltpu.SemaphoreType.DMA((4, len(weights))),
        ],
        cost_estimate=COST,
        compiler_params=LIMIT,
    )(core, acts, gain, *map(in_hbm, weights))


def table_kernel(layer, lengths_ref, state_ref, out_ref, held, sems):
    chunks = out_ref.shape[0]
    slots, heads, head, _ = held.shape
    per = slots // chunks

    def fetch(sequence, slot):
        return pltpu.make_async_copy(
            state_ref.at[layer, sequence], held.at[slot], sems.at[slot]
        )

    def start(sequence, slot):
        live = lengths_ref[sequence] > STEP

        @pl.when(live & (slot < slots))
        def _():
            fetch(sequence, slot).start()

        return slot + live.astype(jnp.int32)

    count = lax.fori_loop(0, state_ref.shape[1], start, jnp.int32(0))
    for idx in range(chunks):
        for slot in range(idx * per, (idx + 1) * per):

            @pl.when(slot < count)
            def _():
                fetch(0, slot).wait()

            @pl.when(slot >= count)
            def _():
                held[slot] = jnp.zeros_like(held[slot])

        parts = [held[idx * per + k].reshape(heads * head, head) for k in range(per)]
        out_ref[idx] = jnp.concatenate(parts, axis=1).astype(jnp.bfloat16)


def table(layer, slots, lengths, state):
    _, _, heads, head, _ = state.shape
    per = 4
    return pl.pallas_call(
        functools.partial(table_kernel, layer),
        out_shape=pltpu.VMEM((slots // per, heads * head, per * head), jnp.bfloat16),
        in_specs=[SMEM, ANY],
        out_specs=VMEM,
        scratch_shapes=[
            pltpu.VMEM((slots, heads, head, head), jnp.float32),
            pltpu.SemaphoreType.DMA((slots,)),
        ],
        cost_estimate=COST,
        compiler_params=LIMIT,
    )(lengths, in_hbm(state))


def vectors_of(layer, block, lanes, decay_ref, rate_ref):
    head = block.shape[1] // 6
    recept, key, value, decay_pre, rate_pre, gate_pre = [
        block[:, m * head : (m + 1) * head] for m in range(6)
    ]
    decay_in = decay_ref[layer : layer + 1, lanes] + decay_pre
    decay = jnp.exp(-math.exp(-0.5) * jax.nn.sigmoid(decay_in))
    rate = jax.nn.sigmoid(rate_ref[layer : layer + 1, lanes] + rate_pre)
    length = jnp.maximum(jnp.sqrt(jnp.sum(key * key, axis=1, keepdims=True)), 1e-12)
    unit = key / length
    return recept, value, gate_pre, decay, length, unit, unit * rate


def readout_kernel(
    layer, arrived_ref, lengths_ref, decay_ref, rate_ref, gain_ref, table_ref, mixed_ref, column_ref
):
    heads, count, wide = arrived_ref.shape
    head = wide // 6
    units, reads, kept = [], [], []
    for h in range(heads):
        lanes = slice(h * head, (h + 1) * head)
        block = arrived_ref[h].astype(jnp.float32)
        recept, value, gate_pre, decay, length, unit, learned = vectors_of(
            layer, block, lanes, decay_ref, rate_ref
        )
        units.append(unit)
        reads.append(decay * recept)
        dot = jnp.sum(learned * recept, axis=1, keepdims=True)
        kept.append((value * length, dot, jax.nn.sigmoid(gate_pre)))
    per = table_ref.shape[2] // head
    group = 8
    shape = (2 * heads * group, per * head)
    row = lax.broadcasted_iota(jnp.int32, shape, 0) % group
    spot = lax.broadcasted_iota(jnp.int32, shape, 1) // head
    lane_head = lax.broadcasted_iota(jnp.int32, (group, heads * head), 1) // head
    summed = ([], [])
    for g in range(count // group):
        rows = slice(g * group, (g + 1) * group)
        left = jnp.concatenate(
            [jnp.concatenate([v[rows]] * per, axis=1) for v in units + reads], axis=0
        )
        product = jnp.zeros((shape[0], heads * head), jnp.float32)
        for part in range(group // per):
            chosen = jnp.where(row == spot + part * per, left, 0.0).astype(jnp.bfloat16)
            product += lax.dot_general(
                chosen, table_ref[g * (group // per) + part], ROWS_BY_ROWS,
                preferred_element_type=jnp.float32,
            )
        for kind in range(2):
            base = kind * heads * group
            total = product[base : base + group]
            for h in range(1, heads):
                piece = product[base + h * group : base + (h + 1) * group]
                total = jnp.where(lane_head == h, piece, total)
            summed[kind].append(total)
    by_unit, by_read = [jnp.concatenate(parts, axis=0) for parts in summed]
    live = jnp.sum((lengths_ref[...] > STEP).astype(jnp.float32), axis=1, keepdims=True)
    active = lax.broadcasted_iota(jnp.int32, (count, 1), 0).astype(jnp.float32) < live
    mixed = []
    for h in range(heads):
        lanes = slice(h * head, (h + 1) * head)
        scaled, dot, gate = kept[h]
        column = scaled - by_unit[:, lanes]
        column_ref[:, lanes] = column
        readout = by_read[:, lanes] + column * dot
        centred = readout - jnp.mean(readout, axis=1, keepdims=True)
        spread_ = jnp.mean(centred * centred, axis=1, keepdims=True)
        normal = centred * lax.rsqrt(spread_ + GROUP_EPS)
        normal = normal * gain_ref[layer : layer + 1, lanes] * gate
        mixed.append(jnp.where(active, normal, 0.0))
    rows = jnp.concatenate(mixed, axis=1).astype(jnp.bfloat16)
    for t in range(mixed_ref.shape[0]):
        mixed_ref[t] = rows


def read_out(layer, arrived, lengths, decay_base, rate_base, group_gain, states, copies):
    heads, count, wide = arrived.shape
    feats = heads * wide // 6
    return pl.pallas_call(
        functools.partial(readout_kernel, layer),
        out_shape=(
            pltpu.HBM((copies, count, feats), jnp.bfloat16),
            pltpu.VMEM((count, feats), jnp.float32),
        ),
        in_specs=[VMEM] * 6,
        out_specs=(VMEM, VMEM),
        cost_estimate=COST,
        compiler_params=LIMIT,
    )(arrived, lengths, decay_base, rate_base, group_gain, states)


def in_two(value):
    high = value.astype(jnp.bfloat16)
    return high, (value - high.astype(jnp.float32)).astype(jnp.bfloat16)


def update_kernel(
    layer, lengths_ref, arrived_ref, decay_ref, rate_ref, column_ref, others_ref, state_ref, *rest
):
    out_ref, held, rows_ref, columns_ref, in_sems, out_sems = rest[-6:]
    count, heads, head, _ = held.shape
    chunks = in_sems.shape[0]
    per = count // chunks

    def fetch(idx):
        span = pl.ds(idx * per, per)
        return pltpu.make_async_copy(state_ref.at[layer, span], held.at[span], in_sems.at[idx])

    def put(idx):
        span = pl.ds(idx * per, per)
        return pltpu.make_async_copy(held.at[span], out_ref.at[layer, span], out_sems.at[idx])

    for idx in range(chunks):
        fetch(idx).start()
    for h in range(heads):
        lanes = slice(h * head, (h + 1) * head)
        block = jnp.concatenate(
            [
                arrived_ref[h].astype(jnp.float32),
                others_ref[layer, :, h * 6 * head : (h + 1) * 6 * head],
            ],
            axis=0,
        )
        _, _, _, decay, _, _, learned = vectors_of(layer, block, lanes, decay_ref, rate_ref)
        rows_ref[:, h, :] = decay
        rows_ref[:, heads + h, :] = learned
    slots = column_ref.shape[0]
    columns_ref[:slots] = column_ref[...]
    columns_ref[slots:] = others_ref[layer, :, heads * 6 * head : heads * 7 * head]
    own = lax.broadcasted_iota(jnp.int32, (heads, heads * head), 0)
    own = own == lax.broadcasted_iota(jnp.int32, (heads, heads * head), 1) // head

    def advance(r, slot):
        live = lengths_ref[r] > STEP

        @pl.when(live)
        def _():
            high, low = in_two(jnp.where(own, columns_ref[pl.ds(slot, 1), :], 0.0))
            vectors = rows_ref[slot]
            right_high, right_low = in_two(vectors[heads:])
            added = lax.dot_general(
                jnp.concatenate([high, high, low], axis=0),
                jnp.concatenate([right_high, right_low, right_high], axis=0),
                (((0,), (0,)), ((), ())), preferred_element_type=jnp.float32,
            )
            for h in range(heads):
                new = held[r, h] * vectors[h : h + 1] + added[h * head : (h + 1) * head]
                held[r, h] = new

        return slot + live.astype(jnp.int32)

    slot = jnp.int32(0)
    for idx in range(chunks):
        fetch(idx).wait()
        slot = lax.fori_loop(idx * per, (idx + 1) * per, advance, slot)
        if idx:
            put(idx - 1).start()
    put(chunks - 1).start()
    for idx in range(chunks):
        put(idx).wait()


def update(layer, lengths, arrived, decay_base, rate_base, column, others, state, earlier):
    _, count, heads, head, _ = state.shape
    more = () if earlier is None else (earlier,)
    return pl.pallas_call(
        functools.partial(update_kernel, layer),
        out_shape=pltpu.HBM(state.shape, state.dtype),
        in_specs=[SMEM] + [VMEM] * 5 + [ANY] + [ANY] * len(more),
        out_specs=ANY,
        scratch_shapes=[
            pltpu.VMEM((count, heads, head, head), jnp.float32),
            pltpu.VMEM((count, 2 * heads, head), jnp.float32),
            pltpu.VMEM((count, heads * head), jnp.float32),
            pltpu.SemaphoreType.DMA((8,)),
            pltpu.SemaphoreType.DMA((8,)),
        ],
        input_output_aliases={7: 0} if more else {},
        cost_estimate=COST,
        compiler_params=LIMIT,
    )(lengths, arrived, decay_base, rate_base, column, others, in_hbm(state), *map(in_hbm, more))


def pack_out_kernel(starts_ref, *rest):
    weights, out_ref = rest[:8], rest[8]
    sems = rest[-1]
    slim, depth = weights[0].shape[0], out_ref.shape[1]
    copies = []
    for idx, weight in enumerate(weights):
        start = pl.multiple_of(starts_ref[idx] * slim, slim)
        copy = pltpu.make_async_copy(
            weight.at[:, pl.ds(0, depth)], out_ref.at[pl.ds(start, slim), :], sems.at[idx]
        )
        copy.start()
        copies.append(copy)
    if len(rest) > 10:
        most_ref, counts = rest[9:11]
        for idx, weight in enumerate(weights):
            copy = pltpu.make_async_copy(
                weight.at[:, pl.ds(depth, LANES)], counts.at[idx], sems.at[8 + idx]
            )
            copy.start()
            copies.append(copy)
    for copy in copies:
        copy.wait()
    if len(rest) > 10:
        most = jnp.max(counts[...].astype(jnp.float32), axis=0)
        most_ref[...] = jnp.max(most, axis=0, keepdims=True)


def pack_out(starts, weights, depth):
    slim, wide = weights[0].shape
    packed = pltpu.VMEM((slim * len(weights), depth), jnp.bfloat16)
    sems = pltpu.SemaphoreType.DMA((2 * len(weights),))
    counted = wide > depth
    counts = [pltpu.VMEM((len(weights), slim, LANES), jnp.bfloat16)] if counted else []
    most = jax.ShapeDtypeStruct((1, LANES), jnp.float32)
    return pl.pallas_call(
        pack_out_kernel,
        out_shape=(packed, most) if counted else packed,
        in_specs=[SMEM] + [ANY] * len(weights),
        out_specs=(VMEM, VMEM) if counted else VMEM,
        scratch_shapes=counts + [sems],
        cost_estimate=COST,
        compiler_params=LIMIT,
    )(starts, *weights)


def columns_of(acts_ref, packed_ref):
    blocks, rows, feats = acts_ref.shape
    result = jnp.zeros((rows, packed_ref.shape[0]), jnp.float32)
    for t in range(blocks):
        result += lax.dot_general(
            acts_ref[t], packed_ref[:, t * feats : (t + 1) * feats], ROWS_BY_ROWS,
            preferred_element_type=jnp.float32,
        )
    return result.astype(jnp.bfloat16)


def finish_kernel(acts_ref, packed_ref, out_ref):
    result = columns_of(acts_ref, packed_ref)
    for copy in range(out_ref.shape[0]):
        out_ref[copy] = result


def place_kernel(acts_ref, packed_ref, lengths_ref, others_ref, out_ref):
    result = columns_of(acts_ref, packed_ref)
    feats = result.shape[1]
    others = others_ref[1, :, others_ref.shape[2] - feats :].astype(jnp.bfloat16)
    every = jnp.concatenate([result.astype(jnp.float32), others.astype(jnp.float32)], axis=0)
    chosen = live_slots(lengths_ref[...], 0, every.shape[0]).astype(jnp.bfloat16)
    out_ref[...] = lax.dot_general(
        chosen, every.astype(jnp.bfloat16), (((0,), (0,)), ((), ())),
        preferred_element_type=jnp.float32,
    ).astype(jnp.bfloat16)


def finish(acts, packed, copies):
    return pl.pallas_call(
        finish_kernel,
        out_shape=pltpu.HBM((copies, acts.shape[1], packed.shape[0]), jnp.bfloat16),
        in_specs=[VMEM, VMEM],
        out_specs=VMEM,
        cost_estimate=COST,
        compiler_params=LIMIT,
        name="finish_0",
    )(acts, packed)


def place(acts, packed, lengths_row, others):
    return pl.pallas_call(
        place_kernel,
        out_shape=pltpu.HBM((lengths_row.shape[1], packed.shape[0]), jnp.bfloat16),
        in_specs=[VMEM] * 4,
        out_specs=VMEM,
        cost_estimate=COST,
        compiler_params=LIMIT,
        name="finish_1",
    )(acts, packed, lengths_row, others)


def spread(value):
    count = lax.axis_size(CHIPS)
    copies = jnp.broadcast_to(value[None], (count,) + value.shape)
    return lax.all_to_all(copies, CHIPS, 0, 0)


def in_order(own, peer, core):
    return jnp.concatenate(
        [jnp.where(core == 0, own, peer), jnp.where(core == 0, peer, own)], axis=0
    )


def beyond_slots(
    tokens, lengths_row, norm_gain, weights, w_out, decay_base, rate_base, group_gain, state
):
    core = lax.axis_index("c")
    count, feats = tokens.shape
    rows = count - SLOTS
    heads, head = state.shape[2], state.shape[-1]
    n_x, n_tp = lax.axis_size("x"), lax.axis_size(TP)
    chosen = live_slots(lengths_row, SLOTS, rows)
    live = jnp.sum((lengths_row > STEP).astype(jnp.float32))
    active = jnp.arange(rows) + SLOTS < live
    mine = jnp.dot(chosen.astype(jnp.bfloat16), tokens, preferred_element_type=jnp.float32)
    mine = mine.astype(jnp.bfloat16)
    held = jnp.argmax(chosen, axis=1)
    out_own = w_out.swapaxes(1, 2)
    out_peer = lax.ppermute(out_own, "c", PAIR)

    def block(natural, layer_parts):
        pairs, outs, gain_in, base, rate_b, gain, state_l = layer_parts
        joined = jnp.concatenate(
            [in_order(pairs[2 * m], pairs[2 * m + 1], core) for m in range(6)], axis=0
        )
        values = natural.astype(jnp.float32)
        factor = lax.rsqrt(jnp.mean(values * values, axis=1, keepdims=True) + RMS_EPS)
        normed = (values * factor * gain_in).astype(jnp.bfloat16)
        projected = lax.dot_general(
            normed, joined, ROWS_BY_ROWS, preferred_element_type=jnp.float32
        ).astype(jnp.bfloat16)
        arrived = lax.all_to_all(projected.reshape(n_x, rows, -1), "x", 0, 0)
        arrived = arrived.transpose(1, 0, 2).astype(jnp.float32)
        recept, key, value, decay_pre, rate_pre, gate_pre = [
            arrived[:, :, m * head : (m + 1) * head] for m in range(6)
        ]
        base, rate_b, gain = [part.reshape(heads, head) for part in (base, rate_b, gain)]
        decay = jnp.exp(-math.exp(-0.5) * jax.nn.sigmoid(base + decay_pre))
        rate = jax.nn.sigmoid(rate_b + rate_pre)
        length = jnp.maximum(jnp.sqrt(jnp.sum(key * key, axis=-1, keepdims=True)), 1e-12)
        unit = key / length
        old = jnp.take(state_l, held, axis=0)
        column = value * length - jnp.sum(old * unit[:, :, None, :], axis=-1)
        dot = jnp.sum(unit * rate * recept, axis=-1, keepdims=True)
        readout = jnp.sum(old * (decay * recept)[:, :, None, :], axis=-1) + column * dot
        centred = readout - jnp.mean(readout, axis=-1, keepdims=True)
        spread_ = jnp.mean(centred * centred, axis=-1, keepdims=True)
        normal = centred * lax.rsqrt(spread_ + GROUP_EPS) * gain * jax.nn.sigmoid(gate_pre)
        mixed = jnp.where(active[:, None, None], normal, 0.0)
        mixed = mixed.astype(jnp.bfloat16).reshape(rows, feats)
        mixed_all = spread(mixed).reshape(n_tp, n_x, rows, feats).transpose(1, 2, 0, 3)
        cols = lax.dot_general(
            mixed_all.reshape(n_x * rows, n_tp * feats), in_order(*outs, core),
            ROWS_BY_ROWS, preferred_element_type=jnp.float32,
        ).astype(jnp.bfloat16)
        blocks = spread(cols.reshape(rows, -1)).reshape(n_tp, n_x, n_x, rows, -1)
        current = blocks.transpose(2, 3, 0, 1, 4)
        here = lax.dynamic_slice_in_dim(current, lax.axis_index("x"), 1, 0)
        here = lax.dynamic_slice_in_dim(here, lax.axis_index(TP), 1, 2).reshape(rows, feats)
        terms = (arrived.reshape(rows, -1), column.reshape(rows, feats), here.astype(jnp.float32))
        return current.reshape(n_x * rows, n_tp * feats), jnp.concatenate(terms, axis=1)

    natural = spread(mine).reshape(n_tp, n_x, rows, feats).transpose(1, 2, 0, 3)
    layers = (weights, (out_own, out_peer), norm_gain, decay_base, rate_base, group_gain, state)
    return lax.scan(block, natural.reshape(n_x * rows, n_tp * feats), layers)[1]


def local(
    tokens, lengths, norm_gain, w_recept, w_key, w_value, w_decay, w_rate, w_gate, w_out,
    decay_base, rate_base, group_gain, state,
):
    core, spot = lax.axis_index("c"), lax.axis_index("x")
    rows, feats = tokens.shape
    n_x, n_tp, n_chips = lax.axis_size("x"), lax.axis_size(TP), lax.axis_size(CHIPS)
    starts = []
    for k in range(n_x):
        source = (spot + n_x - k) % n_x
        starts += [source * 2 + core, source * 2 + 1 - core]
    starts = jnp.stack(starts).astype(jnp.int32)
    core_at = jnp.reshape(core, (1,)).astype(jnp.int32)
    lengths_row = lengths.reshape(1, rows)

    def along_x(layer, more):
        own = jnp.concatenate([w_out.swapaxes(1, 2)[layer]] + more, axis=1)
        return [own] + [
            lax.ppermute(own, "x", [(i, (i + k) % n_x) for i in range(n_x)])
            for k in range(1, n_x)
        ]

    def over_pair(pieces):
        return [p for piece in pieces for p in (piece, lax.ppermute(piece, "c", PAIR))]

    chosen, count = choose(lengths_row, tokens, SLOTS, n_chips)
    acts = lax.all_to_all(chosen, CHIPS, 0, 0)
    weights = []
    for w in (w_recept, w_key, w_value, w_decay, w_rate, w_gate):
        own = w.swapaxes(1, 2)
        weights += [own, lax.ppermute(own, "c", PAIR)]
    states = [table(layer, SLOTS, lengths, state) for layer in range(2)]
    depth = n_tp * feats
    first, most = pack_out(starts, over_pair(along_x(0, [count])), depth)
    packed_out = [first, pack_out(starts, over_pair(along_x(1, [])), depth)]
    operands = (
        tokens, lengths_row, norm_gain, weights, w_out, decay_base, rate_base, group_gain, state
    )
    others = lax.cond(
        most[0, 0] > SLOTS,
        beyond_slots,
        lambda *_: jnp.zeros((2, rows - SLOTS, 8 * feats), jnp.float32),
        *operands,
    )
    new_state = None
    for layer in range(2):
        acts = acts.reshape(n_tp, n_x * SLOTS, feats)
        projected = project(layer, core_at, acts, norm_gain, weights, n_x)
        arrived = lax.all_to_all(projected, "x", 0, 0)
        mixed, column_terms = read_out(
            layer, arrived, lengths_row, decay_base, rate_base, group_gain, states[layer], n_tp
        )
        mixed_all = lax.all_to_all(mixed, TP, 0, 0)
        new_state = update(
            layer, lengths, arrived, decay_base, rate_base, column_terms, others, state, new_state
        )
        if layer == 0:
            current = finish(mixed_all, packed_out[0], n_chips)
            acts = lax.all_to_all(current, CHIPS, 0, 0)
    return place(mixed_all, packed_out[1], lengths_row, others), new_state


def solution(mesh):
    finer = Mesh(mesh.devices.reshape(4, 4, mesh.shape["dp"] // 2, 2), ("z", "y", "x", "c"))
    wide = P(None, None, TP + DP)
    in_specs = (
        (P(DP, TP), P(DP), P()) + (wide,) * 7 + (P(None, TP),) * 3 + (P(None, DP, TP, None, None),)
    )
    out_specs = (P(DP, TP), P(None, DP, TP, None, None))
    return jax.shard_map(local, mesh=finer, in_specs=in_specs, out_specs=out_specs, check_vma=False)
```

profile of v0, /device:TPU:1, one launch (start us, length us, event | category | flops | bytes accessed | tf_op | source)
XLA Modules:
  0.0 145.8 jit_solution(12541301209574087986)
XLA Ops:
  0.6 1.1 slice_bitcast_fusion
  1.7 1.9 %choose.1 = (bf16[64,24,256]{2,1,0:T(8,128)(2,1)}, bf16[32,128]{1,0:T(8,128)(2,1)S(1)}) custom-call(s32[1,32]{1,0:T(1,128)} %bitcast.194, bf16[32,256]{1,0:T(8,128)(2,1)} %tokens_ref.1), custom_call_target="tpu_custom_call" | custom-call | tf_op jit(solution)/shard_map/choose/pallas_call | solution.py:61
  3.6 3.4 %collective-permute-start.12 = (bf16[32,4224]{1,0:T(8,128)(2,1)S(1)}, bf16[32,4224]{1,0:T(8,128)(2,1)S(1)}, u32[]{:S(2)}, u32[]{:S(2)}) collective-permute-start(bf16[32,4224]{1,0:T(8,128)(2,1)S(1)} %pad_maximum_fusion.rest_0_), channel_id=1, source_target_pairs={{0,6},{2,0},{4,2},{6,4},{1,7},{3,1},{5,3},{7,5},{8,14},{10,8},{12,... | collective-permute-start | bytes 811016 | tf_op jit(solution)/shard_map/ppermute | solution.py:561
  7.0 0.5 collective-permute-start.10
  7.5 0.6 collective-permute-start.8
  8.1 1.5 %collective-permute-start.1 = (bf16[2,32,4096]{2,1,0:T(8,128)(2,1)}, bf16[2,32,4096]{2,1,0:T(8,128)(2,1)S(1)}, u32[]{:S(2)}, u32[]{:S(2)}) collective-permute-start(bf16[2,32,4096]{2,1,0:T(8,128)(2,1)} %bitcast.163), channel_id=1, source_target_pairs={{0,1},{1,0},{2,3},{3,2},{4,5},{5,4},{6,7},{7,6},{8,9},{9,8},{10,11... | collective-permute-start | bytes 1572872 | tf_op jit(solution)/shard_map/ppermute | solution.py:573
  9.6 0.0 collective-permute-start.2
  9.6 3.7 %collective-permute-done.12.rest_6_ = bf16[32,4224]{1,0:T(8,128)(2,1)S(1)} collective-permute-done((bf16[32,4224]{1,0:T(8,128)(2,1)S(1)}, bf16[32,4224]{1,0:T(8,128)(2,1)S(1)}, u32[]{:S(2)}, u32[]{:S(2)}) %collective-permute-start.12) | collective-permute-done | bytes 270368 | tf_op jit(solution)/shard_map/ppermute | solution.py:561
  13.3 6.2 %collective-permute-start.3 = (bf16[2,32,4096]{2,1,0:T(8,128)(2,1)}, bf16[2,32,4096]{2,1,0:T(8,128)(2,1)S(1)}, u32[]{:S(2)}, u32[]{:S(2)}) collective-permute-start(bf16[2,32,4096]{2,1,0:T(8,128)(2,1)} %bitcast.171), channel_id=1, source_target_pairs={{0,1},{1,0},{2,3},{3,2},{4,5},{5,4},{6,7},{7,6},{8,9},{9,8},{10,11... | collective-permute-start | bytes 1572872 | tf_op jit(solution)/shard_map/ppermute | solution.py:573
  19.5 0.0 collective-permute-done.10.rest_4_
  19.5 0.0 collective-permute-start.4
  19.5 3.2 %collective-permute-done.8.rest_2_ = bf16[32,4224]{1,0:T(8,128)(2,1)S(1)} collective-permute-done((bf16[32,4224]{1,0:T(8,128)(2,1)S(1)}, bf16[32,4224]{1,0:T(8,128)(2,1)S(1)}, u32[]{:S(2)}, u32[]{:S(2)}) %collective-permute-start.8) | collective-permute-done | bytes 270368 | tf_op jit(solution)/shard_map/ppermute | solution.py:561
  22.7 0.5 collective-permute-start.5
  23.2 0.1 collective-permute-start.6
  23.3 0.0 collective-permute-done.2.rest_3_
  23.3 0.4 collective-permute-start.7
  23.7 0.0 collective-permute-done.3.rest_5_
  23.7 0.1 collective-permute-start.13
  23.8 0.0 collective-permute-done.4.rest_7_
  23.8 0.4 collective-permute-start.11
  24.2 0.7 collective-permute-done.5.rest_9_
  24.9 0.4 collective-permute-start.9
  25.3 0.4 copy-done.16
  25.8 0.1 stack.35.starts_ref
  25.9 0.8 copy-done.18
  26.7 0.0 copy-start.23
  26.7 0.0 copy-start.24
  26.7 0.0 copy-start.25
  26.7 0.0 copy-start.26
  26.7 0.0 collective-permute-done.7.rest_1_
  26.8 0.1 collective-permute-done.11.rest_5_
  26.8 0.4 collective-permute-done.9.rest_3_
  27.2 0.9 shard_map.152
  28.2 1.3 copy-done.2
  29.7 0.7 conditional.1
  29.7 0.7 broadcast.169
  30.3 24.8 %all_to_all.67 = bf16[64,24,256]{2,1,0:T(8,128)(2,1)S(1)} all-to-all(bf16[64,24,256]{2,1,0:T(8,128)(2,1)} %get-tuple-element.439), channel_id=1, replica_groups=mesh['z'=4,'y'=4,'x'=4,'c'=2] {'z','y','x'}, dimensions={0} | all-to-all | bytes 1572864 | tf_op jit(solution)/shard_map/all_to_all | solution.py:569
  55.1 3.9 %shard_map.149 = bf16[4,24,384]{2,1,0:T(8,128)(2,1)} custom-call(s32[1]{0:T(128)} %bitcast.6.core_ref, bf16[16,96,256]{2,1,0:T(8,128)(2,1)S(1)} %bitcast.158, f32[2,4096]{1,0:T(2,128)S(1)} %copy-done.21, bf16[2,32,4096]{2,1,0:T(8,128)(2,1)} %bitcast.164, bf16[2,32,4096]{2,1,0:T(8,128)(2,1)} %copy-done.10, bf16[2,32,4096]{2,1,0:T(8,128)(2,1)} %bitcast.168, ...), custom_call_target="tpu_custom_call" | custom-call | flops 2147483648 | bytes 8388608 | tf_op jit(solution)/shard_map/pallas_call | solution.py:120
  59.0 3.3 %all-to-all-start.5 = ((bf16[4,24,384]{2,1,0:T(8,128)(2,1)}), bf16[4,24,384]{2,1,0:T(8,128)(2,1)S(1)}, u32[]{:S(2)}, u32[]{:S(2)}) async-start(bf16[4,24,384]{2,1,0:T(8,128)(2,1)} %shard_map.149), calls=%async_computation.5 | async-start | bytes 147456 | tf_op jit(solution)/shard_map/all_to_all | solution.py:591
  62.3 2.8 %shard_map.150.table_ref = bf16[6,256,256]{2,1,0:T(8,128)(2,1)S(1)} custom-call(s32[32]{0:T(128)S(1)} %copy-done.25, f32[2,32,4,64,64]{4,3,2,1,0:T(8,128)} %state_ref.7), custom_call_target="tpu_custom_call" | custom-call | flops 2147483648 | bytes 8388608 | tf_op jit(solution)/shard_map/pallas_call | solution.py:172
  65.1 1.7 %all-to-all-done.5.arrived_ref = bf16[4,24,384]{2,1,0:T(8,128)(2,1)S(1)} async-done(((bf16[4,24,384]{2,1,0:T(8,128)(2,1)}), bf16[4,24,384]{2,1,0:T(8,128)(2,1)S(1)}, u32[]{:S(2)}, u32[]{:S(2)}) %all-to-all-start.5) | async-done | bytes 73760 | tf_op jit(solution)/shard_map/all_to_all | solution.py:591
  66.8 1.9 %shard_map.151 = (bf16[16,24,256]{2,1,0:T(8,128)(2,1)}, f32[24,256]{1,0:T(8,128)S(1)}) custom-call(bf16[4,24,384]{2,1,0:T(8,128)(2,1)S(1)} %all-to-all-done.5.arrived_ref, s32[1,32]{1,0:T(1,128)S(1)} %bitcast.196, f32[2,256]{1,0:T(2,128)S(1)} %copy-done.22, f32[2,256]{1,0:T(2,128)S(1)} %copy-done.23, f32[2,256]{1,0:T(2,128)S(1)} %copy-done.26, ...), custom_call_target="tpu_custom_call" | custom-call | flops 2147483648 | bytes 8388608 | tf_op jit(solution)/shard_map/pallas_call | solution.py:264
  68.7 10.7 %all_to_all.68.acts_ref = bf16[16,24,256]{2,1,0:T(8,128)(2,1)S(1)} all-to-all(bf16[16,24,256]{2,1,0:T(8,128)(2,1)} %get-tuple-element.440), channel_id=1, replica_groups=mesh['z'=4,'y'=4,'x'=4,'c'=2] {'z','y'}, dimensions={0} | all-to-all | bytes 393216 | tf_op jit(solution)/shard_map/all_to_all | solution.py:595
  79.4 1.6 %finish_0.1 = bf16[64,24,256]{2,1,0:T(8,128)(2,1)} custom-call(bf16[16,24,256]{2,1,0:T(8,128)(2,1)S(1)} %all_to_all.68.acts_ref, bf16[256,4096]{1,0:T(8,128)(2,1)S(1)} %copy-done.3), custom_call_target="tpu_custom_call" | custom-call | flops 2147483648 | bytes 8388608 | tf_op jit(solution)/shard_map/finish_0/pallas_call | solution.py:444
  81.0 5.0 %all-to-all-start.7 = ((bf16[64,24,256]{2,1,0:T(8,128)(2,1)}), bf16[64,24,256]{2,1,0:T(8,128)(2,1)S(1)}, u32[]{:S(2)}, u32[]{:S(2)}) async-start(bf16[64,24,256]{2,1,0:T(8,128)(2,1)} %finish_0.1), calls=%async_computation.7 | async-start | bytes 1572864 | tf_op jit(solution)/shard_map/all_to_all | solution.py:601
  86.1 2.3 %collective-permute-start.19 = (bf16[32,4096]{1,0:T(8,128)(2,1)S(1)}, bf16[32,4096]{1,0:T(8,128)(2,1)S(1)}, u32[]{:S(2)}, u32[]{:S(2)}) collective-permute-start(bf16[32,4096]{1,0:T(8,128)(2,1)S(1)} %get-tuple-element.565.rest_0_), channel_id=1, source_target_pairs={{0,6},{2,0},{4,2},{6,4},{1,7},{3,1},{5,3},{7,5},{8,14},{10,8},{12,... | collective-permute-start | bytes 786440 | tf_op jit(solution)/shard_map/ppermute | solution.py:561
  88.4 0.6 collective-permute-start.17
  88.9 0.6 collective-permute-start.15
  89.5 5.0 %collective-permute-start.14 = (bf16[32,4096]{1,0:T(8,128)(2,1)S(1)}, bf16[32,4096]{1,0:T(8,128)(2,1)S(1)}, u32[]{:S(2)}, u32[]{:S(2)}) collective-permute-start(bf16[32,4096]{1,0:T(8,128)(2,1)S(1)} %get-tuple-element.565.rest_0_), channel_id=1, source_target_pairs={{0,1},{1,0},{2,3},{3,2},{4,5},{5,4},{6,7},{7,6},{8,9},{9,8},{10,11... | collective-permute-start | bytes 786440 | tf_op jit(solution)/shard_map/ppermute | solution.py:566
  94.5 3.4 %collective-permute-done.19.rest_6_ = bf16[32,4096]{1,0:T(8,128)(2,1)S(1)} collective-permute-done((bf16[32,4096]{1,0:T(8,128)(2,1)S(1)}, bf16[32,4096]{1,0:T(8,128)(2,1)S(1)}, u32[]{:S(2)}, u32[]{:S(2)}) %collective-permute-start.19) | collective-permute-done | bytes 262176 | tf_op jit(solution)/shard_map/ppermute | solution.py:561
  97.9 7.5 %collective-permute-start.20 = (bf16[32,4096]{1,0:T(8,128)(2,1)S(1)}, bf16[32,4096]{1,0:T(8,128)(2,1)S(1)}, u32[]{:S(2)}, u32[]{:S(2)}) collective-permute-start(bf16[32,4096]{1,0:T(8,128)(2,1)S(1)} %collective-permute-done.19.rest_6_), channel_id=1, source_target_pairs={{0,1},{1,0},{2,3},{3,2},{4,5},{5,4},{6,7},{7,6},{8,9},{9,8},{10,11... | collective-permute-start | bytes 786440 | tf_op jit(solution)/shard_map/ppermute | solution.py:566
  105.4 1.5 %collective-permute-start.18 = (bf16[32,4096]{1,0:T(8,128)(2,1)S(1)}, bf16[32,4096]{1,0:T(8,128)(2,1)S(1)}, u32[]{:S(2)}, u32[]{:S(2)}) collective-permute-start(bf16[32,4096]{1,0:T(8,128)(2,1)S(1)} %collective-permute-done.17.rest_4_), channel_id=1, source_target_pairs={{0,1},{1,0},{2,3},{3,2},{4,5},{5,4},{6,7},{7,6},{8,9},{9,8},{10,11... | collective-permute-start | bytes 786440 | tf_op jit(solution)/shard_map/ppermute | solution.py:566
  106.9 2.5 %collective-permute-start.16 = (bf16[32,4096]{1,0:T(8,128)(2,1)S(1)}, bf16[32,4096]{1,0:T(8,128)(2,1)S(1)}, u32[]{:S(2)}, u32[]{:S(2)}) collective-permute-start(bf16[32,4096]{1,0:T(8,128)(2,1)S(1)} %collective-permute-done.15.rest_2_), channel_id=1, source_target_pairs={{0,1},{1,0},{2,3},{3,2},{4,5},{5,4},{6,7},{7,6},{8,9},{9,8},{10,11... | collective-permute-start | bytes 786440 | tf_op jit(solution)/shard_map/ppermute | solution.py:566
  109.4 2.8 %shard_map.154.table_ref = bf16[6,256,256]{2,1,0:T(8,128)(2,1)S(1)} custom-call(s32[32]{0:T(128)S(1)} %copy-done.25, f32[2,32,4,64,64]{4,3,2,1,0:T(8,128)} %state_ref.7), custom_call_target="tpu_custom_call" | custom-call | flops 2147483648 | bytes 8388608 | tf_op jit(solution)/shard_map/pallas_call | solution.py:172
  112.3 0.9 shard_map.156.packed_ref
  113.2 1.3 copy-done
  114.5 3.9 %shard_map.153 = bf16[4,24,384]{2,1,0:T(8,128)(2,1)} custom-call(s32[1]{0:T(128)} %bitcast.6.core_ref, bf16[16,96,256]{2,1,0:T(8,128)(2,1)S(1)} %bitcast.157, f32[2,4096]{1,0:T(2,128)S(1)} %copy-done.21, bf16[2,32,4096]{2,1,0:T(8,128)(2,1)} %bitcast.165, bf16[2,32,4096]{2,1,0:T(8,128)(2,1)} %copy-done.10, bf16[2,32,4096]{2,1,0:T(8,128)(2,1)} %bitcast.169, ...), custom_call_target="tpu_custom_call" | custom-call | flops 2147483648 | bytes 8388608 | tf_op jit(solution)/shard_map/pallas_call | solution.py:120
  118.4 3.3 %all-to-all-start.8 = ((bf16[4,24,384]{2,1,0:T(8,128)(2,1)}), bf16[4,24,384]{2,1,0:T(8,128)(2,1)S(1)}, u32[]{:S(2)}, u32[]{:S(2)}) async-start(bf16[4,24,384]{2,1,0:T(8,128)(2,1)} %shard_map.153), calls=%async_computation.8 | async-start | bytes 147456 | tf_op jit(solution)/shard_map/all_to_all | solution.py:591
  121.7 5.9 %shard_map.157.rest_0_ = f32[2,32,4,64,64]{4,3,2,1,0:T(8,128)} custom-call(s32[32]{0:T(128)S(1)} %copy-done.25, bf16[4,24,384]{2,1,0:T(8,128)(2,1)S(1)} %all-to-all-done.5.arrived_ref, f32[2,256]{1,0:T(2,128)S(1)} %copy-done.22, f32[2,256]{1,0:T(2,128)S(1)} %copy-done.23, f32[24,256]{1,0:T(8,128)S(1)} %get-tuple-element.446.column_ref, ...), custom_call_target="tpu_custom_call" | custom-call | flops 2147483648 | bytes 8388608 | tf_op jit(solution)/shard_map/pallas_call | solution.py:351
  127.6 1.9 %shard_map.155 = (bf16[16,24,256]{2,1,0:T(8,128)(2,1)}, f32[24,256]{1,0:T(8,128)S(1)}) custom-call(bf16[4,24,384]{2,1,0:T(8,128)(2,1)S(1)} %all-to-all-done.8.arrived_ref, s32[1,32]{1,0:T(1,128)S(1)} %bitcast.197, f32[2,256]{1,0:T(2,128)S(1)} %copy-done.22, f32[2,256]{1,0:T(2,128)S(1)} %copy-done.23, f32[2,256]{1,0:T(2,128)S(1)} %copy-done.26, ...), custom_call_target="tpu_custom_call" | custom-call | flops 2147483648 | bytes 8388608 | tf_op jit(solution)/shard_map/pallas_call | solution.py:264
  129.6 6.6 %all-to-all-start.9 = ((bf16[16,24,256]{2,1,0:T(8,128)(2,1)}), bf16[16,24,256]{2,1,0:T(8,128)(2,1)S(1)}, u32[]{:S(2)}, u32[]{:S(2)}) async-start(bf16[16,24,256]{2,1,0:T(8,128)(2,1)} %get-tuple-element.443), calls=%async_computation.9 | async-start | bytes 393216 | tf_op jit(solution)/shard_map/all_to_all | solution.py:595
  136.2 6.0 %shard_map.158 = f32[2,32,4,64,64]{4,3,2,1,0:T(8,128)} custom-call(s32[32]{0:T(128)S(1)} %copy-done.25, bf16[4,24,384]{2,1,0:T(8,128)(2,1)S(1)} %all-to-all-done.8.arrived_ref, f32[2,256]{1,0:T(2,128)S(1)} %copy-done.22, f32[2,256]{1,0:T(2,128)S(1)} %copy-done.23, f32[24,256]{1,0:T(8,128)S(1)} %get-tuple-element.445.column_ref, ...), custom_call_target="tpu_custom_call", output_to_operand_aliasing={{}: (7, {})} | custom-call | flops 2147483648 | bytes 8388608 | tf_op jit(solution)/shard_map/pallas_call | solution.py:351
  142.2 1.2 all-to-all-done.9.acts_ref
  143.4 2.4 %finish_1.1 = bf16[32,256]{1,0:T(8,128)(2,1)} custom-call(bf16[16,24,256]{2,1,0:T(8,128)(2,1)S(1)} %all-to-all-done.9.acts_ref, bf16[256,4096]{1,0:T(8,128)(2,1)S(1)} %copy-done.1, s32[1,32]{1,0:T(1,128)S(1)} %bitcast.198, f32[2,8,2048]{2,1,0:T(8,128)} %get-tuple-element.850.others_ref), custom_call_target="tpu_custom_call" | custom-call | flops 2147483648 | bytes 8388608 | tf_op jit(solution)/shard_map/finish_1/pallas_call | solution.py:456
  (40 shorter events, 0.1 us)
Async XLA Ops:
  3.6 9.7 %collective-permute-start.12 = (bf16[32,4224]{1,0:T(8,128)(2,1)S(1)}, bf16[32,4224]{1,0:T(8,128)(2,1)S(1)}, u32[]{:S(2)}, u32[]{:S(2)}) collective-permute-start(bf16[32,4224]{1,0:T(8,128)(2,1)S(1)} %pad_maximum_fusion.rest_0_), channel_id=1, source_target_pairs={{0,6},{2,0},{4,2},{6,4},{1,7},{3,1},{5,3},{7,5},{8,14},{10,8},{12,... | collective-permute-start | bytes 811016 | tf_op jit(solution)/shard_map/ppermute | solution.py:561
  7.0 12.5 %collective-permute-start.10 = (bf16[32,4224]{1,0:T(8,128)(2,1)S(1)}, bf16[32,4224]{1,0:T(8,128)(2,1)S(1)}, u32[]{:S(2)}, u32[]{:S(2)}) collective-permute-start(bf16[32,4224]{1,0:T(8,128)(2,1)S(1)} %pad_maximum_fusion.rest_0_), channel_id=1, source_target_pairs={{0,4},{2,6},{4,0},{6,2},{1,5},{3,7},{5,1},{7,3},{8,12},{10,14},{12... | collective-permute-start | bytes 811016 | tf_op jit(solution)/shard_map/ppermute | solution.py:561
  7.5 15.2 %collective-permute-start.8 = (bf16[32,4224]{1,0:T(8,128)(2,1)S(1)}, bf16[32,4224]{1,0:T(8,128)(2,1)S(1)}, u32[]{:S(2)}, u32[]{:S(2)}) collective-permute-start(bf16[32,4224]{1,0:T(8,128)(2,1)S(1)} %pad_maximum_fusion.rest_0_), channel_id=1, source_target_pairs={{0,2},{2,4},{4,6},{6,0},{1,3},{3,5},{5,7},{7,1},{8,10},{10,12},{12... | collective-permute-start | bytes 811016 | tf_op jit(solution)/shard_map/ppermute | solution.py:561
  8.1 15.1 %collective-permute-start.1 = (bf16[2,32,4096]{2,1,0:T(8,128)(2,1)}, bf16[2,32,4096]{2,1,0:T(8,128)(2,1)S(1)}, u32[]{:S(2)}, u32[]{:S(2)}) collective-permute-start(bf16[2,32,4096]{2,1,0:T(8,128)(2,1)} %bitcast.163), channel_id=1, source_target_pairs={{0,1},{1,0},{2,3},{3,2},{4,5},{5,4},{6,7},{7,6},{8,9},{9,8},{10,11... | collective-permute-start | bytes 1572872 | tf_op jit(solution)/shard_map/ppermute | solution.py:573
  9.6 13.6 %collective-permute-start.2 = (bf16[2,32,4096]{2,1,0:T(8,128)(2,1)}, bf16[2,32,4096]{2,1,0:T(8,128)(2,1)S(1)}, u32[]{:S(2)}, u32[]{:S(2)}) collective-permute-start(bf16[2,32,4096]{2,1,0:T(8,128)(2,1)} %bitcast.167), channel_id=1, source_target_pairs={{0,1},{1,0},{2,3},{3,2},{4,5},{5,4},{6,7},{7,6},{8,9},{9,8},{10,11... | collective-permute-start | bytes 1572872 | tf_op jit(solution)/shard_map/ppermute | solution.py:573
  13.3 10.4 %collective-permute-start.3 = (bf16[2,32,4096]{2,1,0:T(8,128)(2,1)}, bf16[2,32,4096]{2,1,0:T(8,128)(2,1)S(1)}, u32[]{:S(2)}, u32[]{:S(2)}) collective-permute-start(bf16[2,32,4096]{2,1,0:T(8,128)(2,1)} %bitcast.171), channel_id=1, source_target_pairs={{0,1},{1,0},{2,3},{3,2},{4,5},{5,4},{6,7},{7,6},{8,9},{9,8},{10,11... | collective-permute-start | bytes 1572872 | tf_op jit(solution)/shard_map/ppermute | solution.py:573
  19.5 4.3 %collective-permute-start.4 = (bf16[2,32,4096]{2,1,0:T(8,128)(2,1)}, bf16[2,32,4096]{2,1,0:T(8,128)(2,1)S(1)}, u32[]{:S(2)}, u32[]{:S(2)}) collective-permute-start(bf16[2,32,4096]{2,1,0:T(8,128)(2,1)} %bitcast.175), channel_id=1, source_target_pairs={{0,1},{1,0},{2,3},{3,2},{4,5},{5,4},{6,7},{7,6},{8,9},{9,8},{10,11... | collective-permute-start | bytes 1572872 | tf_op jit(solution)/shard_map/ppermute | solution.py:573
  22.7 2.2 %collective-permute-start.5 = (bf16[2,32,4096]{2,1,0:T(8,128)(2,1)}, bf16[2,32,4096]{2,1,0:T(8,128)(2,1)S(1)}, u32[]{:S(2)}, u32[]{:S(2)}) collective-permute-start(bf16[2,32,4096]{2,1,0:T(8,128)(2,1)} %bitcast.179), channel_id=1, source_target_pairs={{0,1},{1,0},{2,3},{3,2},{4,5},{5,4},{6,7},{7,6},{8,9},{9,8},{10,11... | collective-permute-start | bytes 1572872 | tf_op jit(solution)/shard_map/ppermute | solution.py:573
  23.2 1.0 copy-start.10
  23.2 2.7 %collective-permute-start.6 = (bf16[2,32,4096]{2,1,0:T(8,128)(2,1)}, bf16[2,32,4096]{2,1,0:T(8,128)(2,1)S(1)}, u32[]{:S(2)}, u32[]{:S(2)}) collective-permute-start(bf16[2,32,4096]{2,1,0:T(8,128)(2,1)} %bitcast.183), channel_id=1, source_target_pairs={{0,1},{1,0},{2,3},{3,2},{4,5},{5,4},{6,7},{7,6},{8,9},{9,8},{10,11... | collective-permute-start | bytes 1572872 | tf_op jit(solution)/shard_map/ppermute | solution.py:573
  23.3 1.7 %copy-start.11 = (bf16[2,32,4096]{2,1,0:T(8,128)(2,1)}, bf16[2,32,4096]{2,1,0:T(8,128)(2,1)S(1)}, u32[]{:S(2)}) copy-start(bf16[2,32,4096]{2,1,0:T(8,128)(2,1)S(1)} %collective-permute-done.2.rest_3_) | copy-start | bytes 1572868
  23.3 3.5 %collective-permute-start.7 = (bf16[32,4224]{1,0:T(8,128)(2,1)S(1)}, bf16[32,4224]{1,0:T(8,128)(2,1)S(1)}, u32[]{:S(2)}, u32[]{:S(2)}) collective-permute-start(bf16[32,4224]{1,0:T(8,128)(2,1)S(1)} %pad_maximum_fusion.rest_0_), channel_id=1, source_target_pairs={{0,1},{1,0},{2,3},{3,2},{4,5},{5,4},{6,7},{7,6},{8,9},{9,8},{10,11... | collective-permute-start | bytes 811016 | tf_op jit(solution)/shard_map/ppermute | solution.py:566
  23.7 1.6 %copy-start.12 = (bf16[2,32,4096]{2,1,0:T(8,128)(2,1)}, bf16[2,32,4096]{2,1,0:T(8,128)(2,1)S(1)}, u32[]{:S(2)}) copy-start(bf16[2,32,4096]{2,1,0:T(8,128)(2,1)S(1)} %collective-permute-done.3.rest_5_) | copy-start | bytes 1572868
  23.7 3.0 %collective-permute-start.13 = (bf16[32,4224]{1,0:T(8,128)(2,1)S(1)}, bf16[32,4224]{1,0:T(8,128)(2,1)S(1)}, u32[]{:S(2)}, u32[]{:S(2)}) collective-permute-start(bf16[32,4224]{1,0:T(8,128)(2,1)S(1)} %collective-permute-done.12.rest_6_), channel_id=1, source_target_pairs={{0,1},{1,0},{2,3},{3,2},{4,5},{5,4},{6,7},{7,6},{8,9},{9,8},{10,11... | collective-permute-start | bytes 811016 | tf_op jit(solution)/shard_map/ppermute | solution.py:566
  23.8 1.5 %copy-start.14 = (bf16[2,32,4096]{2,1,0:T(8,128)(2,1)}, bf16[2,32,4096]{2,1,0:T(8,128)(2,1)S(1)}, u32[]{:S(2)}) copy-start(bf16[2,32,4096]{2,1,0:T(8,128)(2,1)S(1)} %collective-permute-done.4.rest_7_) | copy-start | bytes 1572868
  23.8 3.0 %collective-permute-start.11 = (bf16[32,4224]{1,0:T(8,128)(2,1)S(1)}, bf16[32,4224]{1,0:T(8,128)(2,1)S(1)}, u32[]{:S(2)}, u32[]{:S(2)}) collective-permute-start(bf16[32,4224]{1,0:T(8,128)(2,1)S(1)} %collective-permute-done.10.rest_4_), channel_id=1, source_target_pairs={{0,1},{1,0},{2,3},{3,2},{4,5},{5,4},{6,7},{7,6},{8,9},{9,8},{10,11... | collective-permute-start | bytes 811016 | tf_op jit(solution)/shard_map/ppermute | solution.py:566
  24.9 0.8 copy-start.16
  24.9 2.3 %collective-permute-start.9 = (bf16[32,4224]{1,0:T(8,128)(2,1)S(1)}, bf16[32,4224]{1,0:T(8,128)(2,1)S(1)}, u32[]{:S(2)}, u32[]{:S(2)}) collective-permute-start(bf16[32,4224]{1,0:T(8,128)(2,1)S(1)} %collective-permute-done.8.rest_2_), channel_id=1, source_target_pairs={{0,1},{1,0},{2,3},{3,2},{4,5},{5,4},{6,7},{7,6},{8,9},{9,8},{10,11... | collective-permute-start | bytes 811016 | tf_op jit(solution)/shard_map/ppermute | solution.py:566
  25.9 0.8 copy-start.18
  26.7 2.9 %copy-start.4 = (bf16[2,4096,32]{1,2,0:T(8,128)(2,1)S(1)}, bf16[2,4096,32]{1,2,0:T(8,128)(2,1)}, u32[]{:S(2)}) copy-start(bf16[2,4096,32]{1,2,0:T(8,128)(2,1)} %param.21) | copy-start | bytes 1572868
  26.7 2.9 %copy-start.5 = (bf16[2,4096,32]{1,2,0:T(8,128)(2,1)S(1)}, bf16[2,4096,32]{1,2,0:T(8,128)(2,1)}, u32[]{:S(2)}) copy-start(bf16[2,4096,32]{1,2,0:T(8,128)(2,1)} %param.22) | copy-start | bytes 1572868
  26.7 2.9 %copy-start.21 = (f32[2,4096]{1,0:T(2,128)S(1)}, f32[2,4096]{1,0:T(2,128)}, u32[]{:S(2)}) copy-start(f32[2,4096]{1,0:T(2,128)} %gain_ref.6) | copy-start | bytes 98308
  26.7 2.9 %copy-start.22 = (f32[2,256]{1,0:T(2,128)S(1)}, f32[2,256]{1,0:T(2,128)}, u32[]{:S(2)}) copy-start(f32[2,256]{1,0:T(2,128)} %decay_ref.7) | copy-start | bytes 6148
  26.7 2.9 %copy-start.23 = (f32[2,256]{1,0:T(2,128)S(1)}, f32[2,256]{1,0:T(2,128)}, u32[]{:S(2)}) copy-start(f32[2,256]{1,0:T(2,128)} %rate_ref.7) | copy-start | bytes 6148
  26.7 2.9 %copy-start.24 = (bf16[32,256]{1,0:T(8,128)(2,1)S(1)}, bf16[32,256]{1,0:T(8,128)(2,1)}, u32[]{:S(2)}) copy-start(bf16[32,256]{1,0:T(8,128)(2,1)} %tokens_ref.1) | copy-start | bytes 49156
  26.7 2.9 %copy-start.25 = (s32[32]{0:T(128)S(1)}, s32[32]{0:T(128)}, u32[]{:S(2)}) copy-start(s32[32]{0:T(128)} %lengths_ref.7) | copy-start | bytes 388
  26.7 2.9 %copy-start.26 = (f32[2,256]{1,0:T(2,128)S(1)}, f32[2,256]{1,0:T(2,128)}, u32[]{:S(2)}) copy-start(f32[2,256]{1,0:T(2,128)} %gain_ref.7) | copy-start | bytes 6148
  28.2 1.4 copy-start.2
  59.0 7.8 %all-to-all-start.5 = ((bf16[4,24,384]{2,1,0:T(8,128)(2,1)}), bf16[4,24,384]{2,1,0:T(8,128)(2,1)S(1)}, u32[]{:S(2)}, u32[]{:S(2)}) async-start(bf16[4,24,384]{2,1,0:T(8,128)(2,1)} %shard_map.149), calls=%async_computation.5 | async-start | bytes 147456 | tf_op jit(solution)/shard_map/all_to_all | solution.py:591
  66.8 12.6 %copy-start.3 = (bf16[256,4096]{1,0:T(8,128)(2,1)S(1)}, bf16[256,4096]{1,0:T(8,128)(2,1)}, u32[]{:S(2)}) copy-start(bf16[256,4096]{1,0:T(8,128)(2,1)} %copy-done.2) | copy-start | bytes 6291460
  81.0 33.5 %all-to-all-start.7 = ((bf16[64,24,256]{2,1,0:T(8,128)(2,1)}), bf16[64,24,256]{2,1,0:T(8,128)(2,1)S(1)}, u32[]{:S(2)}, u32[]{:S(2)}) async-start(bf16[64,24,256]{2,1,0:T(8,128)(2,1)} %finish_0.1), calls=%async_computation.7 | async-start | bytes 1572864 | tf_op jit(solution)/shard_map/all_to_all | solution.py:601
  86.1 11.8 %collective-permute-start.19 = (bf16[32,4096]{1,0:T(8,128)(2,1)S(1)}, bf16[32,4096]{1,0:T(8,128)(2,1)S(1)}, u32[]{:S(2)}, u32[]{:S(2)}) collective-permute-start(bf16[32,4096]{1,0:T(8,128)(2,1)S(1)} %get-tuple-element.565.rest_0_), channel_id=1, source_target_pairs={{0,6},{2,0},{4,2},{6,4},{1,7},{3,1},{5,3},{7,5},{8,14},{10,8},{12,... | collective-permute-start | bytes 786440 | tf_op jit(solution)/shard_map/ppermute | solution.py:561
  88.4 17.1 %collective-permute-start.17 = (bf16[32,4096]{1,0:T(8,128)(2,1)S(1)}, bf16[32,4096]{1,0:T(8,128)(2,1)S(1)}, u32[]{:S(2)}, u32[]{:S(2)}) collective-permute-start(bf16[32,4096]{1,0:T(8,128)(2,1)S(1)} %get-tuple-element.565.rest_0_), channel_id=1, source_target_pairs={{0,4},{2,6},{4,0},{6,2},{1,5},{3,7},{5,1},{7,3},{8,12},{10,14},{12... | collective-permute-start | bytes 786440 | tf_op jit(solution)/shard_map/ppermute | solution.py:561
  88.9 18.0 %collective-permute-start.15 = (bf16[32,4096]{1,0:T(8,128)(2,1)S(1)}, bf16[32,4096]{1,0:T(8,128)(2,1)S(1)}, u32[]{:S(2)}, u32[]{:S(2)}) collective-permute-start(bf16[32,4096]{1,0:T(8,128)(2,1)S(1)} %get-tuple-element.565.rest_0_), channel_id=1, source_target_pairs={{0,2},{2,4},{4,6},{6,0},{1,3},{3,5},{5,7},{7,1},{8,10},{10,12},{12... | collective-permute-start | bytes 786440 | tf_op jit(solution)/shard_map/ppermute | solution.py:561
  89.5 22.7 %collective-permute-start.14 = (bf16[32,4096]{1,0:T(8,128)(2,1)S(1)}, bf16[32,4096]{1,0:T(8,128)(2,1)S(1)}, u32[]{:S(2)}, u32[]{:S(2)}) collective-permute-start(bf16[32,4096]{1,0:T(8,128)(2,1)S(1)} %get-tuple-element.565.rest_0_), channel_id=1, source_target_pairs={{0,1},{1,0},{2,3},{3,2},{4,5},{5,4},{6,7},{7,6},{8,9},{9,8},{10,11... | collective-permute-start | bytes 786440 | tf_op jit(solution)/shard_map/ppermute | solution.py:566
  97.9 14.3 %collective-permute-start.20 = (bf16[32,4096]{1,0:T(8,128)(2,1)S(1)}, bf16[32,4096]{1,0:T(8,128)(2,1)S(1)}, u32[]{:S(2)}, u32[]{:S(2)}) collective-permute-start(bf16[32,4096]{1,0:T(8,128)(2,1)S(1)} %collective-permute-done.19.rest_6_), channel_id=1, source_target_pairs={{0,1},{1,0},{2,3},{3,2},{4,5},{5,4},{6,7},{7,6},{8,9},{9,8},{10,11... | collective-permute-start | bytes 786440 | tf_op jit(solution)/shard_map/ppermute | solution.py:566
  105.4 6.8 %collective-permute-start.18 = (bf16[32,4096]{1,0:T(8,128)(2,1)S(1)}, bf16[32,4096]{1,0:T(8,128)(2,1)S(1)}, u32[]{:S(2)}, u32[]{:S(2)}) collective-permute-start(bf16[32,4096]{1,0:T(8,128)(2,1)S(1)} %collective-permute-done.17.rest_4_), channel_id=1, source_target_pairs={{0,1},{1,0},{2,3},{3,2},{4,5},{5,4},{6,7},{7,6},{8,9},{9,8},{10,11... | collective-permute-start | bytes 786440 | tf_op jit(solution)/shard_map/ppermute | solution.py:566
  106.9 5.3 %collective-permute-start.16 = (bf16[32,4096]{1,0:T(8,128)(2,1)S(1)}, bf16[32,4096]{1,0:T(8,128)(2,1)S(1)}, u32[]{:S(2)}, u32[]{:S(2)}) collective-permute-start(bf16[32,4096]{1,0:T(8,128)(2,1)S(1)} %collective-permute-done.15.rest_2_), channel_id=1, source_target_pairs={{0,1},{1,0},{2,3},{3,2},{4,5},{5,4},{6,7},{7,6},{8,9},{9,8},{10,11... | collective-permute-start | bytes 786440 | tf_op jit(solution)/shard_map/ppermute | solution.py:566
  113.2 1.4 copy-start
  118.4 9.2 %all-to-all-start.8 = ((bf16[4,24,384]{2,1,0:T(8,128)(2,1)}), bf16[4,24,384]{2,1,0:T(8,128)(2,1)S(1)}, u32[]{:S(2)}, u32[]{:S(2)}) async-start(bf16[4,24,384]{2,1,0:T(8,128)(2,1)} %shard_map.153), calls=%async_computation.8 | async-start | bytes 147456 | tf_op jit(solution)/shard_map/all_to_all | solution.py:591
  129.6 13.8 %all-to-all-start.9 = ((bf16[16,24,256]{2,1,0:T(8,128)(2,1)}), bf16[16,24,256]{2,1,0:T(8,128)(2,1)S(1)}, u32[]{:S(2)}, u32[]{:S(2)}) async-start(bf16[16,24,256]{2,1,0:T(8,128)(2,1)} %get-tuple-element.443), calls=%async_computation.9 | async-start | bytes 393216 | tf_op jit(solution)/shard_map/all_to_all | solution.py:595
  136.2 7.2 %copy-start.1 = (bf16[256,4096]{1,0:T(8,128)(2,1)S(1)}, bf16[256,4096]{1,0:T(8,128)(2,1)}, u32[]{:S(2)}) copy-start(bf16[256,4096]{1,0:T(8,128)(2,1)} %copy-done) | copy-start | bytes 6291460
where the time goes:
time: 149 us; the launch traced here: 146 us
  starting transfers between devices  52.3 us (35%)
  Pallas kernels  36.8 us (25%)
  blocking collectives  35.5 us (24%)
  waiting for transfers between devices  14.4 us (10%)
  local copies, waits for them, and re-layouts  5.83 us (4%)
    all_to_all x1, blocking collectives, local(): acts = lax.all_to_all(chosen, CHIPS, 0, 0)  24.8 us
    ppermute x8, starting transfers between devices, over_pair(): lax.ppermute(piece, 'c', PAIR)  17.8 us
    pallas_call x2, Pallas kernels, update(): pl.pallas_call(functools.partial(update_kernel, layer), out_shape=pltpu.H...  11.9 us
    all_to_all x1, blocking collectives, local(): mixed_all = lax.all_to_all(mixed, TP, 0, 0)  10.7 us
    ppermute x6, waiting for transfers between devices, along_x(): lax.ppermute(own, 'x', [(i, (i + k) % n_x) for i in range(n_x)])  10.3 us
    ppermute x6, starting transfers between devices, local(): weights += [own, lax.ppermute(own, 'c', PAIR)]  8.29 us
    ppermute x6, starting transfers between devices, along_x(): lax.ppermute(own, 'x', [(i, (i + k) % n_x) for i in range(n_x)])  7.94 us
    pallas_call x2, Pallas kernels, project(): pl.pallas_call(functools.partial(project_kernel, layer), out_shape=pltpu....  7.78 us
  transfers between devices with their start and end apart: 24, of which 8 were waited for; matrix products, arithmetic and copies ran while one was open for 0% of the time, Pallas kernels for 13%

commit v1 on v0

--- a/solution.py
+++ b/solution.py
@@ -128,7 +128,7 @@
         ],
         cost_estimate=COST,
         compiler_params=LIMIT,
-    )(core, acts, gain, *map(in_hbm, weights))
+    )(core, acts, gain, *weights)
 
 
 def table_kernel(layer, lengths_ref, state_ref, out_ref, held, sems):
@@ -366,73 +366,79 @@
     )(lengths, arrived, decay_base, rate_base, column, others, in_hbm(state), *map(in_hbm, more))
 
 
-def pack_out_kernel(starts_ref, *rest):
-    weights, out_ref = rest[:8], rest[8]
-    sems = rest[-1]
-    slim, depth = weights[0].shape[0], out_ref.shape[1]
+def most_kernel(*refs):
+    weights, (out_ref, counts, sems) = refs[:8], refs[8:]
     copies = []
     for idx, weight in enumerate(weights):
-        start = pl.multiple_of(starts_ref[idx] * slim, slim)
+        _, wide = weight.shape
         copy = pltpu.make_async_copy(
-            weight.at[:, pl.ds(0, depth)], out_ref.at[pl.ds(start, slim), :], sems.at[idx]
+            weight.at[:, pl.ds(wide - LANES, LANES)], counts.at[idx], sems.at[idx]
         )
         copy.start()
         copies.append(copy)
-    if len(rest) > 10:
-        most_ref, counts = rest[9:11]
+    for copy in copies:
+        copy.wait()
+    most = jnp.max(counts[...].astype(jnp.float32), axis=0)
+    out_ref[...] = jnp.max(most, axis=0, keepdims=True)
+
+
+def most_live(weights):
+    return pl.pallas_call(
+        most_kernel,
+        out_shape=jax.ShapeDtypeStruct((1, LANES), jnp.float32),
+        in_specs=[ANY] * len(weights),
+        out_specs=VMEM,
+        scratch_shapes=[
+            pltpu.VMEM((len(weights), weights[0].shape[0], LANES), jnp.bfloat16),
+            pltpu.SemaphoreType.DMA((len(weights),)),
+        ],
+        cost_estimate=COST,
+        compiler_params=LIMIT,
+        name="most_live",
+    )(*weights)
+
+
+def columns_of(starts_ref, acts_ref, weights, held, sems):
+    blocks, rows, feats = acts_ref.shape
+    wide, depth = held.shape
+    slim = weights[0].shape[0]
+    chunks = sems.shape[0]
+    copies = []
+    for chunk in range(chunks):
+        span = pl.ds(chunk * (depth // chunks), depth // chunks)
         for idx, weight in enumerate(weights):
+            start = pl.multiple_of(starts_ref[idx] * slim, slim)
             copy = pltpu.make_async_copy(
-                weight.at[:, pl.ds(depth, LANES)], counts.at[idx], sems.at[8 + idx]
+                weight.at[:, span], held.at[pl.ds(start, slim), span], sems.at[chunk, idx]
             )
             copy.start()
             copies.append(copy)
-    for copy in copies:
-        copy.wait()
-    if len(rest) > 10:
-        most = jnp.max(counts[...].astype(jnp.float32), axis=0)
-        most_ref[...] = jnp.max(most, axis=0, keepdims=True)
-
-
-def pack_out(starts, weights, depth):
-    slim, wide = weights[0].shape
-    packed = pltpu.VMEM((slim * len(weights), depth), jnp.bfloat16)
-    sems = pltpu.SemaphoreType.DMA((2 * len(weights),))
-    counted = wide > depth
-    counts = [pltpu.VMEM((len(weights), slim, LANES), jnp.bfloat16)] if counted else []
-    most = jax.ShapeDtypeStruct((1, LANES), jnp.float32)
-    return pl.pallas_call(
-        pack_out_kernel,
-        out_shape=(packed, most) if counted else packed,
-        in_specs=[SMEM] + [ANY] * len(weights),
-        out_specs=(VMEM, VMEM) if counted else VMEM,
-        scratch_shapes=counts + [sems],
-        cost_estimate=COST,
-        compiler_params=LIMIT,
-    )(starts, *weights)
-
-
-def columns_of(acts_ref, packed_ref):
-    blocks, rows, feats = acts_ref.shape
-    result = jnp.zeros((rows, packed_ref.shape[0]), jnp.float32)
+    result = jnp.zeros((rows, wide), jnp.float32)
     for t in range(blocks):
+        if t % (blocks // chunks) == 0:
+            first = t // (blocks // chunks) * len(weights)
+            for copy in copies[first : first + len(weights)]:
+                copy.wait()
         result += lax.dot_general(
-            acts_ref[t], packed_ref[:, t * feats : (t + 1) * feats], ROWS_BY_ROWS,
+            acts_ref[t], held[:, t * feats : (t + 1) * feats], ROWS_BY_ROWS,
             preferred_element_type=jnp.float32,
         )
     return result.astype(jnp.bfloat16)
 
 
-def finish_kernel(acts_ref, packed_ref, out_ref):
-    result = columns_of(acts_ref, packed_ref)
+def finish_kernel(starts_ref, acts_ref, *rest):
+    weights, (out_ref, held, sems) = rest[:8], rest[8:]
+    result = columns_of(starts_ref, acts_ref, weights, held, sems)
     for copy in range(out_ref.shape[0]):
         out_ref[copy] = result
 
 
-def place_kernel(acts_ref, packed_ref, lengths_ref, others_ref, out_ref):
-    result = columns_of(acts_ref, packed_ref)
+def place_kernel(starts_ref, acts_ref, lengths_ref, others_ref, *rest):
+    weights, (out_ref, held, sems) = rest[:8], rest[8:]
+    result = columns_of(starts_ref, acts_ref, weights, held, sems)
     feats = result.shape[1]
-    others = others_ref[1, :, others_ref.shape[2] - feats :].astype(jnp.bfloat16)
-    every = jnp.concatenate([result.astype(jnp.float32), others.astype(jnp.float32)], axis=0)
+    others = others_ref[1, :, others_ref.shape[2] - feats :]
+    every = jnp.concatenate([result.astype(jnp.float32), others], axis=0)
     chosen = live_slots(lengths_ref[...], 0, every.shape[0]).astype(jnp.bfloat16)
     out_ref[...] = lax.dot_general(
         chosen, every.astype(jnp.bfloat16), (((0,), (0,)), ((), ())),
@@ -440,28 +446,40 @@
     ).astype(jnp.bfloat16)
 
 
-def finish(acts, packed, copies):
+def column_scratch(acts, weights):
+    depth = acts.shape[0] * acts.shape[2]
+    return [
+        pltpu.VMEM((weights[0].shape[0] * len(weights), depth), jnp.bfloat16),
+        pltpu.SemaphoreType.DMA((4, len(weights))),
+    ]
+
+
+def finish(starts, acts, weights, copies):
+    wide = weights[0].shape[0] * len(weights)
     return pl.pallas_call(
         finish_kernel,
-        out_shape=pltpu.HBM((copies, acts.shape[1], packed.shape[0]), jnp.bfloat16),
-        in_specs=[VMEM, VMEM],
+        out_shape=pltpu.HBM((copies, acts.shape[1], wide), jnp.bfloat16),
+        in_specs=[SMEM, VMEM] + [ANY] * len(weights),
         out_specs=VMEM,
+        scratch_shapes=column_scratch(acts, weights),
         cost_estimate=COST,
         compiler_params=LIMIT,
         name="finish_0",
-    )(acts, packed)
-
-
-def place(acts, packed, lengths_row, others):
+    )(starts, acts, *weights)
+
+
+def place(starts, acts, lengths_row, others, weights):
+    wide = weights[0].shape[0] * len(weights)
     return pl.pallas_call(
         place_kernel,
-        out_shape=pltpu.HBM((lengths_row.shape[1], packed.shape[0]), jnp.bfloat16),
-        in_specs=[VMEM] * 4,
+        out_shape=pltpu.HBM((lengths_row.shape[1], wide), jnp.bfloat16),
+        in_specs=[SMEM] + [VMEM] * 3 + [ANY] * len(weights),
         out_specs=VMEM,
+        scratch_shapes=column_scratch(acts, weights),
         cost_estimate=COST,
         compiler_params=LIMIT,
         name="finish_1",
-    )(acts, packed, lengths_row, others)
+    )(starts, acts, lengths_row, others, *weights)
 
 
 def spread(value):
@@ -572,9 +590,8 @@
         own = w.swapaxes(1, 2)
         weights += [own, lax.ppermute(own, "c", PAIR)]
     states = [table(layer, SLOTS, lengths, state) for layer in range(2)]
-    depth = n_tp * feats
-    first, most = pack_out(starts, over_pair(along_x(0, [count])), depth)
-    packed_out = [first, pack_out(starts, over_pair(along_x(1, [])), depth)]
+    columns = [over_pair(along_x(0, [count])), over_pair(along_x(1, []))]
+    most = most_live(columns[0])
     operands = (
         tokens, lengths_row, norm_gain, weights, w_out, decay_base, rate_base, group_gain, state
     )
@@ -597,9 +614,9 @@
             layer, lengths, arrived, decay_base, rate_base, column_terms, others, state, new_state
         )
         if layer == 0:
-            current = finish(mixed_all, packed_out[0], n_chips)
+            current = finish(starts, mixed_all, columns[0], n_chips)
             acts = lax.all_to_all(current, CHIPS, 0, 0)
-    return place(mixed_all, packed_out[1], lengths_row, others), new_state
+    return place(starts, mixed_all, lengths_row, others, columns[1]), new_state
 
 
 def solution(mesh):

time: 149 us -> 147 us (0.987)
  blocking collectives: 35.5 us -> 0 us
  waiting for transfers between devices: 14.4 us -> 35.3 us
  starting transfers between devices: 52.3 us -> 65.4 us
  local copies, waits for them, and re-layouts: 5.83 us -> 3.39 us
  Pallas kernels: 36.8 us -> 39.2 us
    all_to_all x2 -> x0, blocking collectives: 35.5 us -> none  [the longest x1 24.8 us: local(): acts = lax.all_to_all(chosen, CHIPS, 0, 0)]
    all_to_all x0 -> x1, waiting for transfers between devices: none -> 15.2 us  [local(): acts = lax.all_to_all(chosen, CHIPS, 0, 0)]
    all_to_all x0 -> x1, starting transfers between devices: none -> 9.6 us  [local(): acts = lax.all_to_all(chosen, CHIPS, 0, 0)]
    all_to_all x1 -> x2, waiting for transfers between devices: 1.18 us -> 8.31 us  [local(): mixed_all = lax.all_to_all(mixed, TP, 0, 0)]
    all_to_all x1 -> x2, starting transfers between devices: 6.64 us -> 10.2 us  [local(): mixed_all = lax.all_to_all(mixed, TP, 0, 0)]
    ppermute x6, waiting for transfers between devices: 10.3 us -> 7.49 us  [along_x(): lax.ppermute(own, 'x', [(i, (i + k) % n_x) for i in range(n_x)])]
    unnamed x36 -> x24, local copies, waits for them, and re-layouts: 4.02 us -> 1.57 us
    pallas_call x1, Pallas kernels: 1.63 us -> 3.96 us  [finish(): pl.pallas_call(finish_kernel, out_shape=pltpu.HBM((copies, acts.shape[1],...]
  transfers between devices with their start and end apart: 24 -> 26, of which waited for: 8 -> 13; matrix products, arithmetic and copies ran while one was open for 0% -> 0% of each run, Pallas kernels for 13% -> 16%
where the time goes in v1:
time: 147 us; the launch traced here: 145 us
  starting transfers between devices  65.4 us (44%)
  Pallas kernels  39.2 us (27%)
  waiting for transfers between devices  35.3 us (24%)
  local copies, waits for them, and re-layouts  3.39 us (2%)
    ppermute x8, starting transfers between devices, over_pair(): lax.ppermute(piece, 'c', PAIR)  17.9 us
    all_to_all x1, waiting for transfers between devices, local(): acts = lax.all_to_all(chosen, CHIPS, 0, 0)  15.2 us
    pallas_call x2, Pallas kernels, update(): pl.pallas_call(functools.partial(update_kernel, layer), out_shape=pltpu.H...  11.7 us
    all_to_all x2, starting transfers between devices, local(): mixed_all = lax.all_to_all(mixed, TP, 0, 0)  10.2 us
    all_to_all x1, starting transfers between devices, local(): acts = lax.all_to_all(chosen, CHIPS, 0, 0)  9.6 us
    all_to_all x2, waiting for transfers between devices, local(): mixed_all = lax.all_to_all(mixed, TP, 0, 0)  8.31 us
    ppermute x6, starting transfers between devices, local(): weights += [own, lax.ppermute(own, 'c', PAIR)]  8.22 us
    ppermute x6, starting transfers between devices, along_x(): lax.ppermute(own, 'x', [(i, (i + k) % n_x) for i in range(n_x)])  7.94 us
  transfers between devices with their start and end apart: 26, of which 13 were waited for; matrix products, arithmetic and copies ran while one was open for 0% of the time, Pallas kernels for 16%

profile of v1, /device:TPU:1, one launch (start us, length us, event | category | flops | bytes accessed | tf_op | source)
XLA Modules:
  0.0 144.6 jit_solution(7828841633299304652)
XLA Ops:
  0.6 1.1 slice_bitcast_fusion
  1.7 1.9 %choose.1 = (bf16[64,24,256]{2,1,0:T(8,128)(2,1)}, bf16[32,128]{1,0:T(8,128)(2,1)S(1)}) custom-call(s32[1,32]{1,0:T(1,128)} %bitcast.167, bf16[32,256]{1,0:T(8,128)(2,1)} %tokens_ref.1), custom_call_target="tpu_custom_call" | custom-call | tf_op jit(solution)/shard_map/choose/pallas_call | solution.py:61
  3.7 3.4 %collective-permute-start.12 = (bf16[32,4224]{1,0:T(8,128)(2,1)S(1)}, bf16[32,4224]{1,0:T(8,128)(2,1)S(1)}, u32[]{:S(2)}, u32[]{:S(2)}) collective-permute-start(bf16[32,4224]{1,0:T(8,128)(2,1)S(1)} %pad_maximum_fusion.rest_0_.refs_0_), channel_id=1, source_target_pairs={{0,6},{2,0},{4,2},{6,4},{1,7},{3,1},{5,3},{7,5},{8,14},{10,8},{12,... | collective-permute-start | bytes 811016 | tf_op jit(solution)/shard_map/ppermute | solution.py:579
  7.0 0.5 collective-permute-start.10
  7.5 0.6 collective-permute-start.8
  8.1 1.5 %collective-permute-start.1 = (bf16[2,32,4096]{2,1,0:T(8,128)(2,1)}, bf16[2,32,4096]{2,1,0:T(8,128)(2,1)}, u32[]{:S(2)}, u32[]{:S(2)}) collective-permute-start(bf16[2,32,4096]{2,1,0:T(8,128)(2,1)} %bitcast.17.rest_0_), channel_id=1, source_target_pairs={{0,1},{1,0},{2,3},{3,2},{4,5},{5,4},{6,7},{7,6},{8,9},{9,8},{10,11... | collective-permute-start | bytes 1572872 | tf_op jit(solution)/shard_map/ppermute | solution.py:591
  9.7 0.0 collective-permute-start.2
  9.7 3.7 %collective-permute-done.12.rest_6_.refs_6_ = bf16[32,4224]{1,0:T(8,128)(2,1)S(1)} collective-permute-done((bf16[32,4224]{1,0:T(8,128)(2,1)S(1)}, bf16[32,4224]{1,0:T(8,128)(2,1)S(1)}, u32[]{:S(2)}, u32[]{:S(2)}) %collective-permute-start.12) | collective-permute-done | bytes 270368 | tf_op jit(solution)/shard_map/ppermute | solution.py:579
  13.3 6.2 %collective-permute-start.3 = (bf16[2,32,4096]{2,1,0:T(8,128)(2,1)}, bf16[2,32,4096]{2,1,0:T(8,128)(2,1)}, u32[]{:S(2)}, u32[]{:S(2)}) collective-permute-start(bf16[2,32,4096]{2,1,0:T(8,128)(2,1)} %bitcast.19.rest_4_), channel_id=1, source_target_pairs={{0,1},{1,0},{2,3},{3,2},{4,5},{5,4},{6,7},{7,6},{8,9},{9,8},{10,11... | collective-permute-start | bytes 1572872 | tf_op jit(solution)/shard_map/ppermute | solution.py:591
  19.5 0.0 collective-permute-done.10.rest_4_.refs_4_
  19.5 0.0 collective-permute-start.4
  19.5 3.2 %collective-permute-done.8.rest_2_.refs_2_ = bf16[32,4224]{1,0:T(8,128)(2,1)S(1)} collective-permute-done((bf16[32,4224]{1,0:T(8,128)(2,1)S(1)}, bf16[32,4224]{1,0:T(8,128)(2,1)S(1)}, u32[]{:S(2)}, u32[]{:S(2)}) %collective-permute-start.8) | collective-permute-done | bytes 270368 | tf_op jit(solution)/shard_map/ppermute | solution.py:579
  22.7 0.5 collective-permute-start.5
  23.2 0.0 collective-permute-start.6
  23.2 0.0 collective-permute-done.2.rest_3_
  23.2 0.5 collective-permute-start.7
  23.7 0.1 collective-permute-start.13
  23.8 0.4 collective-permute-start.11
  24.3 0.8 collective-permute-done.5.rest_9_
  25.1 0.4 collective-permute-start.9
  25.5 0.4 collective-permute-done.6.rest_11_
  25.9 0.0 copy-start.10
  25.9 0.2 collective-permute-done.7.rest_1_.refs_1_
  26.1 0.4 collective-permute-done.13.rest_7_.refs_7_
  26.5 0.4 collective-permute-done.11.rest_5_.refs_5_
  26.9 0.4 collective-permute-done.9.rest_3_.refs_3_
  27.3 0.1 most_live.1
  27.4 0.6 copy-done
  28.1 0.7 conditional.1
  28.1 0.7 broadcast.169
  28.7 9.6 %all-to-all-start.4 = ((bf16[64,24,256]{2,1,0:T(8,128)(2,1)}), bf16[64,24,256]{2,1,0:T(8,128)(2,1)S(1)}, u32[]{:S(2)}, u32[]{:S(2)}) async-start(bf16[64,24,256]{2,1,0:T(8,128)(2,1)} %get-tuple-element.437), calls=%async_computation.4 | async-start | bytes 1572864 | tf_op jit(solution)/shard_map/all_to_all | solution.py:587
  38.4 15.2 %all-to-all-done.4 = bf16[64,24,256]{2,1,0:T(8,128)(2,1)S(1)} async-done(((bf16[64,24,256]{2,1,0:T(8,128)(2,1)}), bf16[64,24,256]{2,1,0:T(8,128)(2,1)S(1)}, u32[]{:S(2)}, u32[]{:S(2)}) %all-to-all-start.4) | async-done | bytes 786464 | tf_op jit(solution)/shard_map/all_to_all | solution.py:587
  53.5 3.9 %shard_map.149 = bf16[4,24,384]{2,1,0:T(8,128)(2,1)} custom-call(s32[1]{0:T(128)} %bitcast.14.core_ref, bf16[16,96,256]{2,1,0:T(8,128)(2,1)S(1)} %bitcast.158, f32[2,4096]{1,0:T(2,128)S(1)} %copy-done.2, bf16[2,32,4096]{2,1,0:T(8,128)(2,1)} %bitcast.17.rest_0_, bf16[2,32,4096]{2,1,0:T(8,128)(2,1)} %collective-permute-done.1.rest_1_, ...), custom_call_target="tpu_custom_call" | custom-call | flops 2147483648 | bytes 8388608 | tf_op jit(solution)/shard_map/pallas_call | solution.py:120
  57.4 3.3 %all-to-all-start.5 = ((bf16[4,24,384]{2,1,0:T(8,128)(2,1)}), bf16[4,24,384]{2,1,0:T(8,128)(2,1)S(1)}, u32[]{:S(2)}, u32[]{:S(2)}) async-start(bf16[4,24,384]{2,1,0:T(8,128)(2,1)} %shard_map.149), calls=%async_computation.5 | async-start | bytes 147456 | tf_op jit(solution)/shard_map/all_to_all | solution.py:608
  60.8 2.8 %shard_map.150.table_ref = bf16[6,256,256]{2,1,0:T(8,128)(2,1)S(1)} custom-call(s32[32]{0:T(128)S(1)} %copy-done.8, f32[2,32,4,64,64]{4,3,2,1,0:T(8,128)} %state_ref.7), custom_call_target="tpu_custom_call" | custom-call | flops 2147483648 | bytes 8388608 | tf_op jit(solution)/shard_map/pallas_call | solution.py:172
  63.5 1.7 %all-to-all-done.5.arrived_ref = bf16[4,24,384]{2,1,0:T(8,128)(2,1)S(1)} async-done(((bf16[4,24,384]{2,1,0:T(8,128)(2,1)}), bf16[4,24,384]{2,1,0:T(8,128)(2,1)S(1)}, u32[]{:S(2)}, u32[]{:S(2)}) %all-to-all-start.5) | async-done | bytes 73760 | tf_op jit(solution)/shard_map/all_to_all | solution.py:608
  65.2 1.9 %shard_map.151 = (bf16[16,24,256]{2,1,0:T(8,128)(2,1)}, f32[24,256]{1,0:T(8,128)S(1)}) custom-call(bf16[4,24,384]{2,1,0:T(8,128)(2,1)S(1)} %all-to-all-done.5.arrived_ref, s32[1,32]{1,0:T(1,128)S(1)} %bitcast.169, f32[2,256]{1,0:T(2,128)S(1)} %copy-done.4, f32[2,256]{1,0:T(2,128)S(1)} %copy-done.5, f32[2,256]{1,0:T(2,128)S(1)} %copy-done.10, ...), custom_call_target="tpu_custom_call" | custom-call | flops 2147483648 | bytes 8388608 | tf_op jit(solution)/shard_map/pallas_call | solution.py:264
  67.2 3.5 %all-to-all-start.6 = ((bf16[16,24,256]{2,1,0:T(8,128)(2,1)}), bf16[16,24,256]{2,1,0:T(8,128)(2,1)S(1)}, u32[]{:S(2)}, u32[]{:S(2)}) async-start(bf16[16,24,256]{2,1,0:T(8,128)(2,1)} %get-tuple-element.438), calls=%async_computation.6 | async-start | bytes 393216 | tf_op jit(solution)/shard_map/all_to_all | solution.py:612
  70.7 0.1 stack.35.starts_ref
  70.8 7.0 %all-to-all-done.6.acts_ref = bf16[16,24,256]{2,1,0:T(8,128)(2,1)S(1)} async-done(((bf16[16,24,256]{2,1,0:T(8,128)(2,1)}), bf16[16,24,256]{2,1,0:T(8,128)(2,1)S(1)}, u32[]{:S(2)}, u32[]{:S(2)}) %all-to-all-start.6) | async-done | bytes 196640 | tf_op jit(solution)/shard_map/all_to_all | solution.py:612
  77.8 1.0 copy-done.1
  78.8 4.0 %finish_0.1 = bf16[64,24,256]{2,1,0:T(8,128)(2,1)} custom-call(s32[8]{0:T(128)S(1)} %stack.35.starts_ref, bf16[16,24,256]{2,1,0:T(8,128)(2,1)S(1)} %all-to-all-done.6.acts_ref, bf16[32,4224]{1,0:T(8,128)(2,1)S(1)} %pad_maximum_fusion.rest_0_.refs_0_, bf16[32,4224]{1,0:T(8,128)(2,1)S(1)} %collective-permute-done.7.rest_1_.refs_1_, ...), custom_call_target="tpu_custom_call" | custom-call | flops 2147483648 | bytes 8388608 | tf_op jit(solution)/shard_map/finish_0/pallas_call | solution.py:459
  82.8 5.1 %all-to-all-start.7 = ((bf16[64,24,256]{2,1,0:T(8,128)(2,1)}), bf16[64,24,256]{2,1,0:T(8,128)(2,1)S(1)}, u32[]{:S(2)}, u32[]{:S(2)}) async-start(bf16[64,24,256]{2,1,0:T(8,128)(2,1)} %finish_0.1), calls=%async_computation.7 | async-start | bytes 1572864 | tf_op jit(solution)/shard_map/all_to_all | solution.py:618
  87.8 0.0 copy-start.3
  87.8 2.3 %collective-permute-start.19 = (bf16[32,4096]{1,0:T(8,128)(2,1)S(1)}, bf16[32,4096]{1,0:T(8,128)(2,1)S(1)}, u32[]{:S(2)}, u32[]{:S(2)}) collective-permute-start(bf16[32,4096]{1,0:T(8,128)(2,1)S(1)} %get-tuple-element.561.rest_0_), channel_id=1, source_target_pairs={{0,6},{2,0},{4,2},{6,4},{1,7},{3,1},{5,3},{7,5},{8,14},{10,8},{12,... | collective-permute-start | bytes 786440 | tf_op jit(solution)/shard_map/ppermute | solution.py:579
  90.1 0.6 collective-permute-start.17
  90.7 0.6 collective-permute-start.15
  91.3 5.0 %collective-permute-start.14 = (bf16[32,4096]{1,0:T(8,128)(2,1)S(1)}, bf16[32,4096]{1,0:T(8,128)(2,1)S(1)}, u32[]{:S(2)}, u32[]{:S(2)}) collective-permute-start(bf16[32,4096]{1,0:T(8,128)(2,1)S(1)} %get-tuple-element.561.rest_0_), channel_id=1, source_target_pairs={{0,1},{1,0},{2,3},{3,2},{4,5},{5,4},{6,7},{7,6},{8,9},{9,8},{10,11... | collective-permute-start | bytes 786440 | tf_op jit(solution)/shard_map/ppermute | solution.py:584
  96.2 2.8 %shard_map.153.table_ref = bf16[6,256,256]{2,1,0:T(8,128)(2,1)S(1)} custom-call(s32[32]{0:T(128)S(1)} %copy-done.9, f32[2,32,4,64,64]{4,3,2,1,0:T(8,128)} %state_ref.7), custom_call_target="tpu_custom_call" | custom-call | flops 2147483648 | bytes 8388608 | tf_op jit(solution)/shard_map/pallas_call | solution.py:172
  99.0 0.6 collective-permute-done.19.rest_6_
  99.7 7.5 %collective-permute-start.20 = (bf16[32,4096]{1,0:T(8,128)(2,1)S(1)}, bf16[32,4096]{1,0:T(8,128)(2,1)S(1)}, u32[]{:S(2)}, u32[]{:S(2)}) collective-permute-start(bf16[32,4096]{1,0:T(8,128)(2,1)S(1)} %collective-permute-done.19.rest_6_), channel_id=1, source_target_pairs={{0,1},{1,0},{2,3},{3,2},{4,5},{5,4},{6,7},{7,6},{8,9},{9,8},{10,11... | collective-permute-start | bytes 786440 | tf_op jit(solution)/shard_map/ppermute | solution.py:584
  107.2 1.5 %collective-permute-start.18 = (bf16[32,4096]{1,0:T(8,128)(2,1)S(1)}, bf16[32,4096]{1,0:T(8,128)(2,1)S(1)}, u32[]{:S(2)}, u32[]{:S(2)}) collective-permute-start(bf16[32,4096]{1,0:T(8,128)(2,1)S(1)} %collective-permute-done.17.rest_4_), channel_id=1, source_target_pairs={{0,1},{1,0},{2,3},{3,2},{4,5},{5,4},{6,7},{7,6},{8,9},{9,8},{10,11... | collective-permute-start | bytes 786440 | tf_op jit(solution)/shard_map/ppermute | solution.py:584
  108.7 2.5 %collective-permute-start.16 = (bf16[32,4096]{1,0:T(8,128)(2,1)S(1)}, bf16[32,4096]{1,0:T(8,128)(2,1)}, u32[]{:S(2)}, u32[]{:S(2)}) collective-permute-start(bf16[32,4096]{1,0:T(8,128)(2,1)S(1)} %collective-permute-done.15.rest_2_), channel_id=1, source_target_pairs={{0,1},{1,0},{2,3},{3,2},{4,5},{5,4},{6,7},{7,6},{8,9},{9,8},{10,11... | collective-permute-start | bytes 786440 | tf_op jit(solution)/shard_map/ppermute | solution.py:584
  111.2 0.0 all-to-all-done.7
  111.2 3.9 %shard_map.152 = bf16[4,24,384]{2,1,0:T(8,128)(2,1)} custom-call(s32[1]{0:T(128)} %bitcast.14.core_ref, bf16[16,96,256]{2,1,0:T(8,128)(2,1)S(1)} %bitcast.157, f32[2,4096]{1,0:T(2,128)S(1)} %copy-done.3, bf16[2,32,4096]{2,1,0:T(8,128)(2,1)} %bitcast.17.rest_0_, bf16[2,32,4096]{2,1,0:T(8,128)(2,1)} %collective-permute-done.1.rest_1_, ...), custom_call_target="tpu_custom_call" | custom-call | flops 2147483648 | bytes 8388608 | tf_op jit(solution)/shard_map/pallas_call | solution.py:120
  115.1 3.3 %all-to-all-start.8 = ((bf16[4,24,384]{2,1,0:T(8,128)(2,1)}), bf16[4,24,384]{2,1,0:T(8,128)(2,1)S(1)}, u32[]{:S(2)}, u32[]{:S(2)}) async-start(bf16[4,24,384]{2,1,0:T(8,128)(2,1)} %shard_map.152), calls=%async_computation.8 | async-start | bytes 147456 | tf_op jit(solution)/shard_map/all_to_all | solution.py:608
  118.4 0.0 copy-start.11
  118.4 5.9 %shard_map.155.rest_0_ = f32[2,32,4,64,64]{4,3,2,1,0:T(8,128)} custom-call(s32[32]{0:T(128)S(1)} %copy-done.9, bf16[4,24,384]{2,1,0:T(8,128)(2,1)S(1)} %all-to-all-done.5.arrived_ref, f32[2,256]{1,0:T(2,128)S(1)} %copy-done.4, f32[2,256]{1,0:T(2,128)S(1)} %copy-done.6, f32[24,256]{1,0:T(8,128)S(1)} %get-tuple-element.442.column_ref, ...), custom_call_target="tpu_custom_call" | custom-call | flops 2147483648 | bytes 8388608 | tf_op jit(solution)/shard_map/pallas_call | solution.py:351
  124.3 0.0 all-to-all-done.8.arrived_ref
  124.4 1.9 %shard_map.154 = (bf16[16,24,256]{2,1,0:T(8,128)(2,1)}, f32[24,256]{1,0:T(8,128)S(1)}) custom-call(bf16[4,24,384]{2,1,0:T(8,128)(2,1)S(1)} %all-to-all-done.8.arrived_ref, s32[1,32]{1,0:T(1,128)S(1)} %bitcast.170, f32[2,256]{1,0:T(2,128)S(1)} %copy-done.4, f32[2,256]{1,0:T(2,128)S(1)} %copy-done.6, f32[2,256]{1,0:T(2,128)S(1)} %copy-done.11, ...), custom_call_target="tpu_custom_call" | custom-call | flops 2147483648 | bytes 8388608 | tf_op jit(solution)/shard_map/pallas_call | solution.py:264
  126.3 6.6 %all-to-all-start.9 = ((bf16[16,24,256]{2,1,0:T(8,128)(2,1)}), bf16[16,24,256]{2,1,0:T(8,128)(2,1)S(1)}, u32[]{:S(2)}, u32[]{:S(2)}) async-start(bf16[16,24,256]{2,1,0:T(8,128)(2,1)} %get-tuple-element.440), calls=%async_computation.9 | async-start | bytes 393216 | tf_op jit(solution)/shard_map/all_to_all | solution.py:612
  132.9 5.8 %shard_map.156 = f32[2,32,4,64,64]{4,3,2,1,0:T(8,128)} custom-call(s32[32]{0:T(128)S(1)} %copy-done.9, bf16[4,24,384]{2,1,0:T(8,128)(2,1)S(1)} %all-to-all-done.8.arrived_ref, f32[2,256]{1,0:T(2,128)S(1)} %copy-done.4, f32[2,256]{1,0:T(2,128)S(1)} %copy-done.6, f32[24,256]{1,0:T(8,128)S(1)} %get-tuple-element.441.column_ref, ...), custom_call_target="tpu_custom_call", output_to_operand_aliasing={{}: (7, {})} | custom-call | flops 2147483648 | bytes 8388608 | tf_op jit(solution)/shard_map/pallas_call | solution.py:351
  138.8 1.3 all-to-all-done.9.acts_ref
  140.1 4.3 %finish_1.1 = bf16[32,256]{1,0:T(8,128)(2,1)} custom-call(s32[8]{0:T(128)S(1)} %stack.35.starts_ref, bf16[16,24,256]{2,1,0:T(8,128)(2,1)S(1)} %all-to-all-done.9.acts_ref, s32[1,32]{1,0:T(1,128)S(1)} %bitcast.171, f32[2,8,2048]{2,1,0:T(8,128)} %get-tuple-element.846.others_ref, bf16[32,4096]{1,0:T(8,128)(2,1)S(1)} %get-tuple-element.561.rest_0_, ...), custom_call_target="tpu_custom_call" | custom-call | flops 2147483648 | bytes 8388608 | tf_op jit(solution)/shard_map/finish_1/pallas_call | solution.py:473
  (29 shorter events, 0.1 us)
Async XLA Ops:
  3.7 9.7 %collective-permute-start.12 = (bf16[32,4224]{1,0:T(8,128)(2,1)S(1)}, bf16[32,4224]{1,0:T(8,128)(2,1)S(1)}, u32[]{:S(2)}, u32[]{:S(2)}) collective-permute-start(bf16[32,4224]{1,0:T(8,128)(2,1)S(1)} %pad_maximum_fusion.rest_0_.refs_0_), channel_id=1, source_target_pairs={{0,6},{2,0},{4,2},{6,4},{1,7},{3,1},{5,3},{7,5},{8,14},{10,8},{12,... | collective-permute-start | bytes 811016 | tf_op jit(solution)/shard_map/ppermute | solution.py:579
  7.0 12.5 %collective-permute-start.10 = (bf16[32,4224]{1,0:T(8,128)(2,1)S(1)}, bf16[32,4224]{1,0:T(8,128)(2,1)S(1)}, u32[]{:S(2)}, u32[]{:S(2)}) collective-permute-start(bf16[32,4224]{1,0:T(8,128)(2,1)S(1)} %pad_maximum_fusion.rest_0_.refs_0_), channel_id=1, source_target_pairs={{0,4},{2,6},{4,0},{6,2},{1,5},{3,7},{5,1},{7,3},{8,12},{10,14},{12... | collective-permute-start | bytes 811016 | tf_op jit(solution)/shard_map/ppermute | solution.py:579
  7.5 15.2 %collective-permute-start.8 = (bf16[32,4224]{1,0:T(8,128)(2,1)S(1)}, bf16[32,4224]{1,0:T(8,128)(2,1)S(1)}, u32[]{:S(2)}, u32[]{:S(2)}) collective-permute-start(bf16[32,4224]{1,0:T(8,128)(2,1)S(1)} %pad_maximum_fusion.rest_0_.refs_0_), channel_id=1, source_target_pairs={{0,2},{2,4},{4,6},{6,0},{1,3},{3,5},{5,7},{7,1},{8,10},{10,12},{12... | collective-permute-start | bytes 811016 | tf_op jit(solution)/shard_map/ppermute | solution.py:579
  8.1 15.1 %collective-permute-start.1 = (bf16[2,32,4096]{2,1,0:T(8,128)(2,1)}, bf16[2,32,4096]{2,1,0:T(8,128)(2,1)}, u32[]{:S(2)}, u32[]{:S(2)}) collective-permute-start(bf16[2,32,4096]{2,1,0:T(8,128)(2,1)} %bitcast.17.rest_0_), channel_id=1, source_target_pairs={{0,1},{1,0},{2,3},{3,2},{4,5},{5,4},{6,7},{7,6},{8,9},{9,8},{10,11... | collective-permute-start | bytes 1572872 | tf_op jit(solution)/shard_map/ppermute | solution.py:591
  9.7 13.6 %collective-permute-start.2 = (bf16[2,32,4096]{2,1,0:T(8,128)(2,1)}, bf16[2,32,4096]{2,1,0:T(8,128)(2,1)}, u32[]{:S(2)}, u32[]{:S(2)}) collective-permute-start(bf16[2,32,4096]{2,1,0:T(8,128)(2,1)} %bitcast.18.rest_2_), channel_id=1, source_target_pairs={{0,1},{1,0},{2,3},{3,2},{4,5},{5,4},{6,7},{7,6},{8,9},{9,8},{10,11... | collective-permute-start | bytes 1572872 | tf_op jit(solution)/shard_map/ppermute | solution.py:591
  13.3 10.4 %collective-permute-start.3 = (bf16[2,32,4096]{2,1,0:T(8,128)(2,1)}, bf16[2,32,4096]{2,1,0:T(8,128)(2,1)}, u32[]{:S(2)}, u32[]{:S(2)}) collective-permute-start(bf16[2,32,4096]{2,1,0:T(8,128)(2,1)} %bitcast.19.rest_4_), channel_id=1, source_target_pairs={{0,1},{1,0},{2,3},{3,2},{4,5},{5,4},{6,7},{7,6},{8,9},{9,8},{10,11... | collective-permute-start | bytes 1572872 | tf_op jit(solution)/shard_map/ppermute | solution.py:591
  19.5 4.3 %collective-permute-start.4 = (bf16[2,32,4096]{2,1,0:T(8,128)(2,1)}, bf16[2,32,4096]{2,1,0:T(8,128)(2,1)}, u32[]{:S(2)}, u32[]{:S(2)}) collective-permute-start(bf16[2,32,4096]{2,1,0:T(8,128)(2,1)} %bitcast.20.rest_6_), channel_id=1, source_target_pairs={{0,1},{1,0},{2,3},{3,2},{4,5},{5,4},{6,7},{7,6},{8,9},{9,8},{10,11... | collective-permute-start | bytes 1572872 | tf_op jit(solution)/shard_map/ppermute | solution.py:591
  22.7 2.4 %collective-permute-start.5 = (bf16[2,32,4096]{2,1,0:T(8,128)(2,1)}, bf16[2,32,4096]{2,1,0:T(8,128)(2,1)}, u32[]{:S(2)}, u32[]{:S(2)}) collective-permute-start(bf16[2,32,4096]{2,1,0:T(8,128)(2,1)} %bitcast.21.rest_8_), channel_id=1, source_target_pairs={{0,1},{1,0},{2,3},{3,2},{4,5},{5,4},{6,7},{7,6},{8,9},{9,8},{10,11... | collective-permute-start | bytes 1572872 | tf_op jit(solution)/shard_map/ppermute | solution.py:591
  23.2 2.6 %collective-permute-start.6 = (bf16[2,32,4096]{2,1,0:T(8,128)(2,1)}, bf16[2,32,4096]{2,1,0:T(8,128)(2,1)}, u32[]{:S(2)}, u32[]{:S(2)}) collective-permute-start(bf16[2,32,4096]{2,1,0:T(8,128)(2,1)} %bitcast.22.rest_10_), channel_id=1, source_target_pairs={{0,1},{1,0},{2,3},{3,2},{4,5},{5,4},{6,7},{7,6},{8,9},{9,8},{10,11... | collective-permute-start | bytes 1572872 | tf_op jit(solution)/shard_map/ppermute | solution.py:591
  23.2 2.9 %collective-permute-start.7 = (bf16[32,4224]{1,0:T(8,128)(2,1)S(1)}, bf16[32,4224]{1,0:T(8,128)(2,1)S(1)}, u32[]{:S(2)}, u32[]{:S(2)}) collective-permute-start(bf16[32,4224]{1,0:T(8,128)(2,1)S(1)} %pad_maximum_fusion.rest_0_.refs_0_), channel_id=1, source_target_pairs={{0,1},{1,0},{2,3},{3,2},{4,5},{5,4},{6,7},{7,6},{8,9},{9,8},{10,11... | collective-permute-start | bytes 811016 | tf_op jit(solution)/shard_map/ppermute | solution.py:584
  23.7 2.7 %collective-permute-start.13 = (bf16[32,4224]{1,0:T(8,128)(2,1)S(1)}, bf16[32,4224]{1,0:T(8,128)(2,1)S(1)}, u32[]{:S(2)}, u32[]{:S(2)}) collective-permute-start(bf16[32,4224]{1,0:T(8,128)(2,1)S(1)} %collective-permute-done.12.rest_6_.refs_6_), channel_id=1, source_target_pairs={{0,1},{1,0},{2,3},{3,2},{4,5},{5,4},{6,7},{7,6},{8,9},{9,8},{10,11... | collective-permute-start | bytes 811016 | tf_op jit(solution)/shard_map/ppermute | solution.py:584
  23.8 3.0 %collective-permute-start.11 = (bf16[32,4224]{1,0:T(8,128)(2,1)S(1)}, bf16[32,4224]{1,0:T(8,128)(2,1)S(1)}, u32[]{:S(2)}, u32[]{:S(2)}) collective-permute-start(bf16[32,4224]{1,0:T(8,128)(2,1)S(1)} %collective-permute-done.10.rest_4_.refs_4_), channel_id=1, source_target_pairs={{0,1},{1,0},{2,3},{3,2},{4,5},{5,4},{6,7},{7,6},{8,9},{9,8},{10,11... | collective-permute-start | bytes 811016 | tf_op jit(solution)/shard_map/ppermute | solution.py:584
  25.1 2.2 %collective-permute-start.9 = (bf16[32,4224]{1,0:T(8,128)(2,1)S(1)}, bf16[32,4224]{1,0:T(8,128)(2,1)S(1)}, u32[]{:S(2)}, u32[]{:S(2)}) collective-permute-start(bf16[32,4224]{1,0:T(8,128)(2,1)S(1)} %collective-permute-done.8.rest_2_.refs_2_), channel_id=1, source_target_pairs={{0,1},{1,0},{2,3},{3,2},{4,5},{5,4},{6,7},{7,6},{8,9},{9,8},{10,11... | collective-permute-start | bytes 811016 | tf_op jit(solution)/shard_map/ppermute | solution.py:584
  25.8 2.2 %copy-start.2 = (f32[2,4096]{1,0:T(2,128)S(1)}, f32[2,4096]{1,0:T(2,128)}, u32[]{:S(2)}) copy-start(f32[2,4096]{1,0:T(2,128)} %gain_ref.6) | copy-start | bytes 98308
  25.8 2.2 %copy-start.4 = (f32[2,256]{1,0:T(2,128)S(1)}, f32[2,256]{1,0:T(2,128)}, u32[]{:S(2)}) copy-start(f32[2,256]{1,0:T(2,128)} %decay_ref.7) | copy-start | bytes 6148
  25.9 2.2 %copy-start.5 = (f32[2,256]{1,0:T(2,128)S(1)}, f32[2,256]{1,0:T(2,128)}, u32[]{:S(2)}) copy-start(f32[2,256]{1,0:T(2,128)} %rate_ref.7) | copy-start | bytes 6148
  25.9 2.2 %copy-start.7 = (bf16[32,256]{1,0:T(8,128)(2,1)S(1)}, bf16[32,256]{1,0:T(8,128)(2,1)}, u32[]{:S(2)}) copy-start(bf16[32,256]{1,0:T(8,128)(2,1)} %tokens_ref.1) | copy-start | bytes 49156
  25.9 2.2 %copy-start.8 = (s32[32]{0:T(128)S(1)}, s32[32]{0:T(128)}, u32[]{:S(2)}) copy-start(s32[32]{0:T(128)} %lengths_ref.7) | copy-start | bytes 388
  25.9 2.2 %copy-start.10 = (f32[2,256]{1,0:T(2,128)S(1)}, f32[2,256]{1,0:T(2,128)}, u32[]{:S(2)}) copy-start(f32[2,256]{1,0:T(2,128)} %gain_ref.7) | copy-start | bytes 6148
  27.3 0.7 copy-start
  28.7 24.8 %all-to-all-start.4 = ((bf16[64,24,256]{2,1,0:T(8,128)(2,1)}), bf16[64,24,256]{2,1,0:T(8,128)(2,1)S(1)}, u32[]{:S(2)}, u32[]{:S(2)}) async-start(bf16[64,24,256]{2,1,0:T(8,128)(2,1)} %get-tuple-element.437), calls=%async_computation.4 | async-start | bytes 1572864 | tf_op jit(solution)/shard_map/all_to_all | solution.py:587
  57.4 7.8 %all-to-all-start.5 = ((bf16[4,24,384]{2,1,0:T(8,128)(2,1)}), bf16[4,24,384]{2,1,0:T(8,128)(2,1)S(1)}, u32[]{:S(2)}, u32[]{:S(2)}) async-start(bf16[4,24,384]{2,1,0:T(8,128)(2,1)} %shard_map.149), calls=%async_computation.5 | async-start | bytes 147456 | tf_op jit(solution)/shard_map/all_to_all | solution.py:608
  67.2 10.7 %all-to-all-start.6 = ((bf16[16,24,256]{2,1,0:T(8,128)(2,1)}), bf16[16,24,256]{2,1,0:T(8,128)(2,1)S(1)}, u32[]{:S(2)}, u32[]{:S(2)}) async-start(bf16[16,24,256]{2,1,0:T(8,128)(2,1)} %get-tuple-element.438), calls=%async_computation.6 | async-start | bytes 393216 | tf_op jit(solution)/shard_map/all_to_all | solution.py:612
  77.8 1.0 copy-start.1
  78.8 17.5 %copy-start.9 = (s32[32]{0:T(128)S(1)}, s32[32]{0:T(128)}, u32[]{:S(2)}) copy-start(s32[32]{0:T(128)} %lengths_ref.7) | copy-start | bytes 388
  82.8 28.4 %all-to-all-start.7 = ((bf16[64,24,256]{2,1,0:T(8,128)(2,1)}), bf16[64,24,256]{2,1,0:T(8,128)(2,1)S(1)}, u32[]{:S(2)}, u32[]{:S(2)}) async-start(bf16[64,24,256]{2,1,0:T(8,128)(2,1)} %finish_0.1), calls=%async_computation.7 | async-start | bytes 1572864 | tf_op jit(solution)/shard_map/all_to_all | solution.py:618
  87.8 23.4 %copy-start.3 = (f32[2,4096]{1,0:T(2,128)S(1)}, f32[2,4096]{1,0:T(2,128)}, u32[]{:S(2)}) copy-start(f32[2,4096]{1,0:T(2,128)} %gain_ref.6) | copy-start | bytes 98308
  87.8 11.8 %collective-permute-start.19 = (bf16[32,4096]{1,0:T(8,128)(2,1)S(1)}, bf16[32,4096]{1,0:T(8,128)(2,1)S(1)}, u32[]{:S(2)}, u32[]{:S(2)}) collective-permute-start(bf16[32,4096]{1,0:T(8,128)(2,1)S(1)} %get-tuple-element.561.rest_0_), channel_id=1, source_target_pairs={{0,6},{2,0},{4,2},{6,4},{1,7},{3,1},{5,3},{7,5},{8,14},{10,8},{12,... | collective-permute-start | bytes 786440 | tf_op jit(solution)/shard_map/ppermute | solution.py:579
  90.1 17.0 %collective-permute-start.17 = (bf16[32,4096]{1,0:T(8,128)(2,1)S(1)}, bf16[32,4096]{1,0:T(8,128)(2,1)S(1)}, u32[]{:S(2)}, u32[]{:S(2)}) collective-permute-start(bf16[32,4096]{1,0:T(8,128)(2,1)S(1)} %get-tuple-element.561.rest_0_), channel_id=1, source_target_pairs={{0,4},{2,6},{4,0},{6,2},{1,5},{3,7},{5,1},{7,3},{8,12},{10,14},{12... | collective-permute-start | bytes 786440 | tf_op jit(solution)/shard_map/ppermute | solution.py:579
  90.7 18.0 %collective-permute-start.15 = (bf16[32,4096]{1,0:T(8,128)(2,1)S(1)}, bf16[32,4096]{1,0:T(8,128)(2,1)S(1)}, u32[]{:S(2)}, u32[]{:S(2)}) collective-permute-start(bf16[32,4096]{1,0:T(8,128)(2,1)S(1)} %get-tuple-element.561.rest_0_), channel_id=1, source_target_pairs={{0,2},{2,4},{4,6},{6,0},{1,3},{3,5},{5,7},{7,1},{8,10},{10,12},{12... | collective-permute-start | bytes 786440 | tf_op jit(solution)/shard_map/ppermute | solution.py:579
  91.3 47.5 %collective-permute-start.14 = (bf16[32,4096]{1,0:T(8,128)(2,1)S(1)}, bf16[32,4096]{1,0:T(8,128)(2,1)S(1)}, u32[]{:S(2)}, u32[]{:S(2)}) collective-permute-start(bf16[32,4096]{1,0:T(8,128)(2,1)S(1)} %get-tuple-element.561.rest_0_), channel_id=1, source_target_pairs={{0,1},{1,0},{2,3},{3,2},{4,5},{5,4},{6,7},{7,6},{8,9},{9,8},{10,11... | collective-permute-start | bytes 786440 | tf_op jit(solution)/shard_map/ppermute | solution.py:584
  99.7 39.1 %collective-permute-start.20 = (bf16[32,4096]{1,0:T(8,128)(2,1)S(1)}, bf16[32,4096]{1,0:T(8,128)(2,1)S(1)}, u32[]{:S(2)}, u32[]{:S(2)}) collective-permute-start(bf16[32,4096]{1,0:T(8,128)(2,1)S(1)} %collective-permute-done.19.rest_6_), channel_id=1, source_target_pairs={{0,1},{1,0},{2,3},{3,2},{4,5},{5,4},{6,7},{7,6},{8,9},{9,8},{10,11... | collective-permute-start | bytes 786440 | tf_op jit(solution)/shard_map/ppermute | solution.py:584
  107.2 31.6 %collective-permute-start.18 = (bf16[32,4096]{1,0:T(8,128)(2,1)S(1)}, bf16[32,4096]{1,0:T(8,128)(2,1)S(1)}, u32[]{:S(2)}, u32[]{:S(2)}) collective-permute-start(bf16[32,4096]{1,0:T(8,128)(2,1)S(1)} %collective-permute-done.17.rest_4_), channel_id=1, source_target_pairs={{0,1},{1,0},{2,3},{3,2},{4,5},{5,4},{6,7},{7,6},{8,9},{9,8},{10,11... | collective-permute-start | bytes 786440 | tf_op jit(solution)/shard_map/ppermute | solution.py:584
  108.7 30.1 %collective-permute-start.16 = (bf16[32,4096]{1,0:T(8,128)(2,1)S(1)}, bf16[32,4096]{1,0:T(8,128)(2,1)}, u32[]{:S(2)}, u32[]{:S(2)}) collective-permute-start(bf16[32,4096]{1,0:T(8,128)(2,1)S(1)} %collective-permute-done.15.rest_2_), channel_id=1, source_target_pairs={{0,1},{1,0},{2,3},{3,2},{4,5},{5,4},{6,7},{7,6},{8,9},{9,8},{10,11... | collective-permute-start | bytes 786440 | tf_op jit(solution)/shard_map/ppermute | solution.py:584
  111.2 7.2 %copy-start.6 = (f32[2,256]{1,0:T(2,128)S(1)}, f32[2,256]{1,0:T(2,128)}, u32[]{:S(2)}) copy-start(f32[2,256]{1,0:T(2,128)} %rate_ref.7) | copy-start | bytes 6148
  115.1 9.2 %all-to-all-start.8 = ((bf16[4,24,384]{2,1,0:T(8,128)(2,1)}), bf16[4,24,384]{2,1,0:T(8,128)(2,1)S(1)}, u32[]{:S(2)}, u32[]{:S(2)}) async-start(bf16[4,24,384]{2,1,0:T(8,128)(2,1)} %shard_map.152), calls=%async_computation.8 | async-start | bytes 147456 | tf_op jit(solution)/shard_map/all_to_all | solution.py:608
  118.4 5.9 %copy-start.11 = (f32[2,256]{1,0:T(2,128)S(1)}, f32[2,256]{1,0:T(2,128)}, u32[]{:S(2)}) copy-start(f32[2,256]{1,0:T(2,128)} %gain_ref.7) | copy-start | bytes 6148
  126.3 13.8 %all-to-all-start.9 = ((bf16[16,24,256]{2,1,0:T(8,128)(2,1)}), bf16[16,24,256]{2,1,0:T(8,128)(2,1)S(1)}, u32[]{:S(2)}, u32[]{:S(2)}) async-start(bf16[16,24,256]{2,1,0:T(8,128)(2,1)} %get-tuple-element.440), calls=%async_computation.9 | async-start | bytes 393216 | tf_op jit(solution)/shard_map/all_to_all | solution.py:612

commit v2 on v1

--- a/solution.py
+++ b/solution.py
@@ -124,7 +124,7 @@
         out_specs=VMEM,
         scratch_shapes=[
             pltpu.VMEM((wide, depth), jnp.bfloat16),
-            pltpu.SemaphoreType.DMA((4, len(weights))),
+            pltpu.SemaphoreType.DMA((1, len(weights))),
         ],
         cost_estimate=COST,
         compiler_params=LIMIT,
@@ -366,102 +366,66 @@
     )(lengths, arrived, decay_base, rate_base, column, others, in_hbm(state), *map(in_hbm, more))
 
 
-def most_kernel(*refs):
-    weights, (out_ref, counts, sems) = refs[:8], refs[8:]
-    copies = []
-    for idx, weight in enumerate(weights):
-        _, wide = weight.shape
-        copy = pltpu.make_async_copy(
-            weight.at[:, pl.ds(wide - LANES, LANES)], counts.at[idx], sems.at[idx]
-        )
-        copy.start()
-        copies.append(copy)
-    for copy in copies:
-        copy.wait()
-    most = jnp.max(counts[...].astype(jnp.float32), axis=0)
-    out_ref[...] = jnp.max(most, axis=0, keepdims=True)
-
-
-def most_live(weights):
-    return pl.pallas_call(
-        most_kernel,
-        out_shape=jax.ShapeDtypeStruct((1, LANES), jnp.float32),
-        in_specs=[ANY] * len(weights),
-        out_specs=VMEM,
-        scratch_shapes=[
-            pltpu.VMEM((len(weights), weights[0].shape[0], LANES), jnp.bfloat16),
-            pltpu.SemaphoreType.DMA((len(weights),)),
-        ],
-        cost_estimate=COST,
-        compiler_params=LIMIT,
-        name="most_live",
-    )(*weights)
-
-
-def columns_of(starts_ref, acts_ref, weights, held, sems):
+def columns_of(acts_ref, weight):
     blocks, rows, feats = acts_ref.shape
-    wide, depth = held.shape
+    result = jnp.zeros((rows, weight.shape[0]), jnp.float32)
+    for t in range(blocks):
+        result += lax.dot_general(
+            acts_ref[t], weight[:, t * feats : (t + 1) * feats], ROWS_BY_ROWS,
+            preferred_element_type=jnp.float32,
+        )
+    return result
+
+
+def all_columns(starts_ref, acts_ref, weights):
     slim = weights[0].shape[0]
-    chunks = sems.shape[0]
-    copies = []
-    for chunk in range(chunks):
-        span = pl.ds(chunk * (depth // chunks), depth // chunks)
-        for idx, weight in enumerate(weights):
-            start = pl.multiple_of(starts_ref[idx] * slim, slim)
-            copy = pltpu.make_async_copy(
-                weight.at[:, span], held.at[pl.ds(start, slim), span], sems.at[chunk, idx]
-            )
-            copy.start()
-            copies.append(copy)
-    result = jnp.zeros((rows, wide), jnp.float32)
-    for t in range(blocks):
-        if t % (blocks // chunks) == 0:
-            first = t // (blocks // chunks) * len(weights)
-            for copy in copies[first : first + len(weights)]:
-                copy.wait()
-        result += lax.dot_general(
-            acts_ref[t], held[:, t * feats : (t + 1) * feats], ROWS_BY_ROWS,
-            preferred_element_type=jnp.float32,
-        )
-    return result.astype(jnp.bfloat16)
-
-
-def finish_kernel(starts_ref, acts_ref, *rest):
-    weights, (out_ref, held, sems) = rest[:8], rest[8:]
-    result = columns_of(starts_ref, acts_ref, weights, held, sems)
+    wide = slim * len(weights)
+    pieces = [columns_of(acts_ref, weight) for weight in weights]
+    result = jnp.concatenate(pieces, axis=1).astype(jnp.bfloat16)
+    source = lax.broadcasted_iota(jnp.int32, (wide, wide), 0)
+    target = source % slim
+    for idx in range(len(weights)):
+        target += jnp.where(source // slim == idx, starts_ref[idx] * slim, 0)
+    moved = target == lax.broadcasted_iota(jnp.int32, (wide, wide), 1)
+    return jnp.dot(
+        result, jnp.where(moved, 1.0, 0.0).astype(jnp.bfloat16),
+        preferred_element_type=jnp.float32,
+    )
+
+
+def finish_kernel(starts_ref, acts_ref, *refs):
+    weights, (out_ref, most_ref) = refs[:8], refs[8:]
+    depth = acts_ref.shape[0] * acts_ref.shape[2]
+    result = all_columns(starts_ref, acts_ref, weights).astype(jnp.bfloat16)
     for copy in range(out_ref.shape[0]):
         out_ref[copy] = result
-
-
-def place_kernel(starts_ref, acts_ref, lengths_ref, others_ref, *rest):
-    weights, (out_ref, held, sems) = rest[:8], rest[8:]
-    result = columns_of(starts_ref, acts_ref, weights, held, sems)
-    feats = result.shape[1]
-    others = others_ref[1, :, others_ref.shape[2] - feats :]
-    every = jnp.concatenate([result.astype(jnp.float32), others], axis=0)
+    most = weights[0][:, depth:]
+    for weight in weights[1:]:
+        most = jnp.maximum(most, weight[:, depth:])
+    most_ref[...] = jnp.max(most.astype(jnp.float32), axis=0, keepdims=True)
+
+
+def place_kernel(starts_ref, acts_ref, lengths_ref, others_ref, *refs):
+    weights, out_ref = refs[:8], refs[8]
+    result = all_columns(starts_ref, acts_ref, weights)
+    others = others_ref[1, :, others_ref.shape[2] - result.shape[1] :]
+    every = jnp.concatenate([result, others], axis=0).astype(jnp.bfloat16)
     chosen = live_slots(lengths_ref[...], 0, every.shape[0]).astype(jnp.bfloat16)
     out_ref[...] = lax.dot_general(
-        chosen, every.astype(jnp.bfloat16), (((0,), (0,)), ((), ())),
-        preferred_element_type=jnp.float32,
+        chosen, every, (((0,), (0,)), ((), ())), preferred_element_type=jnp.float32
     ).astype(jnp.bfloat16)
-
-
-def column_scratch(acts, weights):
-    depth = acts.shape[0] * acts.shape[2]
-    return [
-        pltpu.VMEM((weights[0].shape[0] * len(weights), depth), jnp.bfloat16),
-        pltpu.SemaphoreType.DMA((4, len(weights))),
-    ]
 
 
 def finish(starts, acts, weights, copies):
     wide = weights[0].shape[0] * len(weights)
     return pl.pallas_call(
         finish_kernel,
-        out_shape=pltpu.HBM((copies, acts.shape[1], wide), jnp.bfloat16),
-        in_specs=[SMEM, VMEM] + [ANY] * len(weights),
-        out_specs=VMEM,
-        scratch_shapes=column_scratch(acts, weights),
+        out_shape=(
+            pltpu.HBM((copies, acts.shape[1], wide), jnp.bfloat16),
+            jax.ShapeDtypeStruct((1, LANES), jnp.float32),
+        ),
+        in_specs=[SMEM, VMEM] + [VMEM] * len(weights),
+        out_specs=(VMEM, VMEM),
         cost_estimate=COST,
         compiler_params=LIMIT,
         name="finish_0",
@@ -473,9 +437,8 @@
     return pl.pallas_call(
         place_kernel,
         out_shape=pltpu.HBM((lengths_row.shape[1], wide), jnp.bfloat16),
-        in_specs=[SMEM] + [VMEM] * 3 + [ANY] * len(weights),
+        in_specs=[SMEM] + [VMEM] * (3 + len(weights)),
         out_specs=VMEM,
-        scratch_shapes=column_scratch(acts, weights),
         cost_estimate=COST,
         compiler_params=LIMIT,
         name="finish_1",
@@ -591,15 +554,8 @@
         weights += [own, lax.ppermute(own, "c", PAIR)]
     states = [table(layer, SLOTS, lengths, state) for layer in range(2)]
     columns = [over_pair(along_x(0, [count])), over_pair(along_x(1, []))]
-    most = most_live(columns[0])
     operands = (
         tokens, lengths_row, norm_gain, weights, w_out, decay_base, rate_base, group_gain, state
-    )
-    others = lax.cond(
-        most[0, 0] > SLOTS,
-        beyond_slots,
-        lambda *_: jnp.zeros((2, rows - SLOTS, 8 * feats), jnp.float32),
-        *operands,
     )
     new_state = None
     for layer in range(2):
@@ -610,12 +566,18 @@
             layer, arrived, lengths_row, decay_base, rate_base, group_gain, states[layer], n_tp
         )
         mixed_all = lax.all_to_all(mixed, TP, 0, 0)
+        if layer == 0:
+            current, most = finish(starts, mixed_all, columns[0], n_chips)
+            others = lax.cond(
+                most[0, 0] > SLOTS,
+                beyond_slots,
+                lambda *_: jnp.zeros((2, rows - SLOTS, 8 * feats), jnp.float32),
+                *operands,
+            )
+            acts = lax.all_to_all(current, CHIPS, 0, 0)
         new_state = update(
             layer, lengths, arrived, decay_base, rate_base, column_terms, others, state, new_state
         )
-        if layer == 0:
-            current = finish(starts, mixed_all, columns[0], n_chips)
-            acts = lax.all_to_all(current, CHIPS, 0, 0)
     return place(starts, mixed_all, lengths_row, others, columns[1]), new_state
 
 

time: 147 us -> 130 us (0.88)
  the two profiles are of different devices: /device:TPU:1 before, /device:TPU:0 now
where the time goes in v2:
time: 130 us; the launch traced here: 129 us
  starting transfers between devices  45.2 us (35%)
  waiting for transfers between devices  40.7 us (31%)
  Pallas kernels  39.2 us (30%)
  local copies, waits for them, and re-layouts  2.48 us (2%)
    all_to_all x1, waiting for transfers between devices, local(): acts = lax.all_to_all(chosen, CHIPS, 0, 0)  15.3 us
    pallas_call x2, Pallas kernels, update(): pl.pallas_call(functools.partial(update_kernel, layer), out_shape=pltpu.H...  15.2 us
    ppermute x6, waiting for transfers between devices, along_x(): lax.ppermute(own, 'x', [(i, (i + k) % n_x) for i in range(n_x)])  14.5 us
    all_to_all x1, starting transfers between devices, local(): acts = lax.all_to_all(chosen, CHIPS, 0, 0)  11.5 us
    all_to_all x2, starting transfers between devices, local(): mixed_all = lax.all_to_all(mixed, TP, 0, 0)  10.4 us
    ppermute x6, starting transfers between devices, along_x(): lax.ppermute(own, 'x', [(i, (i + k) % n_x) for i in range(n_x)])  9.13 us
    all_to_all x2, waiting for transfers between devices, local(): mixed_all = lax.all_to_all(mixed, TP, 0, 0)  8.78 us
    pallas_call x2, Pallas kernels, project(): pl.pallas_call(functools.partial(project_kernel, layer), out_shape=pltpu....  7.14 us
  transfers between devices with their start and end apart: 26, of which 7 were waited for; matrix products, arithmetic and copies ran while one was open for 1% of the time, Pallas kernels for 26%

profile of v2, /device:TPU:0, one launch (start us, length us, event | category | flops | bytes accessed | tf_op | source)
XLA Modules:
  0.0 128.7 jit_solution(17628043977631829381)
XLA Ops:
  0.6 0.0 copy-start
  0.6 0.0 copy-start.2
  0.7 0.0 copy-start.10
  0.7 0.1 collective-permute-start.1
  0.8 0.5 collective-permute-start.2
  1.3 0.1 collective-permute-start.3
  1.4 0.4 collective-permute-start.4
  1.8 0.1 collective-permute-start.5
  1.9 1.9 %choose.1 = (bf16[64,24,256]{2,1,0:T(8,128)(2,1)}, bf16[32,128]{1,0:T(8,128)(2,1)S(1)}) custom-call(s32[1,32]{1,0:T(1,128)} %bitcast.194, bf16[32,256]{1,0:T(8,128)(2,1)} %tokens_ref.1), custom_call_target="tpu_custom_call" | custom-call | tf_op jit(solution)/shard_map/choose/pallas_call | solution.py:61
  3.8 11.5 %all-to-all-start.4 = ((bf16[64,24,256]{2,1,0:T(8,128)(2,1)}), bf16[64,24,256]{2,1,0:T(8,128)(2,1)S(1)}, u32[]{:S(2)}, u32[]{:S(2)}) async-start(bf16[64,24,256]{2,1,0:T(8,128)(2,1)} %get-tuple-element.439), calls=%async_computation.4 | async-start | bytes 1572864 | tf_op jit(solution)/shard_map/all_to_all | solution.py:550
  15.3 1.1 slice_bitcast_fusion
  16.4 0.0 collective-permute-done.1.rest_1_
  16.4 0.2 collective-permute-start.6
  16.6 0.6 copy-done.8
  17.2 0.0 collective-permute-done.2.rest_3_
  17.2 2.9 %collective-permute-start.12 = (bf16[32,4224]{1,0:T(8,128)(2,1)S(1)}, bf16[32,4224]{1,0:T(8,128)(2,1)S(1)}, u32[]{:S(2)}, u32[]{:S(2)}) collective-permute-start(bf16[32,4224]{1,0:T(8,128)(2,1)S(1)} %pad_maximum_fusion.refs_0_), channel_id=1, source_target_pairs={{0,6},{2,0},{4,2},{6,4},{1,7},{3,1},{5,3},{7,5},{8,14},{10,8},{12,... | collective-permute-start | bytes 811016 | tf_op jit(solution)/shard_map/ppermute | solution.py:542
  20.1 0.0 collective-permute-done.3.rest_5_
  20.1 0.9 collective-permute-start.10
  20.9 0.0 collective-permute-done.4.rest_7_
  20.9 0.9 collective-permute-start.8
  21.8 0.0 collective-permute-done.6.rest_11_
  21.8 15.3 %all-to-all-done.4 = bf16[64,24,256]{2,1,0:T(8,128)(2,1)S(1)} async-done(((bf16[64,24,256]{2,1,0:T(8,128)(2,1)}), bf16[64,24,256]{2,1,0:T(8,128)(2,1)S(1)}, u32[]{:S(2)}, u32[]{:S(2)}) %all-to-all-start.4) | async-done | bytes 786464 | tf_op jit(solution)/shard_map/all_to_all | solution.py:550
  37.1 0.0 copy-start.14
  37.1 3.5 %shard_map.149 = bf16[4,24,384]{2,1,0:T(8,128)(2,1)} custom-call(s32[1]{0:T(128)} %bitcast.14.core_ref, bf16[16,96,256]{2,1,0:T(8,128)(2,1)S(1)} %bitcast.157, f32[2,4096]{1,0:T(2,128)S(1)} %copy-done.10, bf16[2,32,4096]{2,1,0:T(8,128)(2,1)S(1)} %bitcast.165, bf16[2,32,4096]{2,1,0:T(8,128)(2,1)} %copy-done.8, bf16[2,32,4096]{2,1,0:T(8,128)(2,1)S(1)} %bitcast.169, ...), custom_call_target="tpu_custom_call" | custom-call | flops 2147483648 | bytes 8388608 | tf_op jit(solution)/shard_map/pallas_call | solution.py:120
  40.6 3.3 %all-to-all-start.5 = ((bf16[4,24,384]{2,1,0:T(8,128)(2,1)}), bf16[4,24,384]{2,1,0:T(8,128)(2,1)S(1)}, u32[]{:S(2)}, u32[]{:S(2)}) async-start(bf16[4,24,384]{2,1,0:T(8,128)(2,1)} %shard_map.149), calls=%async_computation.5 | async-start | bytes 147456 | tf_op jit(solution)/shard_map/all_to_all | solution.py:564
  44.0 0.0 copy-start.12
  44.0 0.0 copy-start.13
  44.0 0.0 copy-start.15
  44.0 2.8 %shard_map.150.table_ref = bf16[6,256,256]{2,1,0:T(8,128)(2,1)S(1)} custom-call(s32[32]{0:T(128)S(1)} %copy-done.14, f32[2,32,4,64,64]{4,3,2,1,0:T(8,128)} %state_ref.7), custom_call_target="tpu_custom_call" | custom-call | flops 2147483648 | bytes 8388608 | tf_op jit(solution)/shard_map/pallas_call | solution.py:172
  46.8 0.1 collective-permute-start.13
  46.9 0.0 collective-permute-done.10.refs_4_
  46.9 0.5 collective-permute-start.11
  47.4 0.1 collective-permute-start.9
  47.5 2.1 %all-to-all-done.5.arrived_ref = bf16[4,24,384]{2,1,0:T(8,128)(2,1)S(1)} async-done(((bf16[4,24,384]{2,1,0:T(8,128)(2,1)}), bf16[4,24,384]{2,1,0:T(8,128)(2,1)S(1)}, u32[]{:S(2)}, u32[]{:S(2)}) %all-to-all-start.5) | async-done | bytes 73760 | tf_op jit(solution)/shard_map/all_to_all | solution.py:564
  49.6 1.9 %shard_map.151 = (bf16[16,24,256]{2,1,0:T(8,128)(2,1)}, f32[24,256]{1,0:T(8,128)S(1)}) custom-call(bf16[4,24,384]{2,1,0:T(8,128)(2,1)S(1)} %all-to-all-done.5.arrived_ref, s32[1,32]{1,0:T(1,128)S(1)} %bitcast.195, f32[2,256]{1,0:T(2,128)S(1)} %copy-done.12, f32[2,256]{1,0:T(2,128)S(1)} %copy-done.13, f32[2,256]{1,0:T(2,128)S(1)} %copy-done.15, ...), custom_call_target="tpu_custom_call" | custom-call | flops 2147483648 | bytes 8388608 | tf_op jit(solution)/shard_map/pallas_call | solution.py:264
  51.5 3.5 %all-to-all-start.6 = ((bf16[16,24,256]{2,1,0:T(8,128)(2,1)}), bf16[16,24,256]{2,1,0:T(8,128)(2,1)S(1)}, u32[]{:S(2)}, u32[]{:S(2)}) async-start(bf16[16,24,256]{2,1,0:T(8,128)(2,1)} %get-tuple-element.440), calls=%async_computation.6 | async-start | bytes 393216 | tf_op jit(solution)/shard_map/all_to_all | solution.py:568
  55.1 0.1 stack.35.starts_ref
  55.2 0.0 copy-start.11
  55.2 0.0 collective-permute-done.7.refs_1_
  55.2 0.0 collective-permute-done.9.refs_3_
  55.2 8.1 %all-to-all-done.6.acts_ref = bf16[16,24,256]{2,1,0:T(8,128)(2,1)S(1)} async-done(((bf16[16,24,256]{2,1,0:T(8,128)(2,1)}), bf16[16,24,256]{2,1,0:T(8,128)(2,1)S(1)}, u32[]{:S(2)}, u32[]{:S(2)}) %all-to-all-start.6) | async-done | bytes 196640 | tf_op jit(solution)/shard_map/all_to_all | solution.py:568
  63.4 2.8 %finish_0.1 = (bf16[64,24,256]{2,1,0:T(8,128)(2,1)}, f32[1,128]{1,0:T(1,128)S(1)}) custom-call(s32[8]{0:T(128)S(1)} %stack.35.starts_ref, bf16[16,24,256]{2,1,0:T(8,128)(2,1)S(1)} %all-to-all-done.6.acts_ref, bf16[32,4224]{1,0:T(8,128)(2,1)S(1)} %pad_maximum_fusion.refs_0_, bf16[32,4224]{1,0:T(8,128)(2,1)S(1)} %collective-permute-done.7.refs_1_, ...), custom_call_target="tpu_custom_call" | custom-call | flops 2147483648 | bytes 8388608 | tf_op jit(solution)/shard_map/finish_0/pallas_call | solution.py:421
  66.2 0.7 conditional.1
  66.2 0.7 broadcast.169
  66.9 5.4 %all-to-all-start.7 = ((bf16[64,24,256]{2,1,0:T(8,128)(2,1)}), bf16[64,24,256]{2,1,0:T(8,128)(2,1)S(1)}, u32[]{:S(2)}, u32[]{:S(2)}) async-start(bf16[64,24,256]{2,1,0:T(8,128)(2,1)} %get-tuple-element.442), calls=%async_computation.7 | async-start | bytes 1572864 | tf_op jit(solution)/shard_map/all_to_all | solution.py:577
  72.3 2.9 %collective-permute-start.19 = (bf16[32,4096]{1,0:T(8,128)(2,1)S(1)}, bf16[32,4096]{1,0:T(8,128)(2,1)S(1)}, u32[]{:S(2)}, u32[]{:S(2)}) collective-permute-start(bf16[32,4096]{1,0:T(8,128)(2,1)S(1)} %get-tuple-element.565.refs_0_), channel_id=1, source_target_pairs={{0,6},{2,0},{4,2},{6,4},{1,7},{3,1},{5,3},{7,5},{8,14},{10,8},{12,... | collective-permute-start | bytes 786440 | tf_op jit(solution)/shard_map/ppermute | solution.py:542
  75.2 0.9 collective-permute-start.17
  76.0 0.9 collective-permute-start.15
  76.9 2.8 %shard_map.153.table_ref = bf16[6,256,256]{2,1,0:T(8,128)(2,1)S(1)} custom-call(s32[32]{0:T(128)S(1)} %copy-done.14, f32[2,32,4,64,64]{4,3,2,1,0:T(8,128)} %state_ref.7), custom_call_target="tpu_custom_call" | custom-call | flops 2147483648 | bytes 8388608 | tf_op jit(solution)/shard_map/pallas_call | solution.py:172
  79.7 9.6 %collective-permute-done.19.refs_6_ = bf16[32,4096]{1,0:T(8,128)(2,1)S(1)} collective-permute-done((bf16[32,4096]{1,0:T(8,128)(2,1)S(1)}, bf16[32,4096]{1,0:T(8,128)(2,1)S(1)}, u32[]{:S(2)}, u32[]{:S(2)}) %collective-permute-start.19) | collective-permute-done | bytes 262176 | tf_op jit(solution)/shard_map/ppermute | solution.py:542
  89.3 0.0 collective-permute-start.20
  89.3 1.5 %collective-permute-done.17.refs_4_ = bf16[32,4096]{1,0:T(8,128)(2,1)S(1)} collective-permute-done((bf16[32,4096]{1,0:T(8,128)(2,1)S(1)}, bf16[32,4096]{1,0:T(8,128)(2,1)S(1)}, u32[]{:S(2)}, u32[]{:S(2)}) %collective-permute-start.17) | collective-permute-done | bytes 262176 | tf_op jit(solution)/shard_map/ppermute | solution.py:542
  90.8 0.0 collective-permute-start.18
  90.8 3.4 %collective-permute-done.15.refs_2_ = bf16[32,4096]{1,0:T(8,128)(2,1)S(1)} collective-permute-done((bf16[32,4096]{1,0:T(8,128)(2,1)S(1)}, bf16[32,4096]{1,0:T(8,128)(2,1)S(1)}, u32[]{:S(2)}, u32[]{:S(2)}) %collective-permute-start.15) | collective-permute-done | bytes 262176 | tf_op jit(solution)/shard_map/ppermute | solution.py:542
  94.2 0.0 collective-permute-start.16
  94.2 3.6 %shard_map.152 = bf16[4,24,384]{2,1,0:T(8,128)(2,1)} custom-call(s32[1]{0:T(128)} %bitcast.14.core_ref, bf16[16,96,256]{2,1,0:T(8,128)(2,1)S(1)} %bitcast.158, f32[2,4096]{1,0:T(2,128)S(1)} %copy-done.11, bf16[2,32,4096]{2,1,0:T(8,128)(2,1)} %bitcast.164, bf16[2,32,4096]{2,1,0:T(8,128)(2,1)} %copy-done.8, bf16[2,32,4096]{2,1,0:T(8,128)(2,1)} %bitcast.168, ...), custom_call_target="tpu_custom_call" | custom-call | flops 2147483648 | bytes 8388608 | tf_op jit(solution)/shard_map/pallas_call | solution.py:120
  97.9 3.3 %all-to-all-start.8 = ((bf16[4,24,384]{2,1,0:T(8,128)(2,1)}), bf16[4,24,384]{2,1,0:T(8,128)(2,1)S(1)}, u32[]{:S(2)}, u32[]{:S(2)}) async-start(bf16[4,24,384]{2,1,0:T(8,128)(2,1)} %shard_map.152), calls=%async_computation.8 | async-start | bytes 147456 | tf_op jit(solution)/shard_map/all_to_all | solution.py:564
  101.2 0.0 copy-start.16
  101.2 7.6 %shard_map.155.rest_0_ = f32[2,32,4,64,64]{4,3,2,1,0:T(8,128)} custom-call(s32[32]{0:T(128)S(1)} %copy-done.14, bf16[4,24,384]{2,1,0:T(8,128)(2,1)S(1)} %all-to-all-done.5.arrived_ref, f32[2,256]{1,0:T(2,128)S(1)} %copy-done.12, f32[2,256]{1,0:T(2,128)S(1)} %copy-done.13, f32[24,256]{1,0:T(8,128)S(1)} %get-tuple-element.446.column_ref, ...), custom_call_target="tpu_custom_call" | custom-call | flops 2147483648 | bytes 8388608 | tf_op jit(solution)/shard_map/pallas_call | solution.py:351
  108.8 1.9 %shard_map.154 = (bf16[16,24,256]{2,1,0:T(8,128)(2,1)}, f32[24,256]{1,0:T(8,128)S(1)}) custom-call(bf16[4,24,384]{2,1,0:T(8,128)(2,1)S(1)} %all-to-all-done.8.arrived_ref, s32[1,32]{1,0:T(1,128)S(1)} %bitcast.197, f32[2,256]{1,0:T(2,128)S(1)} %copy-done.12, f32[2,256]{1,0:T(2,128)S(1)} %copy-done.13, f32[2,256]{1,0:T(2,128)S(1)} %copy-done.16, ...), custom_call_target="tpu_custom_call" | custom-call | flops 2147483648 | bytes 8388608 | tf_op jit(solution)/shard_map/pallas_call | solution.py:264
  110.8 6.9 %all-to-all-start.9 = ((bf16[16,24,256]{2,1,0:T(8,128)(2,1)}), bf16[16,24,256]{2,1,0:T(8,128)(2,1)S(1)}, u32[]{:S(2)}, u32[]{:S(2)}) async-start(bf16[16,24,256]{2,1,0:T(8,128)(2,1)} %get-tuple-element.443), calls=%async_computation.9 | async-start | bytes 393216 | tf_op jit(solution)/shard_map/all_to_all | solution.py:568
  117.7 7.6 %shard_map.156 = f32[2,32,4,64,64]{4,3,2,1,0:T(8,128)} custom-call(s32[32]{0:T(128)S(1)} %copy-done.14, bf16[4,24,384]{2,1,0:T(8,128)(2,1)S(1)} %all-to-all-done.8.arrived_ref, f32[2,256]{1,0:T(2,128)S(1)} %copy-done.12, f32[2,256]{1,0:T(2,128)S(1)} %copy-done.13, f32[24,256]{1,0:T(8,128)S(1)} %get-tuple-element.445.column_ref, ...), custom_call_target="tpu_custom_call", output_to_operand_aliasing={{}: (7, {})} | custom-call | flops 2147483648 | bytes 8388608 | tf_op jit(solution)/shard_map/pallas_call | solution.py:351
  125.4 0.7 all-to-all-done.9.acts_ref
  126.0 2.6 %finish_1.1 = bf16[32,256]{1,0:T(8,128)(2,1)} custom-call(s32[8]{0:T(128)S(1)} %stack.35.starts_ref, bf16[16,24,256]{2,1,0:T(8,128)(2,1)S(1)} %all-to-all-done.9.acts_ref, s32[1,32]{1,0:T(1,128)S(1)} %bitcast.198, f32[2,8,2048]{2,1,0:T(8,128)} %get-tuple-element.850.others_ref, bf16[32,4096]{1,0:T(8,128)(2,1)S(1)} %get-tuple-element.565.refs_0_, ...), custom_call_target="tpu_custom_call" | custom-call | flops 2147483648 | bytes 8388608 | tf_op jit(solution)/shard_map/finish_1/pallas_call | solution.py:437
  (28 shorter events, 0.1 us)
Async XLA Ops:
  0.6 36.5 %copy-start = (bf16[2,4096,32]{1,2,0:T(8,128)(2,1)S(1)}, bf16[2,4096,32]{1,2,0:T(8,128)(2,1)}, u32[]{:S(2)}) copy-start(bf16[2,4096,32]{1,2,0:T(8,128)(2,1)} %param.21) | copy-start | bytes 1572868
  0.6 36.5 %copy-start.2 = (bf16[2,4096,32]{1,2,0:T(8,128)(2,1)S(1)}, bf16[2,4096,32]{1,2,0:T(8,128)(2,1)}, u32[]{:S(2)}) copy-start(bf16[2,4096,32]{1,2,0:T(8,128)(2,1)} %param.22) | copy-start | bytes 1572868
  0.7 36.5 %copy-start.10 = (f32[2,4096]{1,0:T(2,128)S(1)}, f32[2,4096]{1,0:T(2,128)}, u32[]{:S(2)}) copy-start(f32[2,4096]{1,0:T(2,128)} %gain_ref.6) | copy-start | bytes 98308
  0.7 15.7 %collective-permute-start.1 = (bf16[2,32,4096]{2,1,0:T(8,128)(2,1)}, bf16[2,32,4096]{2,1,0:T(8,128)(2,1)S(1)}, u32[]{:S(2)}, u32[]{:S(2)}) collective-permute-start(bf16[2,32,4096]{2,1,0:T(8,128)(2,1)} %bitcast.163), channel_id=1, source_target_pairs={{0,1},{1,0},{2,3},{3,2},{4,5},{5,4},{6,7},{7,6},{8,9},{9,8},{10,11... | collective-permute-start | bytes 1572872 | tf_op jit(solution)/shard_map/ppermute | solution.py:554
  0.8 16.5 %collective-permute-start.2 = (bf16[2,32,4096]{2,1,0:T(8,128)(2,1)}, bf16[2,32,4096]{2,1,0:T(8,128)(2,1)}, u32[]{:S(2)}, u32[]{:S(2)}) collective-permute-start(bf16[2,32,4096]{2,1,0:T(8,128)(2,1)} %bitcast.167), channel_id=1, source_target_pairs={{0,1},{1,0},{2,3},{3,2},{4,5},{5,4},{6,7},{7,6},{8,9},{9,8},{10,11... | collective-permute-start | bytes 1572872 | tf_op jit(solution)/shard_map/ppermute | solution.py:554
  1.3 18.8 %collective-permute-start.3 = (bf16[2,32,4096]{2,1,0:T(8,128)(2,1)}, bf16[2,32,4096]{2,1,0:T(8,128)(2,1)}, u32[]{:S(2)}, u32[]{:S(2)}) collective-permute-start(bf16[2,32,4096]{2,1,0:T(8,128)(2,1)} %bitcast.171), channel_id=1, source_target_pairs={{0,1},{1,0},{2,3},{3,2},{4,5},{5,4},{6,7},{7,6},{8,9},{9,8},{10,11... | collective-permute-start | bytes 1572872 | tf_op jit(solution)/shard_map/ppermute | solution.py:554
  1.4 19.6 %collective-permute-start.4 = (bf16[2,32,4096]{2,1,0:T(8,128)(2,1)}, bf16[2,32,4096]{2,1,0:T(8,128)(2,1)}, u32[]{:S(2)}, u32[]{:S(2)}) collective-permute-start(bf16[2,32,4096]{2,1,0:T(8,128)(2,1)} %bitcast.175), channel_id=1, source_target_pairs={{0,1},{1,0},{2,3},{3,2},{4,5},{5,4},{6,7},{7,6},{8,9},{9,8},{10,11... | collective-permute-start | bytes 1572872 | tf_op jit(solution)/shard_map/ppermute | solution.py:554
  1.8 20.0 %collective-permute-start.5 = (bf16[2,32,4096]{2,1,0:T(8,128)(2,1)}, bf16[2,32,4096]{2,1,0:T(8,128)(2,1)}, u32[]{:S(2)}, u32[]{:S(2)}) collective-permute-start(bf16[2,32,4096]{2,1,0:T(8,128)(2,1)} %bitcast.179), channel_id=1, source_target_pairs={{0,1},{1,0},{2,3},{3,2},{4,5},{5,4},{6,7},{7,6},{8,9},{9,8},{10,11... | collective-permute-start | bytes 1572872 | tf_op jit(solution)/shard_map/ppermute | solution.py:554
  3.8 33.4 %all-to-all-start.4 = ((bf16[64,24,256]{2,1,0:T(8,128)(2,1)}), bf16[64,24,256]{2,1,0:T(8,128)(2,1)S(1)}, u32[]{:S(2)}, u32[]{:S(2)}) async-start(bf16[64,24,256]{2,1,0:T(8,128)(2,1)} %get-tuple-element.439), calls=%async_computation.4 | async-start | bytes 1572864 | tf_op jit(solution)/shard_map/all_to_all | solution.py:550
  16.4 0.8 copy-start.8
  16.4 5.4 %collective-permute-start.6 = (bf16[2,32,4096]{2,1,0:T(8,128)(2,1)}, bf16[2,32,4096]{2,1,0:T(8,128)(2,1)}, u32[]{:S(2)}, u32[]{:S(2)}) collective-permute-start(bf16[2,32,4096]{2,1,0:T(8,128)(2,1)} %bitcast.183), channel_id=1, source_target_pairs={{0,1},{1,0},{2,3},{3,2},{4,5},{5,4},{6,7},{7,6},{8,9},{9,8},{10,11... | collective-permute-start | bytes 1572872 | tf_op jit(solution)/shard_map/ppermute | solution.py:554
  17.2 29.6 %collective-permute-start.12 = (bf16[32,4224]{1,0:T(8,128)(2,1)S(1)}, bf16[32,4224]{1,0:T(8,128)(2,1)S(1)}, u32[]{:S(2)}, u32[]{:S(2)}) collective-permute-start(bf16[32,4224]{1,0:T(8,128)(2,1)S(1)} %pad_maximum_fusion.refs_0_), channel_id=1, source_target_pairs={{0,6},{2,0},{4,2},{6,4},{1,7},{3,1},{5,3},{7,5},{8,14},{10,8},{12,... | collective-permute-start | bytes 811016 | tf_op jit(solution)/shard_map/ppermute | solution.py:542
  20.1 26.8 %collective-permute-start.10 = (bf16[32,4224]{1,0:T(8,128)(2,1)S(1)}, bf16[32,4224]{1,0:T(8,128)(2,1)S(1)}, u32[]{:S(2)}, u32[]{:S(2)}) collective-permute-start(bf16[32,4224]{1,0:T(8,128)(2,1)S(1)} %pad_maximum_fusion.refs_0_), channel_id=1, source_target_pairs={{0,4},{2,6},{4,0},{6,2},{1,5},{3,7},{5,1},{7,3},{8,12},{10,14},{12... | collective-permute-start | bytes 811016 | tf_op jit(solution)/shard_map/ppermute | solution.py:542
  20.9 26.5 %collective-permute-start.8 = (bf16[32,4224]{1,0:T(8,128)(2,1)S(1)}, bf16[32,4224]{1,0:T(8,128)(2,1)S(1)}, u32[]{:S(2)}, u32[]{:S(2)}) collective-permute-start(bf16[32,4224]{1,0:T(8,128)(2,1)S(1)} %pad_maximum_fusion.refs_0_), channel_id=1, source_target_pairs={{0,2},{2,4},{4,6},{6,0},{1,3},{3,5},{5,7},{7,1},{8,10},{10,12},{12... | collective-permute-start | bytes 811016 | tf_op jit(solution)/shard_map/ppermute | solution.py:542
  21.8 33.4 %collective-permute-start.7 = (bf16[32,4224]{1,0:T(8,128)(2,1)S(1)}, bf16[32,4224]{1,0:T(8,128)(2,1)S(1)}, u32[]{:S(2)}, u32[]{:S(2)}) collective-permute-start(bf16[32,4224]{1,0:T(8,128)(2,1)S(1)} %pad_maximum_fusion.refs_0_), channel_id=1, source_target_pairs={{0,1},{1,0},{2,3},{3,2},{4,5},{5,4},{6,7},{7,6},{8,9},{9,8},{10,11... | collective-permute-start | bytes 811016 | tf_op jit(solution)/shard_map/ppermute | solution.py:547
  37.1 6.8 %copy-start.14 = (s32[32]{0:T(128)S(1)}, s32[32]{0:T(128)}, u32[]{:S(2)}) copy-start(s32[32]{0:T(128)} %lengths_ref.7) | copy-start | bytes 388
  40.6 8.9 %all-to-all-start.5 = ((bf16[4,24,384]{2,1,0:T(8,128)(2,1)}), bf16[4,24,384]{2,1,0:T(8,128)(2,1)S(1)}, u32[]{:S(2)}, u32[]{:S(2)}) async-start(bf16[4,24,384]{2,1,0:T(8,128)(2,1)} %shard_map.149), calls=%async_computation.5 | async-start | bytes 147456 | tf_op jit(solution)/shard_map/all_to_all | solution.py:564
  44.0 5.6 %copy-start.12 = (f32[2,256]{1,0:T(2,128)S(1)}, f32[2,256]{1,0:T(2,128)}, u32[]{:S(2)}) copy-start(f32[2,256]{1,0:T(2,128)} %decay_ref.7) | copy-start | bytes 6148
  44.0 5.6 %copy-start.13 = (f32[2,256]{1,0:T(2,128)S(1)}, f32[2,256]{1,0:T(2,128)}, u32[]{:S(2)}) copy-start(f32[2,256]{1,0:T(2,128)} %rate_ref.7) | copy-start | bytes 6148
  44.0 5.6 %copy-start.15 = (f32[2,256]{1,0:T(2,128)S(1)}, f32[2,256]{1,0:T(2,128)}, u32[]{:S(2)}) copy-start(f32[2,256]{1,0:T(2,128)} %gain_ref.7) | copy-start | bytes 6148
  46.8 8.4 %collective-permute-start.13 = (bf16[32,4224]{1,0:T(8,128)(2,1)S(1)}, bf16[32,4224]{1,0:T(8,128)(2,1)S(1)}, u32[]{:S(2)}, u32[]{:S(2)}) collective-permute-start(bf16[32,4224]{1,0:T(8,128)(2,1)S(1)} %collective-permute-done.12.refs_6_), channel_id=1, source_target_pairs={{0,1},{1,0},{2,3},{3,2},{4,5},{5,4},{6,7},{7,6},{8,9},{9,8},{10,11... | collective-permute-start | bytes 811016 | tf_op jit(solution)/shard_map/ppermute | solution.py:547
  46.9 8.3 %collective-permute-start.11 = (bf16[32,4224]{1,0:T(8,128)(2,1)S(1)}, bf16[32,4224]{1,0:T(8,128)(2,1)S(1)}, u32[]{:S(2)}, u32[]{:S(2)}) collective-permute-start(bf16[32,4224]{1,0:T(8,128)(2,1)S(1)} %collective-permute-done.10.refs_4_), channel_id=1, source_target_pairs={{0,1},{1,0},{2,3},{3,2},{4,5},{5,4},{6,7},{7,6},{8,9},{9,8},{10,11... | collective-permute-start | bytes 811016 | tf_op jit(solution)/shard_map/ppermute | solution.py:547
  47.4 7.8 %collective-permute-start.9 = (bf16[32,4224]{1,0:T(8,128)(2,1)S(1)}, bf16[32,4224]{1,0:T(8,128)(2,1)}, u32[]{:S(2)}, u32[]{:S(2)}) collective-permute-start(bf16[32,4224]{1,0:T(8,128)(2,1)S(1)} %collective-permute-done.8.refs_2_), channel_id=1, source_target_pairs={{0,1},{1,0},{2,3},{3,2},{4,5},{5,4},{6,7},{7,6},{8,9},{9,8},{10,11... | collective-permute-start | bytes 811016 | tf_op jit(solution)/shard_map/ppermute | solution.py:547
  51.5 11.8 %all-to-all-start.6 = ((bf16[16,24,256]{2,1,0:T(8,128)(2,1)}), bf16[16,24,256]{2,1,0:T(8,128)(2,1)S(1)}, u32[]{:S(2)}, u32[]{:S(2)}) async-start(bf16[16,24,256]{2,1,0:T(8,128)(2,1)} %get-tuple-element.440), calls=%async_computation.6 | async-start | bytes 393216 | tf_op jit(solution)/shard_map/all_to_all | solution.py:568
  55.2 11.0 %copy-start.1 = (bf16[2,4096,32]{1,2,0:T(8,128)(2,1)S(1)}, bf16[2,4096,32]{1,2,0:T(8,128)(2,1)}, u32[]{:S(2)}) copy-start(bf16[2,4096,32]{1,2,0:T(8,128)(2,1)} %param.21) | copy-start | bytes 1572868
  55.2 11.0 %copy-start.3 = (bf16[2,4096,32]{1,2,0:T(8,128)(2,1)S(1)}, bf16[2,4096,32]{1,2,0:T(8,128)(2,1)}, u32[]{:S(2)}) copy-start(bf16[2,4096,32]{1,2,0:T(8,128)(2,1)} %param.22) | copy-start | bytes 1572868
  55.2 11.0 %copy-start.11 = (f32[2,4096]{1,0:T(2,128)S(1)}, f32[2,4096]{1,0:T(2,128)}, u32[]{:S(2)}) copy-start(f32[2,4096]{1,0:T(2,128)} %gain_ref.6) | copy-start | bytes 98308
  66.9 27.3 %all-to-all-start.7 = ((bf16[64,24,256]{2,1,0:T(8,128)(2,1)}), bf16[64,24,256]{2,1,0:T(8,128)(2,1)S(1)}, u32[]{:S(2)}, u32[]{:S(2)}) async-start(bf16[64,24,256]{2,1,0:T(8,128)(2,1)} %get-tuple-element.442), calls=%async_computation.7 | async-start | bytes 1572864 | tf_op jit(solution)/shard_map/all_to_all | solution.py:577
  72.3 17.0 %collective-permute-start.19 = (bf16[32,4096]{1,0:T(8,128)(2,1)S(1)}, bf16[32,4096]{1,0:T(8,128)(2,1)S(1)}, u32[]{:S(2)}, u32[]{:S(2)}) collective-permute-start(bf16[32,4096]{1,0:T(8,128)(2,1)S(1)} %get-tuple-element.565.refs_0_), channel_id=1, source_target_pairs={{0,6},{2,0},{4,2},{6,4},{1,7},{3,1},{5,3},{7,5},{8,14},{10,8},{12,... | collective-permute-start | bytes 786440 | tf_op jit(solution)/shard_map/ppermute | solution.py:542
  75.2 15.6 %collective-permute-start.17 = (bf16[32,4096]{1,0:T(8,128)(2,1)S(1)}, bf16[32,4096]{1,0:T(8,128)(2,1)S(1)}, u32[]{:S(2)}, u32[]{:S(2)}) collective-permute-start(bf16[32,4096]{1,0:T(8,128)(2,1)S(1)} %get-tuple-element.565.refs_0_), channel_id=1, source_target_pairs={{0,4},{2,6},{4,0},{6,2},{1,5},{3,7},{5,1},{7,3},{8,12},{10,14},{12... | collective-permute-start | bytes 786440 | tf_op jit(solution)/shard_map/ppermute | solution.py:542
  76.0 18.2 %collective-permute-start.15 = (bf16[32,4096]{1,0:T(8,128)(2,1)S(1)}, bf16[32,4096]{1,0:T(8,128)(2,1)S(1)}, u32[]{:S(2)}, u32[]{:S(2)}) collective-permute-start(bf16[32,4096]{1,0:T(8,128)(2,1)S(1)} %get-tuple-element.565.refs_0_), channel_id=1, source_target_pairs={{0,2},{2,4},{4,6},{6,0},{1,3},{3,5},{5,7},{7,1},{8,10},{10,12},{12... | collective-permute-start | bytes 786440 | tf_op jit(solution)/shard_map/ppermute | solution.py:542
  76.9 48.4 %collective-permute-start.14 = (bf16[32,4096]{1,0:T(8,128)(2,1)S(1)}, bf16[32,4096]{1,0:T(8,128)(2,1)S(1)}, u32[]{:S(2)}, u32[]{:S(2)}) collective-permute-start(bf16[32,4096]{1,0:T(8,128)(2,1)S(1)} %get-tuple-element.565.refs_0_), channel_id=1, source_target_pairs={{0,1},{1,0},{2,3},{3,2},{4,5},{5,4},{6,7},{7,6},{8,9},{9,8},{10,11... | collective-permute-start | bytes 786440 | tf_op jit(solution)/shard_map/ppermute | solution.py:547
  89.3 36.0 %collective-permute-start.20 = (bf16[32,4096]{1,0:T(8,128)(2,1)S(1)}, bf16[32,4096]{1,0:T(8,128)(2,1)S(1)}, u32[]{:S(2)}, u32[]{:S(2)}) collective-permute-start(bf16[32,4096]{1,0:T(8,128)(2,1)S(1)} %collective-permute-done.19.refs_6_), channel_id=1, source_target_pairs={{0,1},{1,0},{2,3},{3,2},{4,5},{5,4},{6,7},{7,6},{8,9},{9,8},{10,11... | collective-permute-start | bytes 786440 | tf_op jit(solution)/shard_map/ppermute | solution.py:547
  90.8 34.5 %collective-permute-start.18 = (bf16[32,4096]{1,0:T(8,128)(2,1)S(1)}, bf16[32,4096]{1,0:T(8,128)(2,1)S(1)}, u32[]{:S(2)}, u32[]{:S(2)}) collective-permute-start(bf16[32,4096]{1,0:T(8,128)(2,1)S(1)} %collective-permute-done.17.refs_4_), channel_id=1, source_target_pairs={{0,1},{1,0},{2,3},{3,2},{4,5},{5,4},{6,7},{7,6},{8,9},{9,8},{10,11... | collective-permute-start | bytes 786440 | tf_op jit(solution)/shard_map/ppermute | solution.py:547
  94.2 31.2 %collective-permute-start.16 = (bf16[32,4096]{1,0:T(8,128)(2,1)S(1)}, bf16[32,4096]{1,0:T(8,128)(2,1)}, u32[]{:S(2)}, u32[]{:S(2)}) collective-permute-start(bf16[32,4096]{1,0:T(8,128)(2,1)S(1)} %collective-permute-done.15.refs_2_), channel_id=1, source_target_pairs={{0,1},{1,0},{2,3},{3,2},{4,5},{5,4},{6,7},{7,6},{8,9},{9,8},{10,11... | collective-permute-start | bytes 786440 | tf_op jit(solution)/shard_map/ppermute | solution.py:547
  97.9 10.9 %all-to-all-start.8 = ((bf16[4,24,384]{2,1,0:T(8,128)(2,1)}), bf16[4,24,384]{2,1,0:T(8,128)(2,1)S(1)}, u32[]{:S(2)}, u32[]{:S(2)}) async-start(bf16[4,24,384]{2,1,0:T(8,128)(2,1)} %shard_map.152), calls=%async_computation.8 | async-start | bytes 147456 | tf_op jit(solution)/shard_map/all_to_all | solution.py:564
  101.2 7.6 %copy-start.16 = (f32[2,256]{1,0:T(2,128)S(1)}, f32[2,256]{1,0:T(2,128)}, u32[]{:S(2)}) copy-start(f32[2,256]{1,0:T(2,128)} %gain_ref.7) | copy-start | bytes 6148
  110.8 15.3 %all-to-all-start.9 = ((bf16[16,24,256]{2,1,0:T(8,128)(2,1)}), bf16[16,24,256]{2,1,0:T(8,128)(2,1)S(1)}, u32[]{:S(2)}, u32[]{:S(2)}) async-start(bf16[16,24,256]{2,1,0:T(8,128)(2,1)} %get-tuple-element.443), calls=%async_computation.9 | async-start | bytes 393216 | tf_op jit(solution)/shard_map/all_to_all | solution.py:568

commit v3 on v2

--- a/solution.py
+++ b/solution.py
@@ -366,37 +366,25 @@
     )(lengths, arrived, decay_base, rate_base, column, others, in_hbm(state), *map(in_hbm, more))
 
 
-def columns_of(acts_ref, weight):
+def all_columns(starts_ref, acts_ref, weights, turned):
     blocks, rows, feats = acts_ref.shape
-    result = jnp.zeros((rows, weight.shape[0]), jnp.float32)
+    slim = weights[0].shape[0]
+    parts = [jnp.zeros((slim, rows), jnp.float32) for _ in weights]
     for t in range(blocks):
-        result += lax.dot_general(
-            acts_ref[t], weight[:, t * feats : (t + 1) * feats], ROWS_BY_ROWS,
-            preferred_element_type=jnp.float32,
-        )
-    return result
-
-
-def all_columns(starts_ref, acts_ref, weights):
-    slim = weights[0].shape[0]
-    wide = slim * len(weights)
-    pieces = [columns_of(acts_ref, weight) for weight in weights]
-    result = jnp.concatenate(pieces, axis=1).astype(jnp.bfloat16)
-    source = lax.broadcasted_iota(jnp.int32, (wide, wide), 0)
-    target = source % slim
-    for idx in range(len(weights)):
-        target += jnp.where(source // slim == idx, starts_ref[idx] * slim, 0)
-    moved = target == lax.broadcasted_iota(jnp.int32, (wide, wide), 1)
-    return jnp.dot(
-        result, jnp.where(moved, 1.0, 0.0).astype(jnp.bfloat16),
-        preferred_element_type=jnp.float32,
-    )
+        span = slice(t * feats, (t + 1) * feats)
+        for idx, weight in enumerate(weights):
+            parts[idx] += lax.dot_general(
+                weight[:, span], acts_ref[t], ROWS_BY_ROWS, preferred_element_type=jnp.float32
+            )
+    for idx, part in enumerate(parts):
+        turned[pl.ds(pl.multiple_of(starts_ref[idx] * slim, slim), slim), :] = part
+    return turned[...].T
 
 
 def finish_kernel(starts_ref, acts_ref, *refs):
-    weights, (out_ref, most_ref) = refs[:8], refs[8:]
+    weights, (out_ref, most_ref, turned) = refs[:8], refs[8:]
     depth = acts_ref.shape[0] * acts_ref.shape[2]
-    result = all_columns(starts_ref, acts_ref, weights).astype(jnp.bfloat16)
+    result = all_columns(starts_ref, acts_ref, weights, turned).astype(jnp.bfloat16)
     for copy in range(out_ref.shape[0]):
         out_ref[copy] = result
     most = weights[0][:, depth:]
@@ -406,10 +394,10 @@
 
 
 def place_kernel(starts_ref, acts_ref, lengths_ref, others_ref, *refs):
-    weights, out_ref = refs[:8], refs[8]
-    result = all_columns(starts_ref, acts_ref, weights)
+    weights, (out_ref, turned) = refs[:8], refs[8:]
+    result = all_columns(starts_ref, acts_ref, weights, turned).astype(jnp.bfloat16)
     others = others_ref[1, :, others_ref.shape[2] - result.shape[1] :]
-    every = jnp.concatenate([result, others], axis=0).astype(jnp.bfloat16)
+    every = jnp.concatenate([result.astype(jnp.float32), others], axis=0).astype(jnp.bfloat16)
     chosen = live_slots(lengths_ref[...], 0, every.shape[0]).astype(jnp.bfloat16)
     out_ref[...] = lax.dot_general(
         chosen, every, (((0,), (0,)), ((), ())), preferred_element_type=jnp.float32
@@ -426,6 +414,7 @@
         ),
         in_specs=[SMEM, VMEM] + [VMEM] * len(weights),
         out_specs=(VMEM, VMEM),
+        scratch_shapes=[pltpu.VMEM((wide, acts.shape[1]), jnp.float32)],
         cost_estimate=COST,
         compiler_params=LIMIT,
         name="finish_0",
@@ -439,6 +428,7 @@
         out_shape=pltpu.HBM((lengths_row.shape[1], wide), jnp.bfloat16),
         in_specs=[SMEM] + [VMEM] * (3 + len(weights)),
         out_specs=VMEM,
+        scratch_shapes=[pltpu.VMEM((wide, acts.shape[1]), jnp.float32)],
         cost_estimate=COST,
         compiler_params=LIMIT,
         name="finish_1",

time: 130 us -> 129 us (level)
  no operation moved by 1% of the time
where the time goes in v3:
time: 129 us; the launch traced here: 128 us
  starting transfers between devices  45.2 us (35%)
  waiting for transfers between devices  40.7 us (32%)
  Pallas kernels  38.9 us (30%)
  local copies, waits for them, and re-layouts  2.48 us (2%)
    all_to_all x1, waiting for transfers between devices, local(): acts = lax.all_to_all(chosen, CHIPS, 0, 0)  15.3 us
    pallas_call x2, Pallas kernels, update(): pl.pallas_call(functools.partial(update_kernel, layer), out_shape=pltpu.H...  15.2 us
    ppermute x6, waiting for transfers between devices, along_x(): lax.ppermute(own, 'x', [(i, (i + k) % n_x) for i in range(n_x)])  14.5 us
    all_to_all x1, starting transfers between devices, local(): acts = lax.all_to_all(chosen, CHIPS, 0, 0)  11.5 us
    all_to_all x2, starting transfers between devices, local(): mixed_all = lax.all_to_all(mixed, TP, 0, 0)  10.4 us
    ppermute x6, starting transfers between devices, along_x(): lax.ppermute(own, 'x', [(i, (i + k) % n_x) for i in range(n_x)])  9.13 us
    all_to_all x2, waiting for transfers between devices, local(): mixed_all = lax.all_to_all(mixed, TP, 0, 0)  8.77 us
    pallas_call x2, Pallas kernels, project(): pl.pallas_call(functools.partial(project_kernel, layer), out_shape=pltpu....  7.14 us
  transfers between devices with their start and end apart: 26, of which 7 were waited for; matrix products, arithmetic and copies ran while one was open for 1% of the time, Pallas kernels for 26%

profile of v3, /device:TPU:0, one launch (start us, length us, event | category | flops | bytes accessed | tf_op | source)
XLA Modules:
  0.0 128.4 jit_solution(3281107101388290881)
XLA Ops:
  0.6 0.0 copy-start
  0.6 0.0 copy-start.2
  0.7 0.0 copy-start.10
  0.7 0.1 collective-permute-start.1
  0.8 0.5 collective-permute-start.2
  1.3 0.1 collective-permute-start.3
  1.4 0.4 collective-permute-start.4
  1.8 0.1 collective-permute-start.5
  1.9 1.9 %choose.1 = (bf16[64,24,256]{2,1,0:T(8,128)(2,1)}, bf16[32,128]{1,0:T(8,128)(2,1)S(1)}) custom-call(s32[1,32]{1,0:T(1,128)} %bitcast.194, bf16[32,256]{1,0:T(8,128)(2,1)} %tokens_ref.1), custom_call_target="tpu_custom_call" | custom-call | tf_op jit(solution)/shard_map/choose/pallas_call | solution.py:61
  3.8 11.5 %all-to-all-start.4 = ((bf16[64,24,256]{2,1,0:T(8,128)(2,1)}), bf16[64,24,256]{2,1,0:T(8,128)(2,1)S(1)}, u32[]{:S(2)}, u32[]{:S(2)}) async-start(bf16[64,24,256]{2,1,0:T(8,128)(2,1)} %get-tuple-element.439), calls=%async_computation.4 | async-start | bytes 1572864 | tf_op jit(solution)/shard_map/all_to_all | solution.py:540
  15.3 1.1 slice_bitcast_fusion
  16.4 0.0 collective-permute-done.1.rest_1_
  16.4 0.2 collective-permute-start.6
  16.6 0.6 copy-done.8
  17.2 0.0 collective-permute-done.2.rest_3_
  17.2 2.9 %collective-permute-start.12 = (bf16[32,4224]{1,0:T(8,128)(2,1)S(1)}, bf16[32,4224]{1,0:T(8,128)(2,1)S(1)}, u32[]{:S(2)}, u32[]{:S(2)}) collective-permute-start(bf16[32,4224]{1,0:T(8,128)(2,1)S(1)} %pad_maximum_fusion.refs_0_), channel_id=1, source_target_pairs={{0,6},{2,0},{4,2},{6,4},{1,7},{3,1},{5,3},{7,5},{8,14},{10,8},{12,... | collective-permute-start | bytes 811016 | tf_op jit(solution)/shard_map/ppermute | solution.py:532
  20.1 0.0 collective-permute-done.3.rest_5_
  20.1 0.9 collective-permute-start.10
  20.9 0.0 collective-permute-done.4.rest_7_
  20.9 0.9 collective-permute-start.8
  21.8 0.0 collective-permute-done.6.rest_11_
  21.8 15.3 %all-to-all-done.4 = bf16[64,24,256]{2,1,0:T(8,128)(2,1)S(1)} async-done(((bf16[64,24,256]{2,1,0:T(8,128)(2,1)}), bf16[64,24,256]{2,1,0:T(8,128)(2,1)S(1)}, u32[]{:S(2)}, u32[]{:S(2)}) %all-to-all-start.4) | async-done | bytes 786464 | tf_op jit(solution)/shard_map/all_to_all | solution.py:540
  37.1 0.0 copy-start.14
  37.1 3.5 %shard_map.149 = bf16[4,24,384]{2,1,0:T(8,128)(2,1)} custom-call(s32[1]{0:T(128)} %bitcast.14.core_ref, bf16[16,96,256]{2,1,0:T(8,128)(2,1)S(1)} %bitcast.157, f32[2,4096]{1,0:T(2,128)S(1)} %copy-done.10, bf16[2,32,4096]{2,1,0:T(8,128)(2,1)S(1)} %bitcast.165, bf16[2,32,4096]{2,1,0:T(8,128)(2,1)} %copy-done.8, bf16[2,32,4096]{2,1,0:T(8,128)(2,1)S(1)} %bitcast.169, ...), custom_call_target="tpu_custom_call" | custom-call | flops 2147483648 | bytes 8388608 | tf_op jit(solution)/shard_map/pallas_call | solution.py:120
  40.6 3.3 %all-to-all-start.5 = ((bf16[4,24,384]{2,1,0:T(8,128)(2,1)}), bf16[4,24,384]{2,1,0:T(8,128)(2,1)S(1)}, u32[]{:S(2)}, u32[]{:S(2)}) async-start(bf16[4,24,384]{2,1,0:T(8,128)(2,1)} %shard_map.149), calls=%async_computation.5 | async-start | bytes 147456 | tf_op jit(solution)/shard_map/all_to_all | solution.py:554
  44.0 0.0 copy-start.12
  44.0 0.0 copy-start.13
  44.0 0.0 copy-start.15
  44.0 2.8 %shard_map.150.table_ref = bf16[6,256,256]{2,1,0:T(8,128)(2,1)S(1)} custom-call(s32[32]{0:T(128)S(1)} %copy-done.14, f32[2,32,4,64,64]{4,3,2,1,0:T(8,128)} %state_ref.7), custom_call_target="tpu_custom_call" | custom-call | flops 2147483648 | bytes 8388608 | tf_op jit(solution)/shard_map/pallas_call | solution.py:172
  46.8 0.1 collective-permute-start.13
  46.9 0.0 collective-permute-done.10.refs_4_
  46.9 0.5 collective-permute-start.11
  47.4 0.1 collective-permute-start.9
  47.5 2.1 %all-to-all-done.5.arrived_ref = bf16[4,24,384]{2,1,0:T(8,128)(2,1)S(1)} async-done(((bf16[4,24,384]{2,1,0:T(8,128)(2,1)}), bf16[4,24,384]{2,1,0:T(8,128)(2,1)S(1)}, u32[]{:S(2)}, u32[]{:S(2)}) %all-to-all-start.5) | async-done | bytes 73760 | tf_op jit(solution)/shard_map/all_to_all | solution.py:554
  49.6 1.9 %shard_map.151 = (bf16[16,24,256]{2,1,0:T(8,128)(2,1)}, f32[24,256]{1,0:T(8,128)S(1)}) custom-call(bf16[4,24,384]{2,1,0:T(8,128)(2,1)S(1)} %all-to-all-done.5.arrived_ref, s32[1,32]{1,0:T(1,128)S(1)} %bitcast.195, f32[2,256]{1,0:T(2,128)S(1)} %copy-done.12, f32[2,256]{1,0:T(2,128)S(1)} %copy-done.13, f32[2,256]{1,0:T(2,128)S(1)} %copy-done.15, ...), custom_call_target="tpu_custom_call" | custom-call | flops 2147483648 | bytes 8388608 | tf_op jit(solution)/shard_map/pallas_call | solution.py:264
  51.5 3.5 %all-to-all-start.6 = ((bf16[16,24,256]{2,1,0:T(8,128)(2,1)}), bf16[16,24,256]{2,1,0:T(8,128)(2,1)S(1)}, u32[]{:S(2)}, u32[]{:S(2)}) async-start(bf16[16,24,256]{2,1,0:T(8,128)(2,1)} %get-tuple-element.440), calls=%async_computation.6 | async-start | bytes 393216 | tf_op jit(solution)/shard_map/all_to_all | solution.py:558
  55.1 0.1 stack.35.starts_ref
  55.2 0.0 copy-start.11
  55.2 0.0 collective-permute-done.7.refs_1_
  55.2 0.0 collective-permute-done.9.refs_3_
  55.2 8.1 %all-to-all-done.6.acts_ref = bf16[16,24,256]{2,1,0:T(8,128)(2,1)S(1)} async-done(((bf16[16,24,256]{2,1,0:T(8,128)(2,1)}), bf16[16,24,256]{2,1,0:T(8,128)(2,1)S(1)}, u32[]{:S(2)}, u32[]{:S(2)}) %all-to-all-start.6) | async-done | bytes 196640 | tf_op jit(solution)/shard_map/all_to_all | solution.py:558
  63.4 2.7 %finish_0.1 = (bf16[64,24,256]{2,1,0:T(8,128)(2,1)}, f32[1,128]{1,0:T(1,128)S(1)}) custom-call(s32[8]{0:T(128)S(1)} %stack.35.starts_ref, bf16[16,24,256]{2,1,0:T(8,128)(2,1)S(1)} %all-to-all-done.6.acts_ref, bf16[32,4224]{1,0:T(8,128)(2,1)S(1)} %pad_maximum_fusion.refs_0_, bf16[32,4224]{1,0:T(8,128)(2,1)S(1)} %collective-permute-done.7.refs_1_, ...), custom_call_target="tpu_custom_call" | custom-call | flops 2147483648 | bytes 8388608 | tf_op jit(solution)/shard_map/finish_0/pallas_call | solution.py:409
  66.1 0.7 conditional.1
  66.1 0.7 broadcast.169
  66.8 5.4 %all-to-all-start.7 = ((bf16[64,24,256]{2,1,0:T(8,128)(2,1)}), bf16[64,24,256]{2,1,0:T(8,128)(2,1)S(1)}, u32[]{:S(2)}, u32[]{:S(2)}) async-start(bf16[64,24,256]{2,1,0:T(8,128)(2,1)} %get-tuple-element.442), calls=%async_computation.7 | async-start | bytes 1572864 | tf_op jit(solution)/shard_map/all_to_all | solution.py:567
  72.2 2.9 %collective-permute-start.19 = (bf16[32,4096]{1,0:T(8,128)(2,1)S(1)}, bf16[32,4096]{1,0:T(8,128)(2,1)S(1)}, u32[]{:S(2)}, u32[]{:S(2)}) collective-permute-start(bf16[32,4096]{1,0:T(8,128)(2,1)S(1)} %get-tuple-element.565.refs_0_), channel_id=1, source_target_pairs={{0,6},{2,0},{4,2},{6,4},{1,7},{3,1},{5,3},{7,5},{8,14},{10,8},{12,... | collective-permute-start | bytes 786440 | tf_op jit(solution)/shard_map/ppermute | solution.py:532
  75.0 0.9 collective-permute-start.17
  75.9 0.9 collective-permute-start.15
  76.8 0.0 collective-permute-start.14
  76.8 2.8 %shard_map.153.table_ref = bf16[6,256,256]{2,1,0:T(8,128)(2,1)S(1)} custom-call(s32[32]{0:T(128)S(1)} %copy-done.14, f32[2,32,4,64,64]{4,3,2,1,0:T(8,128)} %state_ref.7), custom_call_target="tpu_custom_call" | custom-call | flops 2147483648 | bytes 8388608 | tf_op jit(solution)/shard_map/pallas_call | solution.py:172
  79.6 9.6 %collective-permute-done.19.refs_6_ = bf16[32,4096]{1,0:T(8,128)(2,1)S(1)} collective-permute-done((bf16[32,4096]{1,0:T(8,128)(2,1)S(1)}, bf16[32,4096]{1,0:T(8,128)(2,1)S(1)}, u32[]{:S(2)}, u32[]{:S(2)}) %collective-permute-start.19) | collective-permute-done | bytes 262176 | tf_op jit(solution)/shard_map/ppermute | solution.py:532
  89.2 0.0 collective-permute-start.20
  89.2 1.5 %collective-permute-done.17.refs_4_ = bf16[32,4096]{1,0:T(8,128)(2,1)S(1)} collective-permute-done((bf16[32,4096]{1,0:T(8,128)(2,1)S(1)}, bf16[32,4096]{1,0:T(8,128)(2,1)S(1)}, u32[]{:S(2)}, u32[]{:S(2)}) %collective-permute-start.17) | collective-permute-done | bytes 262176 | tf_op jit(solution)/shard_map/ppermute | solution.py:532
  90.7 0.0 collective-permute-start.18
  90.7 3.4 %collective-permute-done.15.refs_2_ = bf16[32,4096]{1,0:T(8,128)(2,1)S(1)} collective-permute-done((bf16[32,4096]{1,0:T(8,128)(2,1)S(1)}, bf16[32,4096]{1,0:T(8,128)(2,1)S(1)}, u32[]{:S(2)}, u32[]{:S(2)}) %collective-permute-start.15) | collective-permute-done | bytes 262176 | tf_op jit(solution)/shard_map/ppermute | solution.py:532
  94.1 3.6 %shard_map.152 = bf16[4,24,384]{2,1,0:T(8,128)(2,1)} custom-call(s32[1]{0:T(128)} %bitcast.14.core_ref, bf16[16,96,256]{2,1,0:T(8,128)(2,1)S(1)} %bitcast.158, f32[2,4096]{1,0:T(2,128)S(1)} %copy-done.11, bf16[2,32,4096]{2,1,0:T(8,128)(2,1)} %bitcast.164, bf16[2,32,4096]{2,1,0:T(8,128)(2,1)} %copy-done.8, bf16[2,32,4096]{2,1,0:T(8,128)(2,1)} %bitcast.168, ...), custom_call_target="tpu_custom_call" | custom-call | flops 2147483648 | bytes 8388608 | tf_op jit(solution)/shard_map/pallas_call | solution.py:120
  97.7 3.3 %all-to-all-start.8 = ((bf16[4,24,384]{2,1,0:T(8,128)(2,1)}), bf16[4,24,384]{2,1,0:T(8,128)(2,1)S(1)}, u32[]{:S(2)}, u32[]{:S(2)}) async-start(bf16[4,24,384]{2,1,0:T(8,128)(2,1)} %shard_map.152), calls=%async_computation.8 | async-start | bytes 147456 | tf_op jit(solution)/shard_map/all_to_all | solution.py:554
  101.0 0.0 copy-start.16
  101.0 7.6 %shard_map.155.rest_0_ = f32[2,32,4,64,64]{4,3,2,1,0:T(8,128)} custom-call(s32[32]{0:T(128)S(1)} %copy-done.14, bf16[4,24,384]{2,1,0:T(8,128)(2,1)S(1)} %all-to-all-done.5.arrived_ref, f32[2,256]{1,0:T(2,128)S(1)} %copy-done.12, f32[2,256]{1,0:T(2,128)S(1)} %copy-done.13, f32[24,256]{1,0:T(8,128)S(1)} %get-tuple-element.446.column_ref, ...), custom_call_target="tpu_custom_call" | custom-call | flops 2147483648 | bytes 8388608 | tf_op jit(solution)/shard_map/pallas_call | solution.py:351
  108.7 1.9 %shard_map.154 = (bf16[16,24,256]{2,1,0:T(8,128)(2,1)}, f32[24,256]{1,0:T(8,128)S(1)}) custom-call(bf16[4,24,384]{2,1,0:T(8,128)(2,1)S(1)} %all-to-all-done.8.arrived_ref, s32[1,32]{1,0:T(1,128)S(1)} %bitcast.197, f32[2,256]{1,0:T(2,128)S(1)} %copy-done.12, f32[2,256]{1,0:T(2,128)S(1)} %copy-done.13, f32[2,256]{1,0:T(2,128)S(1)} %copy-done.16, ...), custom_call_target="tpu_custom_call" | custom-call | flops 2147483648 | bytes 8388608 | tf_op jit(solution)/shard_map/pallas_call | solution.py:264
  110.6 6.9 %all-to-all-start.9 = ((bf16[16,24,256]{2,1,0:T(8,128)(2,1)}), bf16[16,24,256]{2,1,0:T(8,128)(2,1)S(1)}, u32[]{:S(2)}, u32[]{:S(2)}) async-start(bf16[16,24,256]{2,1,0:T(8,128)(2,1)} %get-tuple-element.443), calls=%async_computation.9 | async-start | bytes 393216 | tf_op jit(solution)/shard_map/all_to_all | solution.py:558
  117.6 7.6 %shard_map.156 = f32[2,32,4,64,64]{4,3,2,1,0:T(8,128)} custom-call(s32[32]{0:T(128)S(1)} %copy-done.14, bf16[4,24,384]{2,1,0:T(8,128)(2,1)S(1)} %all-to-all-done.8.arrived_ref, f32[2,256]{1,0:T(2,128)S(1)} %copy-done.12, f32[2,256]{1,0:T(2,128)S(1)} %copy-done.13, f32[24,256]{1,0:T(8,128)S(1)} %get-tuple-element.445.column_ref, ...), custom_call_target="tpu_custom_call", output_to_operand_aliasing={{}: (7, {})} | custom-call | flops 2147483648 | bytes 8388608 | tf_op jit(solution)/shard_map/pallas_call | solution.py:351
  125.2 0.7 all-to-all-done.9.acts_ref
  125.9 2.5 %finish_1.1 = bf16[32,256]{1,0:T(8,128)(2,1)} custom-call(s32[8]{0:T(128)S(1)} %stack.35.starts_ref, bf16[16,24,256]{2,1,0:T(8,128)(2,1)S(1)} %all-to-all-done.9.acts_ref, s32[1,32]{1,0:T(1,128)S(1)} %bitcast.198, f32[2,8,2048]{2,1,0:T(8,128)} %get-tuple-element.850.others_ref, bf16[32,4096]{1,0:T(8,128)(2,1)S(1)} %get-tuple-element.565.refs_0_, ...), custom_call_target="tpu_custom_call" | custom-call | flops 2147483648 | bytes 8388608 | tf_op jit(solution)/shard_map/finish_1/pallas_call | solution.py:426
  (28 shorter events, 0.1 us)
Async XLA Ops:
  0.6 36.5 %copy-start = (bf16[2,4096,32]{1,2,0:T(8,128)(2,1)S(1)}, bf16[2,4096,32]{1,2,0:T(8,128)(2,1)}, u32[]{:S(2)}) copy-start(bf16[2,4096,32]{1,2,0:T(8,128)(2,1)} %param.21) | copy-start | bytes 1572868
  0.6 36.5 %copy-start.2 = (bf16[2,4096,32]{1,2,0:T(8,128)(2,1)S(1)}, bf16[2,4096,32]{1,2,0:T(8,128)(2,1)}, u32[]{:S(2)}) copy-start(bf16[2,4096,32]{1,2,0:T(8,128)(2,1)} %param.22) | copy-start | bytes 1572868
  0.7 36.5 %copy-start.10 = (f32[2,4096]{1,0:T(2,128)S(1)}, f32[2,4096]{1,0:T(2,128)}, u32[]{:S(2)}) copy-start(f32[2,4096]{1,0:T(2,128)} %gain_ref.6) | copy-start | bytes 98308
  0.7 15.7 %collective-permute-start.1 = (bf16[2,32,4096]{2,1,0:T(8,128)(2,1)}, bf16[2,32,4096]{2,1,0:T(8,128)(2,1)S(1)}, u32[]{:S(2)}, u32[]{:S(2)}) collective-permute-start(bf16[2,32,4096]{2,1,0:T(8,128)(2,1)} %bitcast.163), channel_id=1, source_target_pairs={{0,1},{1,0},{2,3},{3,2},{4,5},{5,4},{6,7},{7,6},{8,9},{9,8},{10,11... | collective-permute-start | bytes 1572872 | tf_op jit(solution)/shard_map/ppermute | solution.py:544
  0.8 16.5 %collective-permute-start.2 = (bf16[2,32,4096]{2,1,0:T(8,128)(2,1)}, bf16[2,32,4096]{2,1,0:T(8,128)(2,1)}, u32[]{:S(2)}, u32[]{:S(2)}) collective-permute-start(bf16[2,32,4096]{2,1,0:T(8,128)(2,1)} %bitcast.167), channel_id=1, source_target_pairs={{0,1},{1,0},{2,3},{3,2},{4,5},{5,4},{6,7},{7,6},{8,9},{9,8},{10,11... | collective-permute-start | bytes 1572872 | tf_op jit(solution)/shard_map/ppermute | solution.py:544
  1.3 18.8 %collective-permute-start.3 = (bf16[2,32,4096]{2,1,0:T(8,128)(2,1)}, bf16[2,32,4096]{2,1,0:T(8,128)(2,1)}, u32[]{:S(2)}, u32[]{:S(2)}) collective-permute-start(bf16[2,32,4096]{2,1,0:T(8,128)(2,1)} %bitcast.171), channel_id=1, source_target_pairs={{0,1},{1,0},{2,3},{3,2},{4,5},{5,4},{6,7},{7,6},{8,9},{9,8},{10,11... | collective-permute-start | bytes 1572872 | tf_op jit(solution)/shard_map/ppermute | solution.py:544
  1.4 19.6 %collective-permute-start.4 = (bf16[2,32,4096]{2,1,0:T(8,128)(2,1)}, bf16[2,32,4096]{2,1,0:T(8,128)(2,1)}, u32[]{:S(2)}, u32[]{:S(2)}) collective-permute-start(bf16[2,32,4096]{2,1,0:T(8,128)(2,1)} %bitcast.175), channel_id=1, source_target_pairs={{0,1},{1,0},{2,3},{3,2},{4,5},{5,4},{6,7},{7,6},{8,9},{9,8},{10,11... | collective-permute-start | bytes 1572872 | tf_op jit(solution)/shard_map/ppermute | solution.py:544
  1.8 20.0 %collective-permute-start.5 = (bf16[2,32,4096]{2,1,0:T(8,128)(2,1)}, bf16[2,32,4096]{2,1,0:T(8,128)(2,1)}, u32[]{:S(2)}, u32[]{:S(2)}) collective-permute-start(bf16[2,32,4096]{2,1,0:T(8,128)(2,1)} %bitcast.179), channel_id=1, source_target_pairs={{0,1},{1,0},{2,3},{3,2},{4,5},{5,4},{6,7},{7,6},{8,9},{9,8},{10,11... | collective-permute-start | bytes 1572872 | tf_op jit(solution)/shard_map/ppermute | solution.py:544
  3.8 33.4 %all-to-all-start.4 = ((bf16[64,24,256]{2,1,0:T(8,128)(2,1)}), bf16[64,24,256]{2,1,0:T(8,128)(2,1)S(1)}, u32[]{:S(2)}, u32[]{:S(2)}) async-start(bf16[64,24,256]{2,1,0:T(8,128)(2,1)} %get-tuple-element.439), calls=%async_computation.4 | async-start | bytes 1572864 | tf_op jit(solution)/shard_map/all_to_all | solution.py:540
  16.4 0.8 copy-start.8
  16.4 5.4 %collective-permute-start.6 = (bf16[2,32,4096]{2,1,0:T(8,128)(2,1)}, bf16[2,32,4096]{2,1,0:T(8,128)(2,1)}, u32[]{:S(2)}, u32[]{:S(2)}) collective-permute-start(bf16[2,32,4096]{2,1,0:T(8,128)(2,1)} %bitcast.183), channel_id=1, source_target_pairs={{0,1},{1,0},{2,3},{3,2},{4,5},{5,4},{6,7},{7,6},{8,9},{9,8},{10,11... | collective-permute-start | bytes 1572872 | tf_op jit(solution)/shard_map/ppermute | solution.py:544
  17.2 29.6 %collective-permute-start.12 = (bf16[32,4224]{1,0:T(8,128)(2,1)S(1)}, bf16[32,4224]{1,0:T(8,128)(2,1)S(1)}, u32[]{:S(2)}, u32[]{:S(2)}) collective-permute-start(bf16[32,4224]{1,0:T(8,128)(2,1)S(1)} %pad_maximum_fusion.refs_0_), channel_id=1, source_target_pairs={{0,6},{2,0},{4,2},{6,4},{1,7},{3,1},{5,3},{7,5},{8,14},{10,8},{12,... | collective-permute-start | bytes 811016 | tf_op jit(solution)/shard_map/ppermute | solution.py:532
  20.1 26.8 %collective-permute-start.10 = (bf16[32,4224]{1,0:T(8,128)(2,1)S(1)}, bf16[32,4224]{1,0:T(8,128)(2,1)S(1)}, u32[]{:S(2)}, u32[]{:S(2)}) collective-permute-start(bf16[32,4224]{1,0:T(8,128)(2,1)S(1)} %pad_maximum_fusion.refs_0_), channel_id=1, source_target_pairs={{0,4},{2,6},{4,0},{6,2},{1,5},{3,7},{5,1},{7,3},{8,12},{10,14},{12... | collective-permute-start | bytes 811016 | tf_op jit(solution)/shard_map/ppermute | solution.py:532
  20.9 26.5 %collective-permute-start.8 = (bf16[32,4224]{1,0:T(8,128)(2,1)S(1)}, bf16[32,4224]{1,0:T(8,128)(2,1)S(1)}, u32[]{:S(2)}, u32[]{:S(2)}) collective-permute-start(bf16[32,4224]{1,0:T(8,128)(2,1)S(1)} %pad_maximum_fusion.refs_0_), channel_id=1, source_target_pairs={{0,2},{2,4},{4,6},{6,0},{1,3},{3,5},{5,7},{7,1},{8,10},{10,12},{12... | collective-permute-start | bytes 811016 | tf_op jit(solution)/shard_map/ppermute | solution.py:532
  21.8 33.4 %collective-permute-start.7 = (bf16[32,4224]{1,0:T(8,128)(2,1)S(1)}, bf16[32,4224]{1,0:T(8,128)(2,1)S(1)}, u32[]{:S(2)}, u32[]{:S(2)}) collective-permute-start(bf16[32,4224]{1,0:T(8,128)(2,1)S(1)} %pad_maximum_fusion.refs_0_), channel_id=1, source_target_pairs={{0,1},{1,0},{2,3},{3,2},{4,5},{5,4},{6,7},{7,6},{8,9},{9,8},{10,11... | collective-permute-start | bytes 811016 | tf_op jit(solution)/shard_map/ppermute | solution.py:537
  37.1 6.8 %copy-start.14 = (s32[32]{0:T(128)S(1)}, s32[32]{0:T(128)}, u32[]{:S(2)}) copy-start(s32[32]{0:T(128)} %lengths_ref.7) | copy-start | bytes 388
  40.6 8.9 %all-to-all-start.5 = ((bf16[4,24,384]{2,1,0:T(8,128)(2,1)}), bf16[4,24,384]{2,1,0:T(8,128)(2,1)S(1)}, u32[]{:S(2)}, u32[]{:S(2)}) async-start(bf16[4,24,384]{2,1,0:T(8,128)(2,1)} %shard_map.149), calls=%async_computation.5 | async-start | bytes 147456 | tf_op jit(solution)/shard_map/all_to_all | solution.py:554
  44.0 5.6 %copy-start.12 = (f32[2,256]{1,0:T(2,128)S(1)}, f32[2,256]{1,0:T(2,128)}, u32[]{:S(2)}) copy-start(f32[2,256]{1,0:T(2,128)} %decay_ref.7) | copy-start | bytes 6148
  44.0 5.6 %copy-start.13 = (f32[2,256]{1,0:T(2,128)S(1)}, f32[2,256]{1,0:T(2,128)}, u32[]{:S(2)}) copy-start(f32[2,256]{1,0:T(2,128)} %rate_ref.7) | copy-start | bytes 6148
  44.0 5.6 %copy-start.15 = (f32[2,256]{1,0:T(2,128)S(1)}, f32[2,256]{1,0:T(2,128)}, u32[]{:S(2)}) copy-start(f32[2,256]{1,0:T(2,128)} %gain_ref.7) | copy-start | bytes 6148
  46.8 8.4 %collective-permute-start.13 = (bf16[32,4224]{1,0:T(8,128)(2,1)S(1)}, bf16[32,4224]{1,0:T(8,128)(2,1)S(1)}, u32[]{:S(2)}, u32[]{:S(2)}) collective-permute-start(bf16[32,4224]{1,0:T(8,128)(2,1)S(1)} %collective-permute-done.12.refs_6_), channel_id=1, source_target_pairs={{0,1},{1,0},{2,3},{3,2},{4,5},{5,4},{6,7},{7,6},{8,9},{9,8},{10,11... | collective-permute-start | bytes 811016 | tf_op jit(solution)/shard_map/ppermute | solution.py:537
  46.9 8.3 %collective-permute-start.11 = (bf16[32,4224]{1,0:T(8,128)(2,1)S(1)}, bf16[32,4224]{1,0:T(8,128)(2,1)S(1)}, u32[]{:S(2)}, u32[]{:S(2)}) collective-permute-start(bf16[32,4224]{1,0:T(8,128)(2,1)S(1)} %collective-permute-done.10.refs_4_), channel_id=1, source_target_pairs={{0,1},{1,0},{2,3},{3,2},{4,5},{5,4},{6,7},{7,6},{8,9},{9,8},{10,11... | collective-permute-start | bytes 811016 | tf_op jit(solution)/shard_map/ppermute | solution.py:537
  47.4 7.8 %collective-permute-start.9 = (bf16[32,4224]{1,0:T(8,128)(2,1)S(1)}, bf16[32,4224]{1,0:T(8,128)(2,1)}, u32[]{:S(2)}, u32[]{:S(2)}) collective-permute-start(bf16[32,4224]{1,0:T(8,128)(2,1)S(1)} %collective-permute-done.8.refs_2_), channel_id=1, source_target_pairs={{0,1},{1,0},{2,3},{3,2},{4,5},{5,4},{6,7},{7,6},{8,9},{9,8},{10,11... | collective-permute-start | bytes 811016 | tf_op jit(solution)/shard_map/ppermute | solution.py:537
  51.5 11.8 %all-to-all-start.6 = ((bf16[16,24,256]{2,1,0:T(8,128)(2,1)}), bf16[16,24,256]{2,1,0:T(8,128)(2,1)S(1)}, u32[]{:S(2)}, u32[]{:S(2)}) async-start(bf16[16,24,256]{2,1,0:T(8,128)(2,1)} %get-tuple-element.440), calls=%async_computation.6 | async-start | bytes 393216 | tf_op jit(solution)/shard_map/all_to_all | solution.py:558
  55.2 10.9 %copy-start.1 = (bf16[2,4096,32]{1,2,0:T(8,128)(2,1)S(1)}, bf16[2,4096,32]{1,2,0:T(8,128)(2,1)}, u32[]{:S(2)}) copy-start(bf16[2,4096,32]{1,2,0:T(8,128)(2,1)} %param.21) | copy-start | bytes 1572868
  55.2 10.9 %copy-start.3 = (bf16[2,4096,32]{1,2,0:T(8,128)(2,1)S(1)}, bf16[2,4096,32]{1,2,0:T(8,128)(2,1)}, u32[]{:S(2)}) copy-start(bf16[2,4096,32]{1,2,0:T(8,128)(2,1)} %param.22) | copy-start | bytes 1572868
  55.2 10.9 %copy-start.11 = (f32[2,4096]{1,0:T(2,128)S(1)}, f32[2,4096]{1,0:T(2,128)}, u32[]{:S(2)}) copy-start(f32[2,4096]{1,0:T(2,128)} %gain_ref.6) | copy-start | bytes 98308
  66.8 27.3 %all-to-all-start.7 = ((bf16[64,24,256]{2,1,0:T(8,128)(2,1)}), bf16[64,24,256]{2,1,0:T(8,128)(2,1)S(1)}, u32[]{:S(2)}, u32[]{:S(2)}) async-start(bf16[64,24,256]{2,1,0:T(8,128)(2,1)} %get-tuple-element.442), calls=%async_computation.7 | async-start | bytes 1572864 | tf_op jit(solution)/shard_map/all_to_all | solution.py:567
  72.2 17.0 %collective-permute-start.19 = (bf16[32,4096]{1,0:T(8,128)(2,1)S(1)}, bf16[32,4096]{1,0:T(8,128)(2,1)S(1)}, u32[]{:S(2)}, u32[]{:S(2)}) collective-permute-start(bf16[32,4096]{1,0:T(8,128)(2,1)S(1)} %get-tuple-element.565.refs_0_), channel_id=1, source_target_pairs={{0,6},{2,0},{4,2},{6,4},{1,7},{3,1},{5,3},{7,5},{8,14},{10,8},{12,... | collective-permute-start | bytes 786440 | tf_op jit(solution)/shard_map/ppermute | solution.py:532
  75.0 15.7 %collective-permute-start.17 = (bf16[32,4096]{1,0:T(8,128)(2,1)S(1)}, bf16[32,4096]{1,0:T(8,128)(2,1)S(1)}, u32[]{:S(2)}, u32[]{:S(2)}) collective-permute-start(bf16[32,4096]{1,0:T(8,128)(2,1)S(1)} %get-tuple-element.565.refs_0_), channel_id=1, source_target_pairs={{0,4},{2,6},{4,0},{6,2},{1,5},{3,7},{5,1},{7,3},{8,12},{10,14},{12... | collective-permute-start | bytes 786440 | tf_op jit(solution)/shard_map/ppermute | solution.py:532
  75.9 18.2 %collective-permute-start.15 = (bf16[32,4096]{1,0:T(8,128)(2,1)S(1)}, bf16[32,4096]{1,0:T(8,128)(2,1)S(1)}, u32[]{:S(2)}, u32[]{:S(2)}) collective-permute-start(bf16[32,4096]{1,0:T(8,128)(2,1)S(1)} %get-tuple-element.565.refs_0_), channel_id=1, source_target_pairs={{0,2},{2,4},{4,6},{6,0},{1,3},{3,5},{5,7},{7,1},{8,10},{10,12},{12... | collective-permute-start | bytes 786440 | tf_op jit(solution)/shard_map/ppermute | solution.py:532
  76.8 48.4 %collective-permute-start.14 = (bf16[32,4096]{1,0:T(8,128)(2,1)S(1)}, bf16[32,4096]{1,0:T(8,128)(2,1)S(1)}, u32[]{:S(2)}, u32[]{:S(2)}) collective-permute-start(bf16[32,4096]{1,0:T(8,128)(2,1)S(1)} %get-tuple-element.565.refs_0_), channel_id=1, source_target_pairs={{0,1},{1,0},{2,3},{3,2},{4,5},{5,4},{6,7},{7,6},{8,9},{9,8},{10,11... | collective-permute-start | bytes 786440 | tf_op jit(solution)/shard_map/ppermute | solution.py:537
  89.2 36.0 %collective-permute-start.20 = (bf16[32,4096]{1,0:T(8,128)(2,1)S(1)}, bf16[32,4096]{1,0:T(8,128)(2,1)S(1)}, u32[]{:S(2)}, u32[]{:S(2)}) collective-permute-start(bf16[32,4096]{1,0:T(8,128)(2,1)S(1)} %collective-permute-done.19.refs_6_), channel_id=1, source_target_pairs={{0,1},{1,0},{2,3},{3,2},{4,5},{5,4},{6,7},{7,6},{8,9},{9,8},{10,11... | collective-permute-start | bytes 786440 | tf_op jit(solution)/shard_map/ppermute | solution.py:537
  90.7 34.5 %collective-permute-start.18 = (bf16[32,4096]{1,0:T(8,128)(2,1)S(1)}, bf16[32,4096]{1,0:T(8,128)(2,1)S(1)}, u32[]{:S(2)}, u32[]{:S(2)}) collective-permute-start(bf16[32,4096]{1,0:T(8,128)(2,1)S(1)} %collective-permute-done.17.refs_4_), channel_id=1, source_target_pairs={{0,1},{1,0},{2,3},{3,2},{4,5},{5,4},{6,7},{7,6},{8,9},{9,8},{10,11... | collective-permute-start | bytes 786440 | tf_op jit(solution)/shard_map/ppermute | solution.py:537
  94.1 31.2 %collective-permute-start.16 = (bf16[32,4096]{1,0:T(8,128)(2,1)S(1)}, bf16[32,4096]{1,0:T(8,128)(2,1)}, u32[]{:S(2)}, u32[]{:S(2)}) collective-permute-start(bf16[32,4096]{1,0:T(8,128)(2,1)S(1)} %collective-permute-done.15.refs_2_), channel_id=1, source_target_pairs={{0,1},{1,0},{2,3},{3,2},{4,5},{5,4},{6,7},{7,6},{8,9},{9,8},{10,11... | collective-permute-start | bytes 786440 | tf_op jit(solution)/shard_map/ppermute | solution.py:537
  97.7 10.9 %all-to-all-start.8 = ((bf16[4,24,384]{2,1,0:T(8,128)(2,1)}), bf16[4,24,384]{2,1,0:T(8,128)(2,1)S(1)}, u32[]{:S(2)}, u32[]{:S(2)}) async-start(bf16[4,24,384]{2,1,0:T(8,128)(2,1)} %shard_map.152), calls=%async_computation.8 | async-start | bytes 147456 | tf_op jit(solution)/shard_map/all_to_all | solution.py:554
  101.0 7.7 %copy-start.16 = (f32[2,256]{1,0:T(2,128)S(1)}, f32[2,256]{1,0:T(2,128)}, u32[]{:S(2)}) copy-start(f32[2,256]{1,0:T(2,128)} %gain_ref.7) | copy-start | bytes 6148
  110.6 15.3 %all-to-all-start.9 = ((bf16[16,24,256]{2,1,0:T(8,128)(2,1)}), bf16[16,24,256]{2,1,0:T(8,128)(2,1)S(1)}, u32[]{:S(2)}, u32[]{:S(2)}) async-start(bf16[16,24,256]{2,1,0:T(8,128)(2,1)} %get-tuple-element.443), calls=%async_computation.9 | async-start | bytes 393216 | tf_op jit(solution)/shard_map/all_to_all | solution.py:558

commit v4 on v3

--- a/solution.py
+++ b/solution.py
@@ -282,7 +282,7 @@
 def update_kernel(
     layer, lengths_ref, arrived_ref, decay_ref, rate_ref, column_ref, others_ref, state_ref, *rest
 ):
-    out_ref, held, rows_ref, columns_ref, in_sems, out_sems = rest[-6:]
+    out_ref, held, rows_ref, columns_ref, added_ref, in_sems, out_sems = rest[-7:]
     count, heads, head, _ = held.shape
     chunks = in_sems.shape[0]
     per = count // chunks
@@ -315,22 +315,33 @@
     own = lax.broadcasted_iota(jnp.int32, (heads, heads * head), 0)
     own = own == lax.broadcasted_iota(jnp.int32, (heads, heads * head), 1) // head
 
+    def outer(slot):
+        high, low = in_two(jnp.where(own, columns_ref[pl.ds(slot, 1), :], 0.0))
+        right_high, right_low = in_two(rows_ref[slot, heads:, :])
+        added = lax.dot_general(
+            jnp.concatenate([high, high, low], axis=0),
+            jnp.concatenate([right_high, right_low, right_high], axis=0),
+            (((0,), (0,)), ((), ())), preferred_element_type=jnp.float32,
+        )
+        added_ref[slot] = added.reshape(heads, head, head)
+
+    def tally(r, total):
+        return total + (lengths_ref[r] > STEP).astype(jnp.int32)
+
+    total = lax.fori_loop(0, count, tally, jnp.int32(0))
+
+    @pl.loop(0, (total + 1) // 2)
+    def _(pair):
+        outer(2 * pair)
+        outer(2 * pair + 1)
+
     def advance(r, slot):
         live = lengths_ref[r] > STEP
 
         @pl.when(live)
         def _():
-            high, low = in_two(jnp.where(own, columns_ref[pl.ds(slot, 1), :], 0.0))
-            vectors = rows_ref[slot]
-            right_high, right_low = in_two(vectors[heads:])
-            added = lax.dot_general(
-                jnp.concatenate([high, high, low], axis=0),
-                jnp.concatenate([right_high, right_low, right_high], axis=0),
-                (((0,), (0,)), ((), ())), preferred_element_type=jnp.float32,
-            )
             for h in range(heads):
-                new = held[r, h] * vectors[h : h + 1] + added[h * head : (h + 1) * head]
-                held[r, h] = new
+                held[r, h] = held[r, h] * rows_ref[slot, h : h + 1, :] + added_ref[slot, h]
 
         return slot + live.astype(jnp.int32)
 
@@ -357,6 +368,7 @@
             pltpu.VMEM((count, heads, head, head), jnp.float32),
             pltpu.VMEM((count, 2 * heads, head), jnp.float32),
             pltpu.VMEM((count, heads * head), jnp.float32),
+            pltpu.VMEM((count, heads, head, head), jnp.float32),
             pltpu.SemaphoreType.DMA((8,)),
             pltpu.SemaphoreType.DMA((8,)),
         ],
@@ -528,10 +540,11 @@
 
     def along_x(layer, more):
         own = jnp.concatenate([w_out.swapaxes(1, 2)[layer]] + more, axis=1)
-        return [own] + [
-            lax.ppermute(own, "x", [(i, (i + k) % n_x) for i in range(n_x)])
-            for k in range(1, n_x)
-        ]
+        pieces = [own]
+        for k in range(1, n_x):
+            shift = [(i, (i + k) % n_x) for i in range(n_x)]
+            pieces.append(lax.ppermute(own, "x", shift))
+        return pieces
 
     def over_pair(pieces):
         return [p for piece in pieces for p in (piece, lax.ppermute(piece, "c", PAIR))]

time: 129 us -> 128 us (level)
  the two profiles are of different devices: /device:TPU:0 before, /device:TPU:1 now
where the time goes in v4:
time: 128 us; the launch traced here: 126 us
  starting transfers between devices  63.9 us (50%)
  Pallas kernels  34.5 us (27%)
  waiting for transfers between devices  24.4 us (19%)
  local copies, waits for them, and re-layouts  2.24 us (2%)
    ppermute x8, starting transfers between devices, over_pair(): lax.ppermute(piece, 'c', PAIR)  18.9 us
    all_to_all x1, starting transfers between devices, local(): acts = lax.all_to_all(chosen, CHIPS, 0, 0)  11.2 us
    pallas_call x2, Pallas kernels, update(): pl.pallas_call(functools.partial(update_kernel, layer), out_shape=pltpu.H...  10.9 us
    all_to_all x2, starting transfers between devices, local(): mixed_all = lax.all_to_all(mixed, TP, 0, 0)  10.2 us
    all_to_all x2, waiting for transfers between devices, local(): mixed_all = lax.all_to_all(mixed, TP, 0, 0)  8.66 us
    all_to_all x1, waiting for transfers between devices, local(): acts = lax.all_to_all(chosen, CHIPS, 0, 0)  8.56 us
    all_to_all x1, starting transfers between devices, local(): acts = lax.all_to_all(current, CHIPS, 0, 0)  7.22 us
    ppermute x6, waiting for transfers between devices, along_x(): pieces.append(lax.ppermute(own, 'x', shift))  7.16 us
  transfers between devices with their start and end apart: 26, of which 5 were waited for; matrix products, arithmetic and copies ran while one was open for 1% of the time, Pallas kernels for 23%

profile of v4, /device:TPU:1, one launch (start us, length us, event | category | flops | bytes accessed | tf_op | source)
XLA Modules:
  0.0 126.2 jit_solution(12468757908628206388)
XLA Ops:
  0.6 0.0 copy-start
  0.6 0.0 copy-start.2
  0.7 0.0 copy-start.10
  0.7 1.5 %collective-permute-start.1 = (bf16[2,32,4096]{2,1,0:T(8,128)(2,1)}, bf16[2,32,4096]{2,1,0:T(8,128)(2,1)S(1)}, u32[]{:S(2)}, u32[]{:S(2)}) collective-permute-start(bf16[2,32,4096]{2,1,0:T(8,128)(2,1)} %bitcast.163), channel_id=1, source_target_pairs={{0,1},{1,0},{2,3},{3,2},{4,5},{5,4},{6,7},{7,6},{8,9},{9,8},{10,11... | collective-permute-start | bytes 1572872 | tf_op jit(solution)/shard_map/ppermute | solution.py:557
  2.1 0.1 collective-permute-start.2
  2.2 0.4 collective-permute-start.3
  2.6 0.1 collective-permute-start.4
  2.7 0.4 collective-permute-start.5
  3.1 1.9 %choose.1 = (bf16[64,24,256]{2,1,0:T(8,128)(2,1)}, bf16[32,128]{1,0:T(8,128)(2,1)S(1)}) custom-call(s32[1,32]{1,0:T(1,128)} %bitcast.194, bf16[32,256]{1,0:T(8,128)(2,1)} %tokens_ref.1), custom_call_target="tpu_custom_call" | custom-call | tf_op jit(solution)/shard_map/choose/pallas_call | solution.py:61
  5.0 11.2 %all-to-all-start.4 = ((bf16[64,24,256]{2,1,0:T(8,128)(2,1)}), bf16[64,24,256]{2,1,0:T(8,128)(2,1)S(1)}, u32[]{:S(2)}, u32[]{:S(2)}) async-start(bf16[64,24,256]{2,1,0:T(8,128)(2,1)} %get-tuple-element.439), calls=%async_computation.4 | async-start | bytes 1572864 | tf_op jit(solution)/shard_map/all_to_all | solution.py:553
  16.3 1.1 slice_bitcast_fusion
  17.4 0.0 collective-permute-done.1.rest_1_
  17.4 0.5 collective-permute-start.6
  17.9 0.3 copy-done.8
  18.2 0.0 collective-permute-done.2.rest_3_
  18.2 2.3 %collective-permute-start.12 = (bf16[32,4224]{1,0:T(8,128)(2,1)S(1)}, bf16[32,4224]{1,0:T(8,128)(2,1)S(1)}, u32[]{:S(2)}, u32[]{:S(2)}) collective-permute-start(bf16[32,4224]{1,0:T(8,128)(2,1)S(1)} %pad_maximum_fusion.refs_0_), channel_id=1, source_target_pairs={{0,6},{2,0},{4,2},{6,4},{1,7},{3,1},{5,3},{7,5},{8,14},{10,8},{12,... | collective-permute-start | bytes 811016 | tf_op jit(solution)/shard_map/ppermute | solution.py:546
  20.5 0.0 collective-permute-done.3.rest_5_
  20.5 0.6 collective-permute-start.10
  21.1 0.0 collective-permute-done.4.rest_7_
  21.1 0.6 collective-permute-start.8
  21.7 1.5 %collective-permute-start.7 = (bf16[32,4224]{1,0:T(8,128)(2,1)S(1)}, bf16[32,4224]{1,0:T(8,128)(2,1)S(1)}, u32[]{:S(2)}, u32[]{:S(2)}) collective-permute-start(bf16[32,4224]{1,0:T(8,128)(2,1)S(1)} %pad_maximum_fusion.refs_0_), channel_id=1, source_target_pairs={{0,1},{1,0},{2,3},{3,2},{4,5},{5,4},{6,7},{7,6},{8,9},{9,8},{10,11... | collective-permute-start | bytes 811016 | tf_op jit(solution)/shard_map/ppermute | solution.py:550
  23.2 0.0 collective-permute-done.6.rest_11_
  23.2 8.6 %all-to-all-done.4 = bf16[64,24,256]{2,1,0:T(8,128)(2,1)S(1)} async-done(((bf16[64,24,256]{2,1,0:T(8,128)(2,1)}), bf16[64,24,256]{2,1,0:T(8,128)(2,1)S(1)}, u32[]{:S(2)}, u32[]{:S(2)}) %all-to-all-start.4) | async-done | bytes 786464 | tf_op jit(solution)/shard_map/all_to_all | solution.py:553
  31.8 0.0 copy-start.14
  31.8 3.5 %shard_map.149 = bf16[4,24,384]{2,1,0:T(8,128)(2,1)} custom-call(s32[1]{0:T(128)} %bitcast.14.core_ref, bf16[16,96,256]{2,1,0:T(8,128)(2,1)S(1)} %bitcast.157, f32[2,4096]{1,0:T(2,128)S(1)} %copy-done.10, bf16[2,32,4096]{2,1,0:T(8,128)(2,1)S(1)} %bitcast.165, bf16[2,32,4096]{2,1,0:T(8,128)(2,1)} %copy-done.8, bf16[2,32,4096]{2,1,0:T(8,128)(2,1)S(1)} %bitcast.169, ...), custom_call_target="tpu_custom_call" | custom-call | flops 2147483648 | bytes 8388608 | tf_op jit(solution)/shard_map/pallas_call | solution.py:120
  35.3 3.3 %all-to-all-start.5 = ((bf16[4,24,384]{2,1,0:T(8,128)(2,1)}), bf16[4,24,384]{2,1,0:T(8,128)(2,1)S(1)}, u32[]{:S(2)}, u32[]{:S(2)}) async-start(bf16[4,24,384]{2,1,0:T(8,128)(2,1)} %shard_map.149), calls=%async_computation.5 | async-start | bytes 147456 | tf_op jit(solution)/shard_map/all_to_all | solution.py:567
  38.6 0.0 copy-start.12
  38.6 0.0 copy-start.13
  38.6 0.0 copy-start.15
  38.6 2.8 %shard_map.150.table_ref = bf16[6,256,256]{2,1,0:T(8,128)(2,1)S(1)} custom-call(s32[32]{0:T(128)S(1)} %copy-done.14, f32[2,32,4,64,64]{4,3,2,1,0:T(8,128)} %state_ref.7), custom_call_target="tpu_custom_call" | custom-call | flops 2147483648 | bytes 8388608 | tf_op jit(solution)/shard_map/pallas_call | solution.py:172
  41.4 6.9 %collective-permute-start.13 = (bf16[32,4224]{1,0:T(8,128)(2,1)S(1)}, bf16[32,4224]{1,0:T(8,128)(2,1)S(1)}, u32[]{:S(2)}, u32[]{:S(2)}) collective-permute-start(bf16[32,4224]{1,0:T(8,128)(2,1)S(1)} %collective-permute-done.12.refs_6_), channel_id=1, source_target_pairs={{0,1},{1,0},{2,3},{3,2},{4,5},{5,4},{6,7},{7,6},{8,9},{9,8},{10,11... | collective-permute-start | bytes 811016 | tf_op jit(solution)/shard_map/ppermute | solution.py:550
  48.3 0.0 collective-permute-done.10.refs_4_
  48.3 0.1 collective-permute-start.11
  48.4 0.0 collective-permute-done.8.refs_2_
  48.4 0.4 collective-permute-start.9
  48.8 0.0 all-to-all-done.5.arrived_ref
  48.8 1.9 %shard_map.151 = (bf16[16,24,256]{2,1,0:T(8,128)(2,1)}, f32[24,256]{1,0:T(8,128)S(1)}) custom-call(bf16[4,24,384]{2,1,0:T(8,128)(2,1)S(1)} %all-to-all-done.5.arrived_ref, s32[1,32]{1,0:T(1,128)S(1)} %bitcast.195, f32[2,256]{1,0:T(2,128)S(1)} %copy-done.12, f32[2,256]{1,0:T(2,128)S(1)} %copy-done.13, f32[2,256]{1,0:T(2,128)S(1)} %copy-done.15, ...), custom_call_target="tpu_custom_call" | custom-call | flops 2147483648 | bytes 8388608 | tf_op jit(solution)/shard_map/pallas_call | solution.py:264
  50.7 3.5 %all-to-all-start.6 = ((bf16[16,24,256]{2,1,0:T(8,128)(2,1)}), bf16[16,24,256]{2,1,0:T(8,128)(2,1)S(1)}, u32[]{:S(2)}, u32[]{:S(2)}) async-start(bf16[16,24,256]{2,1,0:T(8,128)(2,1)} %get-tuple-element.440), calls=%async_computation.6 | async-start | bytes 393216 | tf_op jit(solution)/shard_map/all_to_all | solution.py:571
  54.3 0.1 stack.35.starts_ref
  54.4 0.0 copy-start.11
  54.5 7.0 %all-to-all-done.6.acts_ref = bf16[16,24,256]{2,1,0:T(8,128)(2,1)S(1)} async-done(((bf16[16,24,256]{2,1,0:T(8,128)(2,1)}), bf16[16,24,256]{2,1,0:T(8,128)(2,1)S(1)}, u32[]{:S(2)}, u32[]{:S(2)}) %all-to-all-start.6) | async-done | bytes 196640 | tf_op jit(solution)/shard_map/all_to_all | solution.py:571
  61.4 2.7 %finish_0.1 = (bf16[64,24,256]{2,1,0:T(8,128)(2,1)}, f32[1,128]{1,0:T(1,128)S(1)}) custom-call(s32[8]{0:T(128)S(1)} %stack.35.starts_ref, bf16[16,24,256]{2,1,0:T(8,128)(2,1)S(1)} %all-to-all-done.6.acts_ref, bf16[32,4224]{1,0:T(8,128)(2,1)S(1)} %pad_maximum_fusion.refs_0_, bf16[32,4224]{1,0:T(8,128)(2,1)S(1)} %collective-permute-done.7.refs_1_, ...), custom_call_target="tpu_custom_call" | custom-call | flops 2147483648 | bytes 8388608 | tf_op jit(solution)/shard_map/finish_0/pallas_call | solution.py:421
  64.2 0.7 conditional.1
  64.2 0.7 broadcast.169
  64.9 7.2 %all-to-all-start.7 = ((bf16[64,24,256]{2,1,0:T(8,128)(2,1)}), bf16[64,24,256]{2,1,0:T(8,128)(2,1)S(1)}, u32[]{:S(2)}, u32[]{:S(2)}) async-start(bf16[64,24,256]{2,1,0:T(8,128)(2,1)} %get-tuple-element.442), calls=%async_computation.7 | async-start | bytes 1572864 | tf_op jit(solution)/shard_map/all_to_all | solution.py:580
  72.1 2.3 %collective-permute-start.19 = (bf16[32,4096]{1,0:T(8,128)(2,1)S(1)}, bf16[32,4096]{1,0:T(8,128)(2,1)S(1)}, u32[]{:S(2)}, u32[]{:S(2)}) collective-permute-start(bf16[32,4096]{1,0:T(8,128)(2,1)S(1)} %get-tuple-element.565.refs_0_), channel_id=1, source_target_pairs={{0,6},{2,0},{4,2},{6,4},{1,7},{3,1},{5,3},{7,5},{8,14},{10,8},{12,... | collective-permute-start | bytes 786440 | tf_op jit(solution)/shard_map/ppermute | solution.py:546
  74.4 0.6 collective-permute-start.17
  74.9 0.6 collective-permute-start.15
  75.5 2.6 %collective-permute-start.14 = (bf16[32,4096]{1,0:T(8,128)(2,1)S(1)}, bf16[32,4096]{1,0:T(8,128)(2,1)S(1)}, u32[]{:S(2)}, u32[]{:S(2)}) collective-permute-start(bf16[32,4096]{1,0:T(8,128)(2,1)S(1)} %get-tuple-element.565.refs_0_), channel_id=1, source_target_pairs={{0,1},{1,0},{2,3},{3,2},{4,5},{5,4},{6,7},{7,6},{8,9},{9,8},{10,11... | collective-permute-start | bytes 786440 | tf_op jit(solution)/shard_map/ppermute | solution.py:550
  78.1 2.8 %shard_map.153.table_ref = bf16[6,256,256]{2,1,0:T(8,128)(2,1)S(1)} custom-call(s32[32]{0:T(128)S(1)} %copy-done.14, f32[2,32,4,64,64]{4,3,2,1,0:T(8,128)} %state_ref.7), custom_call_target="tpu_custom_call" | custom-call | flops 2147483648 | bytes 8388608 | tf_op jit(solution)/shard_map/pallas_call | solution.py:172
  80.9 5.3 %collective-permute-done.19.refs_6_ = bf16[32,4096]{1,0:T(8,128)(2,1)S(1)} collective-permute-done((bf16[32,4096]{1,0:T(8,128)(2,1)S(1)}, bf16[32,4096]{1,0:T(8,128)(2,1)S(1)}, u32[]{:S(2)}, u32[]{:S(2)}) %collective-permute-start.19) | collective-permute-done | bytes 262176 | tf_op jit(solution)/shard_map/ppermute | solution.py:546
  86.3 4.3 %collective-permute-start.20 = (bf16[32,4096]{1,0:T(8,128)(2,1)S(1)}, bf16[32,4096]{1,0:T(8,128)(2,1)S(1)}, u32[]{:S(2)}, u32[]{:S(2)}) collective-permute-start(bf16[32,4096]{1,0:T(8,128)(2,1)S(1)} %collective-permute-done.19.refs_6_), channel_id=1, source_target_pairs={{0,1},{1,0},{2,3},{3,2},{4,5},{5,4},{6,7},{7,6},{8,9},{9,8},{10,11... | collective-permute-start | bytes 786440 | tf_op jit(solution)/shard_map/ppermute | solution.py:550
  90.6 1.5 %collective-permute-start.18 = (bf16[32,4096]{1,0:T(8,128)(2,1)S(1)}, bf16[32,4096]{1,0:T(8,128)(2,1)S(1)}, u32[]{:S(2)}, u32[]{:S(2)}) collective-permute-start(bf16[32,4096]{1,0:T(8,128)(2,1)S(1)} %collective-permute-done.17.refs_4_), channel_id=1, source_target_pairs={{0,1},{1,0},{2,3},{3,2},{4,5},{5,4},{6,7},{7,6},{8,9},{9,8},{10,11... | collective-permute-start | bytes 786440 | tf_op jit(solution)/shard_map/ppermute | solution.py:550
  92.1 1.8 %collective-permute-done.15.refs_2_ = bf16[32,4096]{1,0:T(8,128)(2,1)S(1)} collective-permute-done((bf16[32,4096]{1,0:T(8,128)(2,1)S(1)}, bf16[32,4096]{1,0:T(8,128)(2,1)S(1)}, u32[]{:S(2)}, u32[]{:S(2)}) %collective-permute-start.15) | collective-permute-done | bytes 262176 | tf_op jit(solution)/shard_map/ppermute | solution.py:546
  93.9 1.6 %collective-permute-start.16 = (bf16[32,4096]{1,0:T(8,128)(2,1)S(1)}, bf16[32,4096]{1,0:T(8,128)(2,1)}, u32[]{:S(2)}, u32[]{:S(2)}) collective-permute-start(bf16[32,4096]{1,0:T(8,128)(2,1)S(1)} %collective-permute-done.15.refs_2_), channel_id=1, source_target_pairs={{0,1},{1,0},{2,3},{3,2},{4,5},{5,4},{6,7},{7,6},{8,9},{9,8},{10,11... | collective-permute-start | bytes 786440 | tf_op jit(solution)/shard_map/ppermute | solution.py:550
  95.4 3.6 %shard_map.152 = bf16[4,24,384]{2,1,0:T(8,128)(2,1)} custom-call(s32[1]{0:T(128)} %bitcast.14.core_ref, bf16[16,96,256]{2,1,0:T(8,128)(2,1)S(1)} %bitcast.158, f32[2,4096]{1,0:T(2,128)S(1)} %copy-done.11, bf16[2,32,4096]{2,1,0:T(8,128)(2,1)} %bitcast.164, bf16[2,32,4096]{2,1,0:T(8,128)(2,1)} %copy-done.8, bf16[2,32,4096]{2,1,0:T(8,128)(2,1)} %bitcast.168, ...), custom_call_target="tpu_custom_call" | custom-call | flops 2147483648 | bytes 8388608 | tf_op jit(solution)/shard_map/pallas_call | solution.py:120
  99.1 3.3 %all-to-all-start.8 = ((bf16[4,24,384]{2,1,0:T(8,128)(2,1)}), bf16[4,24,384]{2,1,0:T(8,128)(2,1)S(1)}, u32[]{:S(2)}, u32[]{:S(2)}) async-start(bf16[4,24,384]{2,1,0:T(8,128)(2,1)} %shard_map.152), calls=%async_computation.8 | async-start | bytes 147456 | tf_op jit(solution)/shard_map/all_to_all | solution.py:567
  102.4 0.0 copy-start.16
  102.4 5.4 %shard_map.155.rest_0_ = f32[2,32,4,64,64]{4,3,2,1,0:T(8,128)} custom-call(s32[32]{0:T(128)S(1)} %copy-done.14, bf16[4,24,384]{2,1,0:T(8,128)(2,1)S(1)} %all-to-all-done.5.arrived_ref, f32[2,256]{1,0:T(2,128)S(1)} %copy-done.12, f32[2,256]{1,0:T(2,128)S(1)} %copy-done.13, f32[24,256]{1,0:T(8,128)S(1)} %get-tuple-element.446.column_ref, ...), custom_call_target="tpu_custom_call" | custom-call | flops 2147483648 | bytes 8388608 | tf_op jit(solution)/shard_map/pallas_call | solution.py:362
  107.9 1.9 %shard_map.154 = (bf16[16,24,256]{2,1,0:T(8,128)(2,1)}, f32[24,256]{1,0:T(8,128)S(1)}) custom-call(bf16[4,24,384]{2,1,0:T(8,128)(2,1)S(1)} %all-to-all-done.8.arrived_ref, s32[1,32]{1,0:T(1,128)S(1)} %bitcast.197, f32[2,256]{1,0:T(2,128)S(1)} %copy-done.12, f32[2,256]{1,0:T(2,128)S(1)} %copy-done.13, f32[2,256]{1,0:T(2,128)S(1)} %copy-done.16, ...), custom_call_target="tpu_custom_call" | custom-call | flops 2147483648 | bytes 8388608 | tf_op jit(solution)/shard_map/pallas_call | solution.py:264
  109.8 6.6 %all-to-all-start.9 = ((bf16[16,24,256]{2,1,0:T(8,128)(2,1)}), bf16[16,24,256]{2,1,0:T(8,128)(2,1)S(1)}, u32[]{:S(2)}, u32[]{:S(2)}) async-start(bf16[16,24,256]{2,1,0:T(8,128)(2,1)} %get-tuple-element.443), calls=%async_computation.9 | async-start | bytes 393216 | tf_op jit(solution)/shard_map/all_to_all | solution.py:571
  116.5 5.4 %shard_map.156 = f32[2,32,4,64,64]{4,3,2,1,0:T(8,128)} custom-call(s32[32]{0:T(128)S(1)} %copy-done.14, bf16[4,24,384]{2,1,0:T(8,128)(2,1)S(1)} %all-to-all-done.8.arrived_ref, f32[2,256]{1,0:T(2,128)S(1)} %copy-done.12, f32[2,256]{1,0:T(2,128)S(1)} %copy-done.13, f32[24,256]{1,0:T(8,128)S(1)} %get-tuple-element.445.column_ref, ...), custom_call_target="tpu_custom_call", output_to_operand_aliasing={{}: (7, {})} | custom-call | flops 2147483648 | bytes 8388608 | tf_op jit(solution)/shard_map/pallas_call | solution.py:362
  121.9 1.7 %all-to-all-done.9.acts_ref = bf16[16,24,256]{2,1,0:T(8,128)(2,1)S(1)} async-done(((bf16[16,24,256]{2,1,0:T(8,128)(2,1)}), bf16[16,24,256]{2,1,0:T(8,128)(2,1)S(1)}, u32[]{:S(2)}, u32[]{:S(2)}) %all-to-all-start.9) | async-done | bytes 196640 | tf_op jit(solution)/shard_map/all_to_all | solution.py:571
  123.7 2.5 %finish_1.1 = bf16[32,256]{1,0:T(8,128)(2,1)} custom-call(s32[8]{0:T(128)S(1)} %stack.35.starts_ref, bf16[16,24,256]{2,1,0:T(8,128)(2,1)S(1)} %all-to-all-done.9.acts_ref, s32[1,32]{1,0:T(1,128)S(1)} %bitcast.198, f32[2,8,2048]{2,1,0:T(8,128)} %get-tuple-element.850.others_ref, bf16[32,4096]{1,0:T(8,128)(2,1)S(1)} %get-tuple-element.565.refs_0_, ...), custom_call_target="tpu_custom_call" | custom-call | flops 2147483648 | bytes 8388608 | tf_op jit(solution)/shard_map/finish_1/pallas_call | solution.py:438
  (28 shorter events, 0.1 us)
Async XLA Ops:
  0.6 31.1 %copy-start = (bf16[2,4096,32]{1,2,0:T(8,128)(2,1)S(1)}, bf16[2,4096,32]{1,2,0:T(8,128)(2,1)}, u32[]{:S(2)}) copy-start(bf16[2,4096,32]{1,2,0:T(8,128)(2,1)} %param.21) | copy-start | bytes 1572868
  0.6 31.1 %copy-start.2 = (bf16[2,4096,32]{1,2,0:T(8,128)(2,1)S(1)}, bf16[2,4096,32]{1,2,0:T(8,128)(2,1)}, u32[]{:S(2)}) copy-start(bf16[2,4096,32]{1,2,0:T(8,128)(2,1)} %param.22) | copy-start | bytes 1572868
  0.7 31.1 %copy-start.10 = (f32[2,4096]{1,0:T(2,128)S(1)}, f32[2,4096]{1,0:T(2,128)}, u32[]{:S(2)}) copy-start(f32[2,4096]{1,0:T(2,128)} %gain_ref.6) | copy-start | bytes 98308
  0.7 16.7 %collective-permute-start.1 = (bf16[2,32,4096]{2,1,0:T(8,128)(2,1)}, bf16[2,32,4096]{2,1,0:T(8,128)(2,1)S(1)}, u32[]{:S(2)}, u32[]{:S(2)}) collective-permute-start(bf16[2,32,4096]{2,1,0:T(8,128)(2,1)} %bitcast.163), channel_id=1, source_target_pairs={{0,1},{1,0},{2,3},{3,2},{4,5},{5,4},{6,7},{7,6},{8,9},{9,8},{10,11... | collective-permute-start | bytes 1572872 | tf_op jit(solution)/shard_map/ppermute | solution.py:557
  2.1 16.1 %collective-permute-start.2 = (bf16[2,32,4096]{2,1,0:T(8,128)(2,1)}, bf16[2,32,4096]{2,1,0:T(8,128)(2,1)}, u32[]{:S(2)}, u32[]{:S(2)}) collective-permute-start(bf16[2,32,4096]{2,1,0:T(8,128)(2,1)} %bitcast.167), channel_id=1, source_target_pairs={{0,1},{1,0},{2,3},{3,2},{4,5},{5,4},{6,7},{7,6},{8,9},{9,8},{10,11... | collective-permute-start | bytes 1572872 | tf_op jit(solution)/shard_map/ppermute | solution.py:557
  2.2 18.3 %collective-permute-start.3 = (bf16[2,32,4096]{2,1,0:T(8,128)(2,1)}, bf16[2,32,4096]{2,1,0:T(8,128)(2,1)}, u32[]{:S(2)}, u32[]{:S(2)}) collective-permute-start(bf16[2,32,4096]{2,1,0:T(8,128)(2,1)} %bitcast.171), channel_id=1, source_target_pairs={{0,1},{1,0},{2,3},{3,2},{4,5},{5,4},{6,7},{7,6},{8,9},{9,8},{10,11... | collective-permute-start | bytes 1572872 | tf_op jit(solution)/shard_map/ppermute | solution.py:557
  2.6 18.5 %collective-permute-start.4 = (bf16[2,32,4096]{2,1,0:T(8,128)(2,1)}, bf16[2,32,4096]{2,1,0:T(8,128)(2,1)}, u32[]{:S(2)}, u32[]{:S(2)}) collective-permute-start(bf16[2,32,4096]{2,1,0:T(8,128)(2,1)} %bitcast.175), channel_id=1, source_target_pairs={{0,1},{1,0},{2,3},{3,2},{4,5},{5,4},{6,7},{7,6},{8,9},{9,8},{10,11... | collective-permute-start | bytes 1572872 | tf_op jit(solution)/shard_map/ppermute | solution.py:557
  2.7 19.0 %collective-permute-start.5 = (bf16[2,32,4096]{2,1,0:T(8,128)(2,1)}, bf16[2,32,4096]{2,1,0:T(8,128)(2,1)}, u32[]{:S(2)}, u32[]{:S(2)}) collective-permute-start(bf16[2,32,4096]{2,1,0:T(8,128)(2,1)} %bitcast.179), channel_id=1, source_target_pairs={{0,1},{1,0},{2,3},{3,2},{4,5},{5,4},{6,7},{7,6},{8,9},{9,8},{10,11... | collective-permute-start | bytes 1572872 | tf_op jit(solution)/shard_map/ppermute | solution.py:557
  5.0 26.7 %all-to-all-start.4 = ((bf16[64,24,256]{2,1,0:T(8,128)(2,1)}), bf16[64,24,256]{2,1,0:T(8,128)(2,1)S(1)}, u32[]{:S(2)}, u32[]{:S(2)}) async-start(bf16[64,24,256]{2,1,0:T(8,128)(2,1)} %get-tuple-element.439), calls=%async_computation.4 | async-start | bytes 1572864 | tf_op jit(solution)/shard_map/all_to_all | solution.py:553
  17.4 0.8 copy-start.8
  17.4 5.8 %collective-permute-start.6 = (bf16[2,32,4096]{2,1,0:T(8,128)(2,1)}, bf16[2,32,4096]{2,1,0:T(8,128)(2,1)}, u32[]{:S(2)}, u32[]{:S(2)}) collective-permute-start(bf16[2,32,4096]{2,1,0:T(8,128)(2,1)} %bitcast.183), channel_id=1, source_target_pairs={{0,1},{1,0},{2,3},{3,2},{4,5},{5,4},{6,7},{7,6},{8,9},{9,8},{10,11... | collective-permute-start | bytes 1572872 | tf_op jit(solution)/shard_map/ppermute | solution.py:557
  18.2 23.2 %collective-permute-start.12 = (bf16[32,4224]{1,0:T(8,128)(2,1)S(1)}, bf16[32,4224]{1,0:T(8,128)(2,1)S(1)}, u32[]{:S(2)}, u32[]{:S(2)}) collective-permute-start(bf16[32,4224]{1,0:T(8,128)(2,1)S(1)} %pad_maximum_fusion.refs_0_), channel_id=1, source_target_pairs={{0,6},{2,0},{4,2},{6,4},{1,7},{3,1},{5,3},{7,5},{8,14},{10,8},{12,... | collective-permute-start | bytes 811016 | tf_op jit(solution)/shard_map/ppermute | solution.py:546
  20.5 27.8 %collective-permute-start.10 = (bf16[32,4224]{1,0:T(8,128)(2,1)S(1)}, bf16[32,4224]{1,0:T(8,128)(2,1)S(1)}, u32[]{:S(2)}, u32[]{:S(2)}) collective-permute-start(bf16[32,4224]{1,0:T(8,128)(2,1)S(1)} %pad_maximum_fusion.refs_0_), channel_id=1, source_target_pairs={{0,4},{2,6},{4,0},{6,2},{1,5},{3,7},{5,1},{7,3},{8,12},{10,14},{12... | collective-permute-start | bytes 811016 | tf_op jit(solution)/shard_map/ppermute | solution.py:546
  21.1 27.3 %collective-permute-start.8 = (bf16[32,4224]{1,0:T(8,128)(2,1)S(1)}, bf16[32,4224]{1,0:T(8,128)(2,1)S(1)}, u32[]{:S(2)}, u32[]{:S(2)}) collective-permute-start(bf16[32,4224]{1,0:T(8,128)(2,1)S(1)} %pad_maximum_fusion.refs_0_), channel_id=1, source_target_pairs={{0,2},{2,4},{4,6},{6,0},{1,3},{3,5},{5,7},{7,1},{8,10},{10,12},{12... | collective-permute-start | bytes 811016 | tf_op jit(solution)/shard_map/ppermute | solution.py:546
  21.7 32.7 %collective-permute-start.7 = (bf16[32,4224]{1,0:T(8,128)(2,1)S(1)}, bf16[32,4224]{1,0:T(8,128)(2,1)S(1)}, u32[]{:S(2)}, u32[]{:S(2)}) collective-permute-start(bf16[32,4224]{1,0:T(8,128)(2,1)S(1)} %pad_maximum_fusion.refs_0_), channel_id=1, source_target_pairs={{0,1},{1,0},{2,3},{3,2},{4,5},{5,4},{6,7},{7,6},{8,9},{9,8},{10,11... | collective-permute-start | bytes 811016 | tf_op jit(solution)/shard_map/ppermute | solution.py:550
  31.8 6.8 %copy-start.14 = (s32[32]{0:T(128)S(1)}, s32[32]{0:T(128)}, u32[]{:S(2)}) copy-start(s32[32]{0:T(128)} %lengths_ref.7) | copy-start | bytes 388
  35.3 13.5 %all-to-all-start.5 = ((bf16[4,24,384]{2,1,0:T(8,128)(2,1)}), bf16[4,24,384]{2,1,0:T(8,128)(2,1)S(1)}, u32[]{:S(2)}, u32[]{:S(2)}) async-start(bf16[4,24,384]{2,1,0:T(8,128)(2,1)} %shard_map.149), calls=%async_computation.5 | async-start | bytes 147456 | tf_op jit(solution)/shard_map/all_to_all | solution.py:567
  38.6 10.2 %copy-start.12 = (f32[2,256]{1,0:T(2,128)S(1)}, f32[2,256]{1,0:T(2,128)}, u32[]{:S(2)}) copy-start(f32[2,256]{1,0:T(2,128)} %decay_ref.7) | copy-start | bytes 6148
  38.6 10.2 %copy-start.13 = (f32[2,256]{1,0:T(2,128)S(1)}, f32[2,256]{1,0:T(2,128)}, u32[]{:S(2)}) copy-start(f32[2,256]{1,0:T(2,128)} %rate_ref.7) | copy-start | bytes 6148
  38.6 10.2 %copy-start.15 = (f32[2,256]{1,0:T(2,128)S(1)}, f32[2,256]{1,0:T(2,128)}, u32[]{:S(2)}) copy-start(f32[2,256]{1,0:T(2,128)} %gain_ref.7) | copy-start | bytes 6148
  41.4 13.0 %collective-permute-start.13 = (bf16[32,4224]{1,0:T(8,128)(2,1)S(1)}, bf16[32,4224]{1,0:T(8,128)(2,1)S(1)}, u32[]{:S(2)}, u32[]{:S(2)}) collective-permute-start(bf16[32,4224]{1,0:T(8,128)(2,1)S(1)} %collective-permute-done.12.refs_6_), channel_id=1, source_target_pairs={{0,1},{1,0},{2,3},{3,2},{4,5},{5,4},{6,7},{7,6},{8,9},{9,8},{10,11... | collective-permute-start | bytes 811016 | tf_op jit(solution)/shard_map/ppermute | solution.py:550
  48.3 6.2 %collective-permute-start.11 = (bf16[32,4224]{1,0:T(8,128)(2,1)S(1)}, bf16[32,4224]{1,0:T(8,128)(2,1)S(1)}, u32[]{:S(2)}, u32[]{:S(2)}) collective-permute-start(bf16[32,4224]{1,0:T(8,128)(2,1)S(1)} %collective-permute-done.10.refs_4_), channel_id=1, source_target_pairs={{0,1},{1,0},{2,3},{3,2},{4,5},{5,4},{6,7},{7,6},{8,9},{9,8},{10,11... | collective-permute-start | bytes 811016 | tf_op jit(solution)/shard_map/ppermute | solution.py:550
  48.4 6.1 %collective-permute-start.9 = (bf16[32,4224]{1,0:T(8,128)(2,1)S(1)}, bf16[32,4224]{1,0:T(8,128)(2,1)}, u32[]{:S(2)}, u32[]{:S(2)}) collective-permute-start(bf16[32,4224]{1,0:T(8,128)(2,1)S(1)} %collective-permute-done.8.refs_2_), channel_id=1, source_target_pairs={{0,1},{1,0},{2,3},{3,2},{4,5},{5,4},{6,7},{7,6},{8,9},{9,8},{10,11... | collective-permute-start | bytes 811016 | tf_op jit(solution)/shard_map/ppermute | solution.py:550
  50.7 10.7 %all-to-all-start.6 = ((bf16[16,24,256]{2,1,0:T(8,128)(2,1)}), bf16[16,24,256]{2,1,0:T(8,128)(2,1)S(1)}, u32[]{:S(2)}, u32[]{:S(2)}) async-start(bf16[16,24,256]{2,1,0:T(8,128)(2,1)} %get-tuple-element.440), calls=%async_computation.6 | async-start | bytes 393216 | tf_op jit(solution)/shard_map/all_to_all | solution.py:571
  54.4 9.7 %copy-start.1 = (bf16[2,4096,32]{1,2,0:T(8,128)(2,1)S(1)}, bf16[2,4096,32]{1,2,0:T(8,128)(2,1)}, u32[]{:S(2)}) copy-start(bf16[2,4096,32]{1,2,0:T(8,128)(2,1)} %param.21) | copy-start | bytes 1572868
  54.4 9.7 %copy-start.3 = (bf16[2,4096,32]{1,2,0:T(8,128)(2,1)S(1)}, bf16[2,4096,32]{1,2,0:T(8,128)(2,1)}, u32[]{:S(2)}) copy-start(bf16[2,4096,32]{1,2,0:T(8,128)(2,1)} %param.22) | copy-start | bytes 1572868
  54.4 9.7 %copy-start.11 = (f32[2,4096]{1,0:T(2,128)S(1)}, f32[2,4096]{1,0:T(2,128)}, u32[]{:S(2)}) copy-start(f32[2,4096]{1,0:T(2,128)} %gain_ref.6) | copy-start | bytes 98308
  64.9 30.6 %all-to-all-start.7 = ((bf16[64,24,256]{2,1,0:T(8,128)(2,1)}), bf16[64,24,256]{2,1,0:T(8,128)(2,1)S(1)}, u32[]{:S(2)}, u32[]{:S(2)}) async-start(bf16[64,24,256]{2,1,0:T(8,128)(2,1)} %get-tuple-element.442), calls=%async_computation.7 | async-start | bytes 1572864 | tf_op jit(solution)/shard_map/all_to_all | solution.py:580
  72.1 14.2 %collective-permute-start.19 = (bf16[32,4096]{1,0:T(8,128)(2,1)S(1)}, bf16[32,4096]{1,0:T(8,128)(2,1)S(1)}, u32[]{:S(2)}, u32[]{:S(2)}) collective-permute-start(bf16[32,4096]{1,0:T(8,128)(2,1)S(1)} %get-tuple-element.565.refs_0_), channel_id=1, source_target_pairs={{0,6},{2,0},{4,2},{6,4},{1,7},{3,1},{5,3},{7,5},{8,14},{10,8},{12,... | collective-permute-start | bytes 786440 | tf_op jit(solution)/shard_map/ppermute | solution.py:546
  74.4 16.2 %collective-permute-start.17 = (bf16[32,4096]{1,0:T(8,128)(2,1)S(1)}, bf16[32,4096]{1,0:T(8,128)(2,1)S(1)}, u32[]{:S(2)}, u32[]{:S(2)}) collective-permute-start(bf16[32,4096]{1,0:T(8,128)(2,1)S(1)} %get-tuple-element.565.refs_0_), channel_id=1, source_target_pairs={{0,4},{2,6},{4,0},{6,2},{1,5},{3,7},{5,1},{7,3},{8,12},{10,14},{12... | collective-permute-start | bytes 786440 | tf_op jit(solution)/shard_map/ppermute | solution.py:546
  74.9 18.9 %collective-permute-start.15 = (bf16[32,4096]{1,0:T(8,128)(2,1)S(1)}, bf16[32,4096]{1,0:T(8,128)(2,1)S(1)}, u32[]{:S(2)}, u32[]{:S(2)}) collective-permute-start(bf16[32,4096]{1,0:T(8,128)(2,1)S(1)} %get-tuple-element.565.refs_0_), channel_id=1, source_target_pairs={{0,2},{2,4},{4,6},{6,0},{1,3},{3,5},{5,7},{7,1},{8,10},{10,12},{12... | collective-permute-start | bytes 786440 | tf_op jit(solution)/shard_map/ppermute | solution.py:546
  75.5 46.4 %collective-permute-start.14 = (bf16[32,4096]{1,0:T(8,128)(2,1)S(1)}, bf16[32,4096]{1,0:T(8,128)(2,1)S(1)}, u32[]{:S(2)}, u32[]{:S(2)}) collective-permute-start(bf16[32,4096]{1,0:T(8,128)(2,1)S(1)} %get-tuple-element.565.refs_0_), channel_id=1, source_target_pairs={{0,1},{1,0},{2,3},{3,2},{4,5},{5,4},{6,7},{7,6},{8,9},{9,8},{10,11... | collective-permute-start | bytes 786440 | tf_op jit(solution)/shard_map/ppermute | solution.py:550
  86.3 35.7 %collective-permute-start.20 = (bf16[32,4096]{1,0:T(8,128)(2,1)S(1)}, bf16[32,4096]{1,0:T(8,128)(2,1)S(1)}, u32[]{:S(2)}, u32[]{:S(2)}) collective-permute-start(bf16[32,4096]{1,0:T(8,128)(2,1)S(1)} %collective-permute-done.19.refs_6_), channel_id=1, source_target_pairs={{0,1},{1,0},{2,3},{3,2},{4,5},{5,4},{6,7},{7,6},{8,9},{9,8},{10,11... | collective-permute-start | bytes 786440 | tf_op jit(solution)/shard_map/ppermute | solution.py:550
  90.6 31.4 %collective-permute-start.18 = (bf16[32,4096]{1,0:T(8,128)(2,1)S(1)}, bf16[32,4096]{1,0:T(8,128)(2,1)S(1)}, u32[]{:S(2)}, u32[]{:S(2)}) collective-permute-start(bf16[32,4096]{1,0:T(8,128)(2,1)S(1)} %collective-permute-done.17.refs_4_), channel_id=1, source_target_pairs={{0,1},{1,0},{2,3},{3,2},{4,5},{5,4},{6,7},{7,6},{8,9},{9,8},{10,11... | collective-permute-start | bytes 786440 | tf_op jit(solution)/shard_map/ppermute | solution.py:550
  93.9 28.1 %collective-permute-start.16 = (bf16[32,4096]{1,0:T(8,128)(2,1)S(1)}, bf16[32,4096]{1,0:T(8,128)(2,1)}, u32[]{:S(2)}, u32[]{:S(2)}) collective-permute-start(bf16[32,4096]{1,0:T(8,128)(2,1)S(1)} %collective-permute-done.15.refs_2_), channel_id=1, source_target_pairs={{0,1},{1,0},{2,3},{3,2},{4,5},{5,4},{6,7},{7,6},{8,9},{9,8},{10,11... | collective-permute-start | bytes 786440 | tf_op jit(solution)/shard_map/ppermute | solution.py:550
  99.1 8.8 %all-to-all-start.8 = ((bf16[4,24,384]{2,1,0:T(8,128)(2,1)}), bf16[4,24,384]{2,1,0:T(8,128)(2,1)S(1)}, u32[]{:S(2)}, u32[]{:S(2)}) async-start(bf16[4,24,384]{2,1,0:T(8,128)(2,1)} %shard_map.152), calls=%async_computation.8 | async-start | bytes 147456 | tf_op jit(solution)/shard_map/all_to_all | solution.py:567
  102.4 5.5 %copy-start.16 = (f32[2,256]{1,0:T(2,128)S(1)}, f32[2,256]{1,0:T(2,128)}, u32[]{:S(2)}) copy-start(f32[2,256]{1,0:T(2,128)} %gain_ref.7) | copy-start | bytes 6148
  109.8 13.8 %all-to-all-start.9 = ((bf16[16,24,256]{2,1,0:T(8,128)(2,1)}), bf16[16,24,256]{2,1,0:T(8,128)(2,1)S(1)}, u32[]{:S(2)}, u32[]{:S(2)}) async-start(bf16[16,24,256]{2,1,0:T(8,128)(2,1)} %get-tuple-element.443), calls=%async_computation.9 | async-start | bytes 393216 | tf_op jit(solution)/shard_map/all_to_all | solution.py:571

commit v5 on v4

--- a/solution.py
+++ b/solution.py
@@ -369,8 +369,8 @@
             pltpu.VMEM((count, 2 * heads, head), jnp.float32),
             pltpu.VMEM((count, heads * head), jnp.float32),
             pltpu.VMEM((count, heads, head, head), jnp.float32),
-            pltpu.SemaphoreType.DMA((8,)),
-            pltpu.SemaphoreType.DMA((8,)),
+            pltpu.SemaphoreType.DMA((16,)),
+            pltpu.SemaphoreType.DMA((16,)),
         ],
         input_output_aliases={7: 0} if more else {},
         cost_estimate=COST,
@@ -540,11 +540,10 @@
 
     def along_x(layer, more):
         own = jnp.concatenate([w_out.swapaxes(1, 2)[layer]] + more, axis=1)
-        pieces = [own]
-        for k in range(1, n_x):
-            shift = [(i, (i + k) % n_x) for i in range(n_x)]
-            pieces.append(lax.ppermute(own, "x", shift))
-        return pieces
+        return [own] + [
+            lax.ppermute(own, "x", [(i, (i + k) % n_x) for i in range(n_x)])
+            for k in range(1, n_x)
+        ]
 
     def over_pair(pieces):
         return [p for piece in pieces for p in (piece, lax.ppermute(piece, "c", PAIR))]

time: 128 us -> 128 us (level)
  no operation moved by 1% of the time
where the time goes in v5:
time: 128 us; the launch traced here: 126 us
  starting transfers between devices  63.9 us (50%)
  Pallas kernels  34.6 us (27%)
  waiting for transfers between devices  24.4 us (19%)
  local copies, waits for them, and re-layouts  2.24 us (2%)
    ppermute x8, starting transfers between devices, over_pair(): lax.ppermute(piece, 'c', PAIR)  18.9 us
    all_to_all x1, starting transfers between devices, local(): acts = lax.all_to_all(chosen, CHIPS, 0, 0)  11.2 us
    pallas_call x2, Pallas kernels, update(): pl.pallas_call(functools.partial(update_kernel, layer), out_shape=pltpu.H...  11 us
    all_to_all x2, starting transfers between devices, local(): mixed_all = lax.all_to_all(mixed, TP, 0, 0)  10.2 us
    all_to_all x2, waiting for transfers between devices, local(): mixed_all = lax.all_to_all(mixed, TP, 0, 0)  8.62 us
    all_to_all x1, waiting for transfers between devices, local(): acts = lax.all_to_all(chosen, CHIPS, 0, 0)  8.56 us
    all_to_all x1, starting transfers between devices, local(): acts = lax.all_to_all(current, CHIPS, 0, 0)  7.22 us
    ppermute x6, waiting for transfers between devices, along_x(): lax.ppermute(own, 'x', [(i, (i + k) % n_x) for i in range(n_x)])  7.16 us
  transfers between devices with their start and end apart: 26, of which 5 were waited for; matrix products, arithmetic and copies ran while one was open for 1% of the time, Pallas kernels for 23%

profile of v5, /device:TPU:1, one launch (start us, length us, event | category | flops | bytes accessed | tf_op | source)
XLA Modules:
  0.0 126.3 jit_solution(8653544264716938420)
XLA Ops:
  0.6 0.0 copy-start
  0.6 0.0 copy-start.2
  0.7 0.0 copy-start.10
  0.7 1.5 %collective-permute-start.1 = (bf16[2,32,4096]{2,1,0:T(8,128)(2,1)}, bf16[2,32,4096]{2,1,0:T(8,128)(2,1)S(1)}, u32[]{:S(2)}, u32[]{:S(2)}) collective-permute-start(bf16[2,32,4096]{2,1,0:T(8,128)(2,1)} %bitcast.163), channel_id=1, source_target_pairs={{0,1},{1,0},{2,3},{3,2},{4,5},{5,4},{6,7},{7,6},{8,9},{9,8},{10,11... | collective-permute-start | bytes 1572872 | tf_op jit(solution)/shard_map/ppermute | solution.py:556
  2.1 0.1 collective-permute-start.2
  2.2 0.4 collective-permute-start.3
  2.6 0.1 collective-permute-start.4
  2.7 0.4 collective-permute-start.5
  3.1 1.9 %choose.1 = (bf16[64,24,256]{2,1,0:T(8,128)(2,1)}, bf16[32,128]{1,0:T(8,128)(2,1)S(1)}) custom-call(s32[1,32]{1,0:T(1,128)} %bitcast.194, bf16[32,256]{1,0:T(8,128)(2,1)} %tokens_ref.1), custom_call_target="tpu_custom_call" | custom-call | tf_op jit(solution)/shard_map/choose/pallas_call | solution.py:61
  5.0 11.2 %all-to-all-start.4 = ((bf16[64,24,256]{2,1,0:T(8,128)(2,1)}), bf16[64,24,256]{2,1,0:T(8,128)(2,1)S(1)}, u32[]{:S(2)}, u32[]{:S(2)}) async-start(bf16[64,24,256]{2,1,0:T(8,128)(2,1)} %get-tuple-element.439), calls=%async_computation.4 | async-start | bytes 1572864 | tf_op jit(solution)/shard_map/all_to_all | solution.py:552
  16.3 1.1 slice_bitcast_fusion
  17.4 0.0 collective-permute-done.1.rest_1_
  17.4 0.5 collective-permute-start.6
  17.9 0.3 copy-done.8
  18.2 0.0 collective-permute-done.2.rest_3_
  18.2 2.3 %collective-permute-start.12 = (bf16[32,4224]{1,0:T(8,128)(2,1)S(1)}, bf16[32,4224]{1,0:T(8,128)(2,1)S(1)}, u32[]{:S(2)}, u32[]{:S(2)}) collective-permute-start(bf16[32,4224]{1,0:T(8,128)(2,1)S(1)} %pad_maximum_fusion.refs_0_), channel_id=1, source_target_pairs={{0,6},{2,0},{4,2},{6,4},{1,7},{3,1},{5,3},{7,5},{8,14},{10,8},{12,... | collective-permute-start | bytes 811016 | tf_op jit(solution)/shard_map/ppermute | solution.py:544
  20.5 0.0 collective-permute-done.3.rest_5_
  20.5 0.6 collective-permute-start.10
  21.1 0.0 collective-permute-done.4.rest_7_
  21.1 0.6 collective-permute-start.8
  21.7 1.5 %collective-permute-start.7 = (bf16[32,4224]{1,0:T(8,128)(2,1)S(1)}, bf16[32,4224]{1,0:T(8,128)(2,1)S(1)}, u32[]{:S(2)}, u32[]{:S(2)}) collective-permute-start(bf16[32,4224]{1,0:T(8,128)(2,1)S(1)} %pad_maximum_fusion.refs_0_), channel_id=1, source_target_pairs={{0,1},{1,0},{2,3},{3,2},{4,5},{5,4},{6,7},{7,6},{8,9},{9,8},{10,11... | collective-permute-start | bytes 811016 | tf_op jit(solution)/shard_map/ppermute | solution.py:549
  23.2 0.0 collective-permute-done.6.rest_11_
  23.2 8.6 %all-to-all-done.4 = bf16[64,24,256]{2,1,0:T(8,128)(2,1)S(1)} async-done(((bf16[64,24,256]{2,1,0:T(8,128)(2,1)}), bf16[64,24,256]{2,1,0:T(8,128)(2,1)S(1)}, u32[]{:S(2)}, u32[]{:S(2)}) %all-to-all-start.4) | async-done | bytes 786464 | tf_op jit(solution)/shard_map/all_to_all | solution.py:552
  31.8 0.0 copy-start.14
  31.8 3.5 %shard_map.149 = bf16[4,24,384]{2,1,0:T(8,128)(2,1)} custom-call(s32[1]{0:T(128)} %bitcast.14.core_ref, bf16[16,96,256]{2,1,0:T(8,128)(2,1)S(1)} %bitcast.157, f32[2,4096]{1,0:T(2,128)S(1)} %copy-done.10, bf16[2,32,4096]{2,1,0:T(8,128)(2,1)S(1)} %bitcast.165, bf16[2,32,4096]{2,1,0:T(8,128)(2,1)} %copy-done.8, bf16[2,32,4096]{2,1,0:T(8,128)(2,1)S(1)} %bitcast.169, ...), custom_call_target="tpu_custom_call" | custom-call | flops 2147483648 | bytes 8388608 | tf_op jit(solution)/shard_map/pallas_call | solution.py:120
  35.3 3.3 %all-to-all-start.5 = ((bf16[4,24,384]{2,1,0:T(8,128)(2,1)}), bf16[4,24,384]{2,1,0:T(8,128)(2,1)S(1)}, u32[]{:S(2)}, u32[]{:S(2)}) async-start(bf16[4,24,384]{2,1,0:T(8,128)(2,1)} %shard_map.149), calls=%async_computation.5 | async-start | bytes 147456 | tf_op jit(solution)/shard_map/all_to_all | solution.py:566
  38.6 0.0 copy-start.12
  38.6 0.0 copy-start.13
  38.6 0.0 copy-start.15
  38.6 2.8 %shard_map.150.table_ref = bf16[6,256,256]{2,1,0:T(8,128)(2,1)S(1)} custom-call(s32[32]{0:T(128)S(1)} %copy-done.14, f32[2,32,4,64,64]{4,3,2,1,0:T(8,128)} %state_ref.7), custom_call_target="tpu_custom_call" | custom-call | flops 2147483648 | bytes 8388608 | tf_op jit(solution)/shard_map/pallas_call | solution.py:172
  41.4 6.9 %collective-permute-start.13 = (bf16[32,4224]{1,0:T(8,128)(2,1)S(1)}, bf16[32,4224]{1,0:T(8,128)(2,1)S(1)}, u32[]{:S(2)}, u32[]{:S(2)}) collective-permute-start(bf16[32,4224]{1,0:T(8,128)(2,1)S(1)} %collective-permute-done.12.refs_6_), channel_id=1, source_target_pairs={{0,1},{1,0},{2,3},{3,2},{4,5},{5,4},{6,7},{7,6},{8,9},{9,8},{10,11... | collective-permute-start | bytes 811016 | tf_op jit(solution)/shard_map/ppermute | solution.py:549
  48.3 0.0 collective-permute-done.10.refs_4_
  48.3 0.1 collective-permute-start.11
  48.4 0.0 collective-permute-done.8.refs_2_
  48.4 0.4 collective-permute-start.9
  48.8 0.0 all-to-all-done.5.arrived_ref
  48.8 1.9 %shard_map.151 = (bf16[16,24,256]{2,1,0:T(8,128)(2,1)}, f32[24,256]{1,0:T(8,128)S(1)}) custom-call(bf16[4,24,384]{2,1,0:T(8,128)(2,1)S(1)} %all-to-all-done.5.arrived_ref, s32[1,32]{1,0:T(1,128)S(1)} %bitcast.195, f32[2,256]{1,0:T(2,128)S(1)} %copy-done.12, f32[2,256]{1,0:T(2,128)S(1)} %copy-done.13, f32[2,256]{1,0:T(2,128)S(1)} %copy-done.15, ...), custom_call_target="tpu_custom_call" | custom-call | flops 2147483648 | bytes 8388608 | tf_op jit(solution)/shard_map/pallas_call | solution.py:264
  50.7 3.5 %all-to-all-start.6 = ((bf16[16,24,256]{2,1,0:T(8,128)(2,1)}), bf16[16,24,256]{2,1,0:T(8,128)(2,1)S(1)}, u32[]{:S(2)}, u32[]{:S(2)}) async-start(bf16[16,24,256]{2,1,0:T(8,128)(2,1)} %get-tuple-element.440), calls=%async_computation.6 | async-start | bytes 393216 | tf_op jit(solution)/shard_map/all_to_all | solution.py:570
  54.3 0.1 stack.35.starts_ref
  54.4 0.0 copy-start.11
  54.5 7.0 %all-to-all-done.6.acts_ref = bf16[16,24,256]{2,1,0:T(8,128)(2,1)S(1)} async-done(((bf16[16,24,256]{2,1,0:T(8,128)(2,1)}), bf16[16,24,256]{2,1,0:T(8,128)(2,1)S(1)}, u32[]{:S(2)}, u32[]{:S(2)}) %all-to-all-start.6) | async-done | bytes 196640 | tf_op jit(solution)/shard_map/all_to_all | solution.py:570
  61.4 2.7 %finish_0.1 = (bf16[64,24,256]{2,1,0:T(8,128)(2,1)}, f32[1,128]{1,0:T(1,128)S(1)}) custom-call(s32[8]{0:T(128)S(1)} %stack.35.starts_ref, bf16[16,24,256]{2,1,0:T(8,128)(2,1)S(1)} %all-to-all-done.6.acts_ref, bf16[32,4224]{1,0:T(8,128)(2,1)S(1)} %pad_maximum_fusion.refs_0_, bf16[32,4224]{1,0:T(8,128)(2,1)S(1)} %collective-permute-done.7.refs_1_, ...), custom_call_target="tpu_custom_call" | custom-call | flops 2147483648 | bytes 8388608 | tf_op jit(solution)/shard_map/finish_0/pallas_call | solution.py:421
  64.2 0.7 conditional.1
  64.2 0.7 broadcast.169
  64.9 7.2 %all-to-all-start.7 = ((bf16[64,24,256]{2,1,0:T(8,128)(2,1)}), bf16[64,24,256]{2,1,0:T(8,128)(2,1)S(1)}, u32[]{:S(2)}, u32[]{:S(2)}) async-start(bf16[64,24,256]{2,1,0:T(8,128)(2,1)} %get-tuple-element.442), calls=%async_computation.7 | async-start | bytes 1572864 | tf_op jit(solution)/shard_map/all_to_all | solution.py:579
  72.1 2.3 %collective-permute-start.19 = (bf16[32,4096]{1,0:T(8,128)(2,1)S(1)}, bf16[32,4096]{1,0:T(8,128)(2,1)S(1)}, u32[]{:S(2)}, u32[]{:S(2)}) collective-permute-start(bf16[32,4096]{1,0:T(8,128)(2,1)S(1)} %get-tuple-element.565.refs_0_), channel_id=1, source_target_pairs={{0,6},{2,0},{4,2},{6,4},{1,7},{3,1},{5,3},{7,5},{8,14},{10,8},{12,... | collective-permute-start | bytes 786440 | tf_op jit(solution)/shard_map/ppermute | solution.py:544
  74.4 0.6 collective-permute-start.17
  74.9 0.6 collective-permute-start.15
  75.5 2.6 %collective-permute-start.14 = (bf16[32,4096]{1,0:T(8,128)(2,1)S(1)}, bf16[32,4096]{1,0:T(8,128)(2,1)S(1)}, u32[]{:S(2)}, u32[]{:S(2)}) collective-permute-start(bf16[32,4096]{1,0:T(8,128)(2,1)S(1)} %get-tuple-element.565.refs_0_), channel_id=1, source_target_pairs={{0,1},{1,0},{2,3},{3,2},{4,5},{5,4},{6,7},{7,6},{8,9},{9,8},{10,11... | collective-permute-start | bytes 786440 | tf_op jit(solution)/shard_map/ppermute | solution.py:549
  78.1 2.8 %shard_map.153.table_ref = bf16[6,256,256]{2,1,0:T(8,128)(2,1)S(1)} custom-call(s32[32]{0:T(128)S(1)} %copy-done.14, f32[2,32,4,64,64]{4,3,2,1,0:T(8,128)} %state_ref.7), custom_call_target="tpu_custom_call" | custom-call | flops 2147483648 | bytes 8388608 | tf_op jit(solution)/shard_map/pallas_call | solution.py:172
  80.9 5.3 %collective-permute-done.19.refs_6_ = bf16[32,4096]{1,0:T(8,128)(2,1)S(1)} collective-permute-done((bf16[32,4096]{1,0:T(8,128)(2,1)S(1)}, bf16[32,4096]{1,0:T(8,128)(2,1)S(1)}, u32[]{:S(2)}, u32[]{:S(2)}) %collective-permute-start.19) | collective-permute-done | bytes 262176 | tf_op jit(solution)/shard_map/ppermute | solution.py:544
  86.3 4.3 %collective-permute-start.20 = (bf16[32,4096]{1,0:T(8,128)(2,1)S(1)}, bf16[32,4096]{1,0:T(8,128)(2,1)S(1)}, u32[]{:S(2)}, u32[]{:S(2)}) collective-permute-start(bf16[32,4096]{1,0:T(8,128)(2,1)S(1)} %collective-permute-done.19.refs_6_), channel_id=1, source_target_pairs={{0,1},{1,0},{2,3},{3,2},{4,5},{5,4},{6,7},{7,6},{8,9},{9,8},{10,11... | collective-permute-start | bytes 786440 | tf_op jit(solution)/shard_map/ppermute | solution.py:549
  90.6 1.5 %collective-permute-start.18 = (bf16[32,4096]{1,0:T(8,128)(2,1)S(1)}, bf16[32,4096]{1,0:T(8,128)(2,1)S(1)}, u32[]{:S(2)}, u32[]{:S(2)}) collective-permute-start(bf16[32,4096]{1,0:T(8,128)(2,1)S(1)} %collective-permute-done.17.refs_4_), channel_id=1, source_target_pairs={{0,1},{1,0},{2,3},{3,2},{4,5},{5,4},{6,7},{7,6},{8,9},{9,8},{10,11... | collective-permute-start | bytes 786440 | tf_op jit(solution)/shard_map/ppermute | solution.py:549
  92.1 1.8 %collective-permute-done.15.refs_2_ = bf16[32,4096]{1,0:T(8,128)(2,1)S(1)} collective-permute-done((bf16[32,4096]{1,0:T(8,128)(2,1)S(1)}, bf16[32,4096]{1,0:T(8,128)(2,1)S(1)}, u32[]{:S(2)}, u32[]{:S(2)}) %collective-permute-start.15) | collective-permute-done | bytes 262176 | tf_op jit(solution)/shard_map/ppermute | solution.py:544
  93.9 1.6 %collective-permute-start.16 = (bf16[32,4096]{1,0:T(8,128)(2,1)S(1)}, bf16[32,4096]{1,0:T(8,128)(2,1)}, u32[]{:S(2)}, u32[]{:S(2)}) collective-permute-start(bf16[32,4096]{1,0:T(8,128)(2,1)S(1)} %collective-permute-done.15.refs_2_), channel_id=1, source_target_pairs={{0,1},{1,0},{2,3},{3,2},{4,5},{5,4},{6,7},{7,6},{8,9},{9,8},{10,11... | collective-permute-start | bytes 786440 | tf_op jit(solution)/shard_map/ppermute | solution.py:549
  95.4 3.6 %shard_map.152 = bf16[4,24,384]{2,1,0:T(8,128)(2,1)} custom-call(s32[1]{0:T(128)} %bitcast.14.core_ref, bf16[16,96,256]{2,1,0:T(8,128)(2,1)S(1)} %bitcast.158, f32[2,4096]{1,0:T(2,128)S(1)} %copy-done.11, bf16[2,32,4096]{2,1,0:T(8,128)(2,1)} %bitcast.164, bf16[2,32,4096]{2,1,0:T(8,128)(2,1)} %copy-done.8, bf16[2,32,4096]{2,1,0:T(8,128)(2,1)} %bitcast.168, ...), custom_call_target="tpu_custom_call" | custom-call | flops 2147483648 | bytes 8388608 | tf_op jit(solution)/shard_map/pallas_call | solution.py:120
  99.1 3.3 %all-to-all-start.8 = ((bf16[4,24,384]{2,1,0:T(8,128)(2,1)}), bf16[4,24,384]{2,1,0:T(8,128)(2,1)S(1)}, u32[]{:S(2)}, u32[]{:S(2)}) async-start(bf16[4,24,384]{2,1,0:T(8,128)(2,1)} %shard_map.152), calls=%async_computation.8 | async-start | bytes 147456 | tf_op jit(solution)/shard_map/all_to_all | solution.py:566
  102.4 0.0 copy-start.16
  102.4 5.5 %shard_map.155.rest_0_ = f32[2,32,4,64,64]{4,3,2,1,0:T(8,128)} custom-call(s32[32]{0:T(128)S(1)} %copy-done.14, bf16[4,24,384]{2,1,0:T(8,128)(2,1)S(1)} %all-to-all-done.5.arrived_ref, f32[2,256]{1,0:T(2,128)S(1)} %copy-done.12, f32[2,256]{1,0:T(2,128)S(1)} %copy-done.13, f32[24,256]{1,0:T(8,128)S(1)} %get-tuple-element.446.column_ref, ...), custom_call_target="tpu_custom_call" | custom-call | flops 2147483648 | bytes 8388608 | tf_op jit(solution)/shard_map/pallas_call | solution.py:362
  107.9 1.9 %shard_map.154 = (bf16[16,24,256]{2,1,0:T(8,128)(2,1)}, f32[24,256]{1,0:T(8,128)S(1)}) custom-call(bf16[4,24,384]{2,1,0:T(8,128)(2,1)S(1)} %all-to-all-done.8.arrived_ref, s32[1,32]{1,0:T(1,128)S(1)} %bitcast.197, f32[2,256]{1,0:T(2,128)S(1)} %copy-done.12, f32[2,256]{1,0:T(2,128)S(1)} %copy-done.13, f32[2,256]{1,0:T(2,128)S(1)} %copy-done.16, ...), custom_call_target="tpu_custom_call" | custom-call | flops 2147483648 | bytes 8388608 | tf_op jit(solution)/shard_map/pallas_call | solution.py:264
  109.9 6.6 %all-to-all-start.9 = ((bf16[16,24,256]{2,1,0:T(8,128)(2,1)}), bf16[16,24,256]{2,1,0:T(8,128)(2,1)S(1)}, u32[]{:S(2)}, u32[]{:S(2)}) async-start(bf16[16,24,256]{2,1,0:T(8,128)(2,1)} %get-tuple-element.443), calls=%async_computation.9 | async-start | bytes 393216 | tf_op jit(solution)/shard_map/all_to_all | solution.py:570
  116.5 5.5 %shard_map.156 = f32[2,32,4,64,64]{4,3,2,1,0:T(8,128)} custom-call(s32[32]{0:T(128)S(1)} %copy-done.14, bf16[4,24,384]{2,1,0:T(8,128)(2,1)S(1)} %all-to-all-done.8.arrived_ref, f32[2,256]{1,0:T(2,128)S(1)} %copy-done.12, f32[2,256]{1,0:T(2,128)S(1)} %copy-done.13, f32[24,256]{1,0:T(8,128)S(1)} %get-tuple-element.445.column_ref, ...), custom_call_target="tpu_custom_call", output_to_operand_aliasing={{}: (7, {})} | custom-call | flops 2147483648 | bytes 8388608 | tf_op jit(solution)/shard_map/pallas_call | solution.py:362
  122.1 1.7 %all-to-all-done.9.acts_ref = bf16[16,24,256]{2,1,0:T(8,128)(2,1)S(1)} async-done(((bf16[16,24,256]{2,1,0:T(8,128)(2,1)}), bf16[16,24,256]{2,1,0:T(8,128)(2,1)S(1)}, u32[]{:S(2)}, u32[]{:S(2)}) %all-to-all-start.9) | async-done | bytes 196640 | tf_op jit(solution)/shard_map/all_to_all | solution.py:570
  123.7 2.5 %finish_1.1 = bf16[32,256]{1,0:T(8,128)(2,1)} custom-call(s32[8]{0:T(128)S(1)} %stack.35.starts_ref, bf16[16,24,256]{2,1,0:T(8,128)(2,1)S(1)} %all-to-all-done.9.acts_ref, s32[1,32]{1,0:T(1,128)S(1)} %bitcast.198, f32[2,8,2048]{2,1,0:T(8,128)} %get-tuple-element.850.others_ref, bf16[32,4096]{1,0:T(8,128)(2,1)S(1)} %get-tuple-element.565.refs_0_, ...), custom_call_target="tpu_custom_call" | custom-call | flops 2147483648 | bytes 8388608 | tf_op jit(solution)/shard_map/finish_1/pallas_call | solution.py:438
  (28 shorter events, 0.1 us)
Async XLA Ops:
  0.6 31.1 %copy-start = (bf16[2,4096,32]{1,2,0:T(8,128)(2,1)S(1)}, bf16[2,4096,32]{1,2,0:T(8,128)(2,1)}, u32[]{:S(2)}) copy-start(bf16[2,4096,32]{1,2,0:T(8,128)(2,1)} %param.21) | copy-start | bytes 1572868
  0.6 31.1 %copy-start.2 = (bf16[2,4096,32]{1,2,0:T(8,128)(2,1)S(1)}, bf16[2,4096,32]{1,2,0:T(8,128)(2,1)}, u32[]{:S(2)}) copy-start(bf16[2,4096,32]{1,2,0:T(8,128)(2,1)} %param.22) | copy-start | bytes 1572868
  0.7 31.1 %copy-start.10 = (f32[2,4096]{1,0:T(2,128)S(1)}, f32[2,4096]{1,0:T(2,128)}, u32[]{:S(2)}) copy-start(f32[2,4096]{1,0:T(2,128)} %gain_ref.6) | copy-start | bytes 98308
  0.7 16.7 %collective-permute-start.1 = (bf16[2,32,4096]{2,1,0:T(8,128)(2,1)}, bf16[2,32,4096]{2,1,0:T(8,128)(2,1)S(1)}, u32[]{:S(2)}, u32[]{:S(2)}) collective-permute-start(bf16[2,32,4096]{2,1,0:T(8,128)(2,1)} %bitcast.163), channel_id=1, source_target_pairs={{0,1},{1,0},{2,3},{3,2},{4,5},{5,4},{6,7},{7,6},{8,9},{9,8},{10,11... | collective-permute-start | bytes 1572872 | tf_op jit(solution)/shard_map/ppermute | solution.py:556
  2.1 16.1 %collective-permute-start.2 = (bf16[2,32,4096]{2,1,0:T(8,128)(2,1)}, bf16[2,32,4096]{2,1,0:T(8,128)(2,1)}, u32[]{:S(2)}, u32[]{:S(2)}) collective-permute-start(bf16[2,32,4096]{2,1,0:T(8,128)(2,1)} %bitcast.167), channel_id=1, source_target_pairs={{0,1},{1,0},{2,3},{3,2},{4,5},{5,4},{6,7},{7,6},{8,9},{9,8},{10,11... | collective-permute-start | bytes 1572872 | tf_op jit(solution)/shard_map/ppermute | solution.py:556
  2.2 18.3 %collective-permute-start.3 = (bf16[2,32,4096]{2,1,0:T(8,128)(2,1)}, bf16[2,32,4096]{2,1,0:T(8,128)(2,1)}, u32[]{:S(2)}, u32[]{:S(2)}) collective-permute-start(bf16[2,32,4096]{2,1,0:T(8,128)(2,1)} %bitcast.171), channel_id=1, source_target_pairs={{0,1},{1,0},{2,3},{3,2},{4,5},{5,4},{6,7},{7,6},{8,9},{9,8},{10,11... | collective-permute-start | bytes 1572872 | tf_op jit(solution)/shard_map/ppermute | solution.py:556
  2.6 18.5 %collective-permute-start.4 = (bf16[2,32,4096]{2,1,0:T(8,128)(2,1)}, bf16[2,32,4096]{2,1,0:T(8,128)(2,1)}, u32[]{:S(2)}, u32[]{:S(2)}) collective-permute-start(bf16[2,32,4096]{2,1,0:T(8,128)(2,1)} %bitcast.175), channel_id=1, source_target_pairs={{0,1},{1,0},{2,3},{3,2},{4,5},{5,4},{6,7},{7,6},{8,9},{9,8},{10,11... | collective-permute-start | bytes 1572872 | tf_op jit(solution)/shard_map/ppermute | solution.py:556
  2.7 19.0 %collective-permute-start.5 = (bf16[2,32,4096]{2,1,0:T(8,128)(2,1)}, bf16[2,32,4096]{2,1,0:T(8,128)(2,1)}, u32[]{:S(2)}, u32[]{:S(2)}) collective-permute-start(bf16[2,32,4096]{2,1,0:T(8,128)(2,1)} %bitcast.179), channel_id=1, source_target_pairs={{0,1},{1,0},{2,3},{3,2},{4,5},{5,4},{6,7},{7,6},{8,9},{9,8},{10,11... | collective-permute-start | bytes 1572872 | tf_op jit(solution)/shard_map/ppermute | solution.py:556
  5.0 26.7 %all-to-all-start.4 = ((bf16[64,24,256]{2,1,0:T(8,128)(2,1)}), bf16[64,24,256]{2,1,0:T(8,128)(2,1)S(1)}, u32[]{:S(2)}, u32[]{:S(2)}) async-start(bf16[64,24,256]{2,1,0:T(8,128)(2,1)} %get-tuple-element.439), calls=%async_computation.4 | async-start | bytes 1572864 | tf_op jit(solution)/shard_map/all_to_all | solution.py:552
  17.4 0.8 copy-start.8
  17.4 5.8 %collective-permute-start.6 = (bf16[2,32,4096]{2,1,0:T(8,128)(2,1)}, bf16[2,32,4096]{2,1,0:T(8,128)(2,1)}, u32[]{:S(2)}, u32[]{:S(2)}) collective-permute-start(bf16[2,32,4096]{2,1,0:T(8,128)(2,1)} %bitcast.183), channel_id=1, source_target_pairs={{0,1},{1,0},{2,3},{3,2},{4,5},{5,4},{6,7},{7,6},{8,9},{9,8},{10,11... | collective-permute-start | bytes 1572872 | tf_op jit(solution)/shard_map/ppermute | solution.py:556
  18.2 23.2 %collective-permute-start.12 = (bf16[32,4224]{1,0:T(8,128)(2,1)S(1)}, bf16[32,4224]{1,0:T(8,128)(2,1)S(1)}, u32[]{:S(2)}, u32[]{:S(2)}) collective-permute-start(bf16[32,4224]{1,0:T(8,128)(2,1)S(1)} %pad_maximum_fusion.refs_0_), channel_id=1, source_target_pairs={{0,6},{2,0},{4,2},{6,4},{1,7},{3,1},{5,3},{7,5},{8,14},{10,8},{12,... | collective-permute-start | bytes 811016 | tf_op jit(solution)/shard_map/ppermute | solution.py:544
  20.5 27.8 %collective-permute-start.10 = (bf16[32,4224]{1,0:T(8,128)(2,1)S(1)}, bf16[32,4224]{1,0:T(8,128)(2,1)S(1)}, u32[]{:S(2)}, u32[]{:S(2)}) collective-permute-start(bf16[32,4224]{1,0:T(8,128)(2,1)S(1)} %pad_maximum_fusion.refs_0_), channel_id=1, source_target_pairs={{0,4},{2,6},{4,0},{6,2},{1,5},{3,7},{5,1},{7,3},{8,12},{10,14},{12... | collective-permute-start | bytes 811016 | tf_op jit(solution)/shard_map/ppermute | solution.py:544
  21.1 27.3 %collective-permute-start.8 = (bf16[32,4224]{1,0:T(8,128)(2,1)S(1)}, bf16[32,4224]{1,0:T(8,128)(2,1)S(1)}, u32[]{:S(2)}, u32[]{:S(2)}) collective-permute-start(bf16[32,4224]{1,0:T(8,128)(2,1)S(1)} %pad_maximum_fusion.refs_0_), channel_id=1, source_target_pairs={{0,2},{2,4},{4,6},{6,0},{1,3},{3,5},{5,7},{7,1},{8,10},{10,12},{12... | collective-permute-start | bytes 811016 | tf_op jit(solution)/shard_map/ppermute | solution.py:544
  21.7 32.7 %collective-permute-start.7 = (bf16[32,4224]{1,0:T(8,128)(2,1)S(1)}, bf16[32,4224]{1,0:T(8,128)(2,1)S(1)}, u32[]{:S(2)}, u32[]{:S(2)}) collective-permute-start(bf16[32,4224]{1,0:T(8,128)(2,1)S(1)} %pad_maximum_fusion.refs_0_), channel_id=1, source_target_pairs={{0,1},{1,0},{2,3},{3,2},{4,5},{5,4},{6,7},{7,6},{8,9},{9,8},{10,11... | collective-permute-start | bytes 811016 | tf_op jit(solution)/shard_map/ppermute | solution.py:549
  31.8 6.8 %copy-start.14 = (s32[32]{0:T(128)S(1)}, s32[32]{0:T(128)}, u32[]{:S(2)}) copy-start(s32[32]{0:T(128)} %lengths_ref.7) | copy-start | bytes 388
  35.3 13.5 %all-to-all-start.5 = ((bf16[4,24,384]{2,1,0:T(8,128)(2,1)}), bf16[4,24,384]{2,1,0:T(8,128)(2,1)S(1)}, u32[]{:S(2)}, u32[]{:S(2)}) async-start(bf16[4,24,384]{2,1,0:T(8,128)(2,1)} %shard_map.149), calls=%async_computation.5 | async-start | bytes 147456 | tf_op jit(solution)/shard_map/all_to_all | solution.py:566
  38.6 10.2 %copy-start.12 = (f32[2,256]{1,0:T(2,128)S(1)}, f32[2,256]{1,0:T(2,128)}, u32[]{:S(2)}) copy-start(f32[2,256]{1,0:T(2,128)} %decay_ref.7) | copy-start | bytes 6148
  38.6 10.2 %copy-start.13 = (f32[2,256]{1,0:T(2,128)S(1)}, f32[2,256]{1,0:T(2,128)}, u32[]{:S(2)}) copy-start(f32[2,256]{1,0:T(2,128)} %rate_ref.7) | copy-start | bytes 6148
  38.6 10.2 %copy-start.15 = (f32[2,256]{1,0:T(2,128)S(1)}, f32[2,256]{1,0:T(2,128)}, u32[]{:S(2)}) copy-start(f32[2,256]{1,0:T(2,128)} %gain_ref.7) | copy-start | bytes 6148
  41.4 13.0 %collective-permute-start.13 = (bf16[32,4224]{1,0:T(8,128)(2,1)S(1)}, bf16[32,4224]{1,0:T(8,128)(2,1)S(1)}, u32[]{:S(2)}, u32[]{:S(2)}) collective-permute-start(bf16[32,4224]{1,0:T(8,128)(2,1)S(1)} %collective-permute-done.12.refs_6_), channel_id=1, source_target_pairs={{0,1},{1,0},{2,3},{3,2},{4,5},{5,4},{6,7},{7,6},{8,9},{9,8},{10,11... | collective-permute-start | bytes 811016 | tf_op jit(solution)/shard_map/ppermute | solution.py:549
  48.3 6.2 %collective-permute-start.11 = (bf16[32,4224]{1,0:T(8,128)(2,1)S(1)}, bf16[32,4224]{1,0:T(8,128)(2,1)S(1)}, u32[]{:S(2)}, u32[]{:S(2)}) collective-permute-start(bf16[32,4224]{1,0:T(8,128)(2,1)S(1)} %collective-permute-done.10.refs_4_), channel_id=1, source_target_pairs={{0,1},{1,0},{2,3},{3,2},{4,5},{5,4},{6,7},{7,6},{8,9},{9,8},{10,11... | collective-permute-start | bytes 811016 | tf_op jit(solution)/shard_map/ppermute | solution.py:549
  48.4 6.1 %collective-permute-start.9 = (bf16[32,4224]{1,0:T(8,128)(2,1)S(1)}, bf16[32,4224]{1,0:T(8,128)(2,1)}, u32[]{:S(2)}, u32[]{:S(2)}) collective-permute-start(bf16[32,4224]{1,0:T(8,128)(2,1)S(1)} %collective-permute-done.8.refs_2_), channel_id=1, source_target_pairs={{0,1},{1,0},{2,3},{3,2},{4,5},{5,4},{6,7},{7,6},{8,9},{9,8},{10,11... | collective-permute-start | bytes 811016 | tf_op jit(solution)/shard_map/ppermute | solution.py:549
  50.7 10.7 %all-to-all-start.6 = ((bf16[16,24,256]{2,1,0:T(8,128)(2,1)}), bf16[16,24,256]{2,1,0:T(8,128)(2,1)S(1)}, u32[]{:S(2)}, u32[]{:S(2)}) async-start(bf16[16,24,256]{2,1,0:T(8,128)(2,1)} %get-tuple-element.440), calls=%async_computation.6 | async-start | bytes 393216 | tf_op jit(solution)/shard_map/all_to_all | solution.py:570
  54.4 9.7 %copy-start.1 = (bf16[2,4096,32]{1,2,0:T(8,128)(2,1)S(1)}, bf16[2,4096,32]{1,2,0:T(8,128)(2,1)}, u32[]{:S(2)}) copy-start(bf16[2,4096,32]{1,2,0:T(8,128)(2,1)} %param.21) | copy-start | bytes 1572868
  54.4 9.7 %copy-start.3 = (bf16[2,4096,32]{1,2,0:T(8,128)(2,1)S(1)}, bf16[2,4096,32]{1,2,0:T(8,128)(2,1)}, u32[]{:S(2)}) copy-start(bf16[2,4096,32]{1,2,0:T(8,128)(2,1)} %param.22) | copy-start | bytes 1572868
  54.4 9.7 %copy-start.11 = (f32[2,4096]{1,0:T(2,128)S(1)}, f32[2,4096]{1,0:T(2,128)}, u32[]{:S(2)}) copy-start(f32[2,4096]{1,0:T(2,128)} %gain_ref.6) | copy-start | bytes 98308
  64.9 30.6 %all-to-all-start.7 = ((bf16[64,24,256]{2,1,0:T(8,128)(2,1)}), bf16[64,24,256]{2,1,0:T(8,128)(2,1)S(1)}, u32[]{:S(2)}, u32[]{:S(2)}) async-start(bf16[64,24,256]{2,1,0:T(8,128)(2,1)} %get-tuple-element.442), calls=%async_computation.7 | async-start | bytes 1572864 | tf_op jit(solution)/shard_map/all_to_all | solution.py:579
  72.1 14.2 %collective-permute-start.19 = (bf16[32,4096]{1,0:T(8,128)(2,1)S(1)}, bf16[32,4096]{1,0:T(8,128)(2,1)S(1)}, u32[]{:S(2)}, u32[]{:S(2)}) collective-permute-start(bf16[32,4096]{1,0:T(8,128)(2,1)S(1)} %get-tuple-element.565.refs_0_), channel_id=1, source_target_pairs={{0,6},{2,0},{4,2},{6,4},{1,7},{3,1},{5,3},{7,5},{8,14},{10,8},{12,... | collective-permute-start | bytes 786440 | tf_op jit(solution)/shard_map/ppermute | solution.py:544
  74.4 16.2 %collective-permute-start.17 = (bf16[32,4096]{1,0:T(8,128)(2,1)S(1)}, bf16[32,4096]{1,0:T(8,128)(2,1)S(1)}, u32[]{:S(2)}, u32[]{:S(2)}) collective-permute-start(bf16[32,4096]{1,0:T(8,128)(2,1)S(1)} %get-tuple-element.565.refs_0_), channel_id=1, source_target_pairs={{0,4},{2,6},{4,0},{6,2},{1,5},{3,7},{5,1},{7,3},{8,12},{10,14},{12... | collective-permute-start | bytes 786440 | tf_op jit(solution)/shard_map/ppermute | solution.py:544
  74.9 18.9 %collective-permute-start.15 = (bf16[32,4096]{1,0:T(8,128)(2,1)S(1)}, bf16[32,4096]{1,0:T(8,128)(2,1)S(1)}, u32[]{:S(2)}, u32[]{:S(2)}) collective-permute-start(bf16[32,4096]{1,0:T(8,128)(2,1)S(1)} %get-tuple-element.565.refs_0_), channel_id=1, source_target_pairs={{0,2},{2,4},{4,6},{6,0},{1,3},{3,5},{5,7},{7,1},{8,10},{10,12},{12... | collective-permute-start | bytes 786440 | tf_op jit(solution)/shard_map/ppermute | solution.py:544
  75.5 46.5 %collective-permute-start.14 = (bf16[32,4096]{1,0:T(8,128)(2,1)S(1)}, bf16[32,4096]{1,0:T(8,128)(2,1)S(1)}, u32[]{:S(2)}, u32[]{:S(2)}) collective-permute-start(bf16[32,4096]{1,0:T(8,128)(2,1)S(1)} %get-tuple-element.565.refs_0_), channel_id=1, source_target_pairs={{0,1},{1,0},{2,3},{3,2},{4,5},{5,4},{6,7},{7,6},{8,9},{9,8},{10,11... | collective-permute-start | bytes 786440 | tf_op jit(solution)/shard_map/ppermute | solution.py:549
  86.3 35.8 %collective-permute-start.20 = (bf16[32,4096]{1,0:T(8,128)(2,1)S(1)}, bf16[32,4096]{1,0:T(8,128)(2,1)S(1)}, u32[]{:S(2)}, u32[]{:S(2)}) collective-permute-start(bf16[32,4096]{1,0:T(8,128)(2,1)S(1)} %collective-permute-done.19.refs_6_), channel_id=1, source_target_pairs={{0,1},{1,0},{2,3},{3,2},{4,5},{5,4},{6,7},{7,6},{8,9},{9,8},{10,11... | collective-permute-start | bytes 786440 | tf_op jit(solution)/shard_map/ppermute | solution.py:549
  90.6 31.5 %collective-permute-start.18 = (bf16[32,4096]{1,0:T(8,128)(2,1)S(1)}, bf16[32,4096]{1,0:T(8,128)(2,1)S(1)}, u32[]{:S(2)}, u32[]{:S(2)}) collective-permute-start(bf16[32,4096]{1,0:T(8,128)(2,1)S(1)} %collective-permute-done.17.refs_4_), channel_id=1, source_target_pairs={{0,1},{1,0},{2,3},{3,2},{4,5},{5,4},{6,7},{7,6},{8,9},{9,8},{10,11... | collective-permute-start | bytes 786440 | tf_op jit(solution)/shard_map/ppermute | solution.py:549
  93.9 28.2 %collective-permute-start.16 = (bf16[32,4096]{1,0:T(8,128)(2,1)S(1)}, bf16[32,4096]{1,0:T(8,128)(2,1)}, u32[]{:S(2)}, u32[]{:S(2)}) collective-permute-start(bf16[32,4096]{1,0:T(8,128)(2,1)S(1)} %collective-permute-done.15.refs_2_), channel_id=1, source_target_pairs={{0,1},{1,0},{2,3},{3,2},{4,5},{5,4},{6,7},{7,6},{8,9},{9,8},{10,11... | collective-permute-start | bytes 786440 | tf_op jit(solution)/shard_map/ppermute | solution.py:549
  99.1 8.8 %all-to-all-start.8 = ((bf16[4,24,384]{2,1,0:T(8,128)(2,1)}), bf16[4,24,384]{2,1,0:T(8,128)(2,1)S(1)}, u32[]{:S(2)}, u32[]{:S(2)}) async-start(bf16[4,24,384]{2,1,0:T(8,128)(2,1)} %shard_map.152), calls=%async_computation.8 | async-start | bytes 147456 | tf_op jit(solution)/shard_map/all_to_all | solution.py:566
  102.4 5.5 %copy-start.16 = (f32[2,256]{1,0:T(2,128)S(1)}, f32[2,256]{1,0:T(2,128)}, u32[]{:S(2)}) copy-start(f32[2,256]{1,0:T(2,128)} %gain_ref.7) | copy-start | bytes 6148
  109.9 13.9 %all-to-all-start.9 = ((bf16[16,24,256]{2,1,0:T(8,128)(2,1)}), bf16[16,24,256]{2,1,0:T(8,128)(2,1)S(1)}, u32[]{:S(2)}, u32[]{:S(2)}) async-start(bf16[16,24,256]{2,1,0:T(8,128)(2,1)} %get-tuple-element.443), calls=%async_computation.9 | async-start | bytes 393216 | tf_op jit(solution)/shard_map/all_to_all | solution.py:570
